TPU v7x, 512 devices: a whole 4x4x16 slice. The times are simulated.
512 devices in a mesh: ep: 32 (over z, core), tp: 16 (over y, x).
Axes of the slice: x: 4, y: 4, z: 16, core: 2. Of those that a mesh axis runs over, the one named last changes fastest.
Arguments:
- attn_rows: bfloat16 [4096, 2048], P('ep'), may hold values from -6 to 6
- attn_gain: float32 [2048], replicated, may hold values from 0.1 to 1.9
- query_weight: bfloat16 [2048, 1024], P(None, 'tp'), may hold values from -0.125 to 0.125
- key_weight: bfloat16 [2048, 1024], P(None, 'tp'), may hold values from -0.125 to 0.125
- value_weight: bfloat16 [2048, 1024], P(None, 'tp'), may hold values from -0.125 to 0.125
- key_bias: bfloat16 [16, 4096], P('tp', 'ep'), may hold values from -14 to 0
- out_weight: bfloat16 [1024, 2048], P(None, 'tp'), may hold values from -0.75 to 0.75
- expert_rows: bfloat16 [4096, 2048], P('ep'), may hold values from -6 to 6
- expert_gain: float32 [2048], replicated, may hold values from 0.1 to 1.9
- expert_ids: int32 [4096, 2], P('ep'), may hold values from 0 to 31, all different within a row; in each aligned block of 128 rows (0 to 127, 128 to 255, ...) at most 16 rows name the same one
- group_logits: float32 [4096, 4], P('ep'), may hold values from -6 to 6
- pair_logits: float32 [4096, 2], P('ep'), may hold values from -6 to 6
- gate_weight: bfloat16 [32, 2048, 2048], P('ep', None, 'tp'), may hold values from -0.125 to 0.125
- up_weight: bfloat16 [32, 2048, 2048], P('ep', None, 'tp'), may hold values from -0.125 to 0.125
- down_weight: bfloat16 [32, 2048, 2048], P('ep', None, 'tp'), may hold values from -0.125 to 0.125
Outputs:
- mixed: bfloat16 [4096, 2048], P('ep', 'tp')
- expert_out: bfloat16 [4096, 2048], P('ep', 'tp')
Inputs may be any that keep to these rules, and one draw needn't show every extreme that they name: `expert_ids`: each row names two different experts; in every aligned block of 128 rows no expert is named more than 16 times.
All inputs are finite; a program needn't handle non-finite values.
Results may differ from a plain program's by a relative error of at most 0.0083.
Values may be sent and summed in bfloat16 or wider, within the bound.
No kernel may reach another device: no remote copies, remote signals or barrier semaphores. Data moves between devices by JAX's collectives and lax.ppermute only.
A program may use at most 64 MiB of HBM per device.

v0:
```python
import jax
import jax.numpy as jnp
from jax import lax
from jax.sharding import PartitionSpec as P

EXPERTS = 32
GROUPS = 4
GROUP_SIZE = 8
CAP = 16


epsilon = 1e-06


def sent_together(arrays, axis, dim, along):
    widths = [a.shape[along] for a in arrays]
    both = jnp.concatenate(arrays, axis=along)
    filled = lax.all_gather(both, axis, axis=dim, tiled=True)
    return tuple(jnp.split(filled, [sum(widths[:k]) for k in range(1, len(widths))], axis=along))


def laid_out(tiles, dim):
    lengths = list(tiles.shape[1:])
    lengths[dim] *= tiles.shape[0]
    return jnp.moveaxis(tiles, 0, dim).reshape(lengths)


def sent_to_all(shard, axis):
    copies = jnp.broadcast_to(shard, (lax.axis_size(axis), *shard.shape))
    return lax.all_to_all(copies, axis, split_axis=0, concat_axis=0, tiled=True)


def collect(shard, axis, dim):
    return laid_out(sent_to_all(shard, axis), dim)


def norm_rows(rows, gain):
    values = rows.astype(jnp.float32)
    scaled = values * lax.rsqrt(jnp.mean(values * values, axis=-1, keepdims=True) + epsilon)
    return (scaled * gain).astype(jnp.bfloat16)


def shards(
    attn_rows,
    attn_gain,
    query_weight,
    key_weight,
    value_weight,
    key_bias,
    out_weight,
    expert_rows,
    expert_gain,
    expert_ids,
    group_logits,
    pair_logits,
    gate_weight,
    up_weight,
    down_weight,
):
    rows_dev = attn_rows.shape[0]
    blocks = lax.axis_size("ep")
    own_start = lax.axis_index("ep") * rows_dev
    heads_local = key_bias.shape[0]
    head_size = query_weight.shape[1] // heads_local
    width_local = heads_local * head_size
    scale = head_size ** (-0.5)
    normed = norm_rows(attn_rows, attn_gain)
    query = jnp.dot(normed, query_weight, preferred_element_type=jnp.float32).astype(jnp.bfloat16)
    query = query.reshape(rows_dev, heads_local, head_size)
    keys = jnp.dot(normed, key_weight, preferred_element_type=jnp.float32).astype(jnp.bfloat16)
    values = jnp.dot(normed, value_weight, preferred_element_type=jnp.float32).astype(jnp.bfloat16)
    pairs = jnp.concatenate([keys, values], axis=1)
    bias_rows = key_bias.T
    query_pos = own_start + jnp.arange(rows_dev)
    init = (
        jnp.zeros((blocks, heads_local, rows_dev), jnp.float32),
        jnp.zeros((blocks, heads_local, rows_dev, head_size), jnp.float32),
    )
    piece = sent_together((pairs, bias_rows), "ep", 0, 1)

    def work(state):
        pair_rows, bias_piece = piece
        count = pair_rows.shape[0]
        spans = count // rows_dev
        key_part = pair_rows[:, :width_local].reshape(count, heads_local, head_size)
        value_part = pair_rows[:, width_local:].reshape(spans, rows_dev, heads_local, head_size)
        scores = (
            jnp.einsum("thd,shd->hts", query, key_part, preferred_element_type=jnp.float32) * scale
        )
        scores = scores + bias_piece.T.astype(jnp.float32)[:, None, :]
        scores = scores.reshape(heads_local, rows_dev, spans, rows_dev)
        causal = jnp.arange(count)[None, :] < query_pos[:, None]
        causal = causal.reshape(rows_dev, spans, rows_dev)
        negative_part = jax.nn.log_sigmoid(-scores)
        log_keep = jnp.where(causal, negative_part, 0.0)
        suffix = lax.cumsum(log_keep, axis=3, reverse=True) - log_keep
        weights = jnp.where(causal, jnp.exp(scores + negative_part + suffix), 0.0).astype(
            jnp.bfloat16
        )
        block_out = jnp.einsum(
            "htnr,nrhd->nhtd", weights, value_part, preferred_element_type=jnp.float32
        )
        block_keep = jnp.transpose(jnp.sum(log_keep, axis=3), (2, 0, 1))
        return (block_keep, block_out)

    def untouched(state):
        return state

    totals, outputs = lax.cond(jnp.int32(0) < own_start + rows_dev, work, untouched, init)
    later = lax.cumsum(totals, axis=0, reverse=True) - totals
    merged = jnp.sum(jnp.exp(later)[..., None] * outputs, axis=0)
    attended = jnp.transpose(merged, (1, 0, 2)).reshape(rows_dev, width_local).astype(jnp.bfloat16)
    mixed = jnp.dot(
        lax.all_gather(attended, "tp", axis=1, tiled=True),
        out_weight,
        preferred_element_type=jnp.float32,
    )
    mixed = mixed.astype(jnp.bfloat16)
    normed = norm_rows(expert_rows, expert_gain)
    width = normed.shape[1]
    cols_local = down_weight.shape[2]
    flattened = expert_ids.reshape(-1)
    picks = flattened.shape[0]
    marks = (flattened[:, None] == jnp.arange(EXPERTS)[None, :]).astype(jnp.int32)
    position = jnp.sum((jnp.cumsum(marks, axis=0) - marks) * marks, axis=1)
    source = jnp.arange(picks) // 2
    send = (
        jnp.zeros((EXPERTS, CAP, width), jnp.bfloat16).at[flattened, position].set(normed[source])
    )
    send = send.reshape(blocks, EXPERTS // blocks, CAP, width)
    shares = jnp.exp(group_logits)
    shares = shares / jnp.sum(shares, axis=1, keepdims=True)
    groups = expert_ids // GROUP_SIZE
    group_marks = (groups[:, :, None] == jnp.arange(GROUPS)[None, None, :]).astype(jnp.float32)
    chosen = jnp.sum(shares[:, None, :] * group_marks, axis=2)
    spread = pair_logits[:, 0] - pair_logits[:, 1]
    pair_share = jnp.stack([jax.nn.sigmoid(spread), jax.nn.sigmoid(-spread)], axis=1)
    route_weights = chosen * pair_share
    narrow = lax.dynamic_slice_in_dim(send, lax.axis_index("tp") * cols_local, cols_local, 3)
    add_piece = collect(
        lax.all_to_all(narrow, "ep", split_axis=0, concat_axis=0, tiled=True), "tp", 3
    )
    gate = jnp.einsum("secd,edf->secf", add_piece, gate_weight, preferred_element_type=jnp.float32)
    up = jnp.einsum("secd,edf->secf", add_piece, up_weight, preferred_element_type=jnp.float32)
    hidden = (jax.nn.silu(gate) * up).astype(jnp.bfloat16)
    result = jnp.einsum(
        "secf,efd->secd", collect(hidden, "tp", 3), down_weight, preferred_element_type=jnp.float32
    ).astype(jnp.bfloat16)
    back = lax.all_to_all(result, "ep", split_axis=0, concat_axis=0, tiled=True).reshape(
        EXPERTS, CAP, cols_local
    )
    picked = back[flattened, position].reshape(expert_rows.shape[0], 2, cols_local)
    combined = jnp.sum(route_weights[:, :, None] * picked.astype(jnp.float32), axis=1)
    expert_out = combined.astype(jnp.bfloat16)
    return (mixed, expert_out)


def solution(mesh):
    placed = (
        P("ep", None),
        P(),
        P(None, "tp"),
        P(None, "tp"),
        P(None, "tp"),
        P("tp", "ep"),
        P(None, "tp"),
        P("ep", None),
        P(),
        P("ep", None),
        P("ep", None),
        P("ep", None),
        P("ep", None, "tp"),
        P("ep", None, "tp"),
        P("ep", None, "tp"),
    )
    return jax.shard_map(
        shards,
        mesh=mesh,
        in_specs=placed,
        out_specs=(P("ep", "tp"), P("ep", "tp")),
        check_vma=False,
    )
```

profile of v0, /device:TPU:6, one launch (start us, length us, event | category | flops | bytes accessed | tf_op | source)
XLA Modules:
  0.0 225.1 jit_solution(5643384250437827587)
XLA Ops:
  11.9 2.3 %gather_fusion = bf16[256,2048]{1,0:T(8,128)(2,1)} fusion(bf16[128,2048]{1,0:T(8,128)(2,1)S(1)} %fusion.30, s32[1024]{0:T(1024)S(1)} %pad_clamp_fusion), kind=kCustom, calls=%fused_computation | custom fusion | bytes 2098176 | tf_op jit(solution)/shard_map/gather | solution.py:128
  14.5 33.3 %scatter_fusion = bf16[32,16,2048]{2,1,0:T(8,128)(2,1)S(1)} fusion(bf16[32,16,2048]{2,1,0:T(8,128)(2,1)S(1)} %broadcast_in_dim.21, s32[256]{0:T(256)S(1)} %bitcast.129, bf16[256,2048]{1,0:T(8,128)(2,1)} %gather_fusion), kind=kCustom, calls=%fused_computation.2 | custom fusion | bytes 3147776 | tf_op jit(solution)/shard_map/scatter | solution.py:128
  47.8 32.5 %all_to_all.23 = bf16[32,1,16,128]{3,2,1,0:T(8,128)(2,1)S(1)} all-to-all(bf16[32,1,16,128]{3,2,1,0:T(8,128)(2,1)S(1)} %dynamic-slice_bitcast_fusion), channel_id=1, replica_groups=mesh['ep'=32,'tp'=16] {'ep'}, dimensions={0} | all-to-all | bytes 262144 | tf_op jit(solution)/shard_map/all_to_all | solution.py:141
  80.3 1.8 broadcast_in_dim.22
  82.1 7.6 %all-to-all-start.1 = ((bf16[16,32,1,16,128]{4,3,1,2,0:T(8,128)(2,1)}), bf16[16,32,1,16,128]{4,3,1,2,0:T(8,128)(2,1)S(1)}, u32[]{:S(2)}, u32[]{:S(2)}) async-start(bf16[16,32,1,16,128]{4,3,1,2,0:T(8,128)(2,1)} %broadcast_in_dim.22), calls=%async_computation.1 | async-start | bytes 4194304 | tf_op jit(solution)/shard_map/all_to_all | solution.py:30
  92.3 22.4 %all-to-all-done.1 = bf16[16,32,1,16,128]{4,3,1,2,0:T(8,128)(2,1)S(1)} async-done(((bf16[16,32,1,16,128]{4,3,1,2,0:T(8,128)(2,1)}), bf16[16,32,1,16,128]{4,3,1,2,0:T(8,128)(2,1)S(1)}, u32[]{:S(2)}, u32[]{:S(2)}) %all-to-all-start.1) | async-done | bytes 2097184 | tf_op jit(solution)/shard_map/all_to_all | solution.py:30
  114.7 3.8 %copy.90 = bf16[32,1,16,16,128]{4,3,2,0,1:T(8,128)(2,1)} copy(bf16[32,1,16,16,128]{4,2,0,1,3:T(8,128)(2,1)S(1)} %bitcast.131) | data formatting | bytes 4194304 | tf_op jit(solution)/shard_map/transpose | solution.py:25
  118.5 2.8 %reshape.363 = bf16[32,16,2048]{2,1,0:T(8,128)(2,1)S(1)} reshape(bf16[32,1,16,16,128]{4,3,2,0,1:T(8,128)(2,1)} %copy.90) | data formatting | bytes 4194304 | tf_op jit(solution)/shard_map/reshape.28
  123.1 1.7 broadcast_in_dim.23
  124.8 9.2 %all-to-all-start.2 = ((bf16[16,32,1,16,128]{4,3,1,2,0:T(8,128)(2,1)}), bf16[16,32,1,16,128]{4,3,1,2,0:T(8,128)(2,1)}, u32[]{:S(2)}, u32[]{:S(2)}) async-start(bf16[16,32,1,16,128]{4,3,1,2,0:T(8,128)(2,1)} %broadcast_in_dim.23), calls=%async_computation.2 | async-start | bytes 4194304 | tf_op jit(solution)/shard_map/all_to_all | solution.py:30
  134.6 18.9 %all-gather.2.cloned.1.call-done = bf16[4096,129]{0,1:T(8,128)(2,1)} async-done(((bf16[128,129]{0,1:T(8,128)(2,1)}), bf16[4096,129]{0,1:T(8,128)(2,1)}) %all-gather.2.cloned.1.call-update) | async-done | bytes 1056784 | tf_op jit(solution)/shard_map/all_gather | solution.py:18
  153.5 19.2 %conditional.1 = (f32[32,1,128,64]{2,3,0,1:T(8,128)}, f32[32,1,128]{2,1,0:T(1,128)S(1)}) conditional(s32[]{:T(128)} %convert_element_type.82, () %tuple.16, (s32[]{:T(128)}, s32[128]{0:T(128)S(1)}, bf16[4096,129]{0,1:T(8,128)(2,1)}, bf16[128,64]{0,1:T(8,128)(2,1)S(1)}) %tuple.17), branch_computations={%region_1.0_spmd, %region_2.5_spmd} | conditional | flops 219160704 | bytes 19064852 | solution.py:109
  154.5 1.5 fusion.11
  156.4 1.4 fusion.4
  157.9 2.4 %copy.79 = f32[128,32,128]{0,1,2:T(8,128)} copy(f32[128,32,128]{2,1,0:T(8,128)S(1)} %bitcast.128) | data formatting | bytes 4194304 | tf_op jit(solution)/shard_map/cond/branch_1_fun/reshape | solution.py:91
  160.2 9.9 %fusion.1 = bf16[128,32,128]{0,1,2:T(8,128)(2,1)S(1)} fusion(f32[128,32,128]{0,1,2:T(8,128)} %copy.79, s32[128]{0:T(128)S(1)} %broadcast_add_fusion, s32[32,128]{0,1:T(8,128)S(1)} %multiply_add_fusion), kind=kOutput, calls=%fused_computation.9 | output fusion | flops 78643200 | bytes 3162624 | tf_op jit(solution)/shard_map/cond/branch_1_fun/reduce_window_sum | solution.py:96
  170.2 2.6 %convolution_bitcast_fusion = f32[32,1,128,64]{2,3,0,1:T(8,128)} fusion(bf16[128,32,128]{0,1,2:T(8,128)(2,1)S(1)} %fusion.1, bf16[4096,129]{0,1:T(8,128)(2,1)} %get-tuple-element.17), kind=kOutput, calls=%fused_computation.22 | convolution fusion | flops 67108864 | bytes 2621440 | tf_op jit(solution)/shard_map/cond/branch_1_fun/htnr,nrhd->nhtd/dot_general | solution.py:100
  172.8 4.0 %copy.91 = bf16[32,1,16,16,128]{4,3,2,0,1:T(8,128)(2,1)S(1)} copy(bf16[32,1,16,16,128]{4,2,0,1,3:T(8,128)(2,1)} %bitcast.26) | data formatting | bytes 4194304 | tf_op jit(solution)/shard_map/transpose | solution.py:25
  176.8 2.3 %reshape.366 = bf16[32,16,2048]{2,1,0:T(8,128)(2,1)} reshape(bf16[32,1,16,16,128]{4,3,2,0,1:T(8,128)(2,1)S(1)} %copy.91) | data formatting | bytes 4194304 | tf_op jit(solution)/shard_map/reshape.35
  179.1 3.0 %fusion.22 = bf16[32,1,16,128]{3,2,1,0:T(8,128)(2,1)} fusion(bf16[32,16,2048]{2,1,0:T(8,128)(2,1)} %reshape.366, bf16[1,2048,128]{2,1,0:T(8,128)(2,1)S(1)} %copy-done.2), kind=kOutput, calls=%fused_computation.44 | convolution fusion | flops 268500992 | bytes 2752512 | tf_op jit(solution)/shard_map/secf,efd->secd/dot_general | solution.py:146
  182.1 7.5 %all-to-all-start.3 = ((bf16[32,1,16,128]{3,2,1,0:T(8,128)(2,1)}), bf16[32,1,16,128]{3,2,1,0:T(8,128)(2,1)S(1)}, u32[]{:S(2)}, u32[]{:S(2)}) async-start(bf16[32,1,16,128]{3,2,1,0:T(8,128)(2,1)} %fusion.22), calls=%async_computation.3 | async-start | bytes 262144 | tf_op jit(solution)/shard_map/all_to_all | solution.py:149
  189.7 1.3 multiply_reduce_fusion
  191.0 23.8 %all_gather.7 = bf16[128,1024]{0,1:T(8,128)(2,1)S(1)} all-gather(bf16[128,64]{0,1:T(8,128)(2,1)S(1)} %multiply_reduce_fusion), channel_id=1, replica_groups=mesh['ep'=32,'tp'=16] {'tp'}, dimensions={1}, use_global_device_ids=true | all-gather | bytes 278528 | tf_op jit(solution)/shard_map/all_gather | solution.py:114
  215.7 1.7 gather_fusion.1
  (71 shorter events, 13.1 us)
Async XLA Ops:
  7.2 114.2 %copy-start = (bf16[1,2048,128]{2,1,0:T(8,128)(2,1)S(1)}, bf16[1,2048,128]{2,1,0:T(8,128)(2,1)}, u32[]{:S(2)}) copy-start(bf16[1,2048,128]{2,1,0:T(8,128)(2,1)} %param.29) | copy-start | bytes 1572868
  82.1 7.6 %copy-start.1 = (bf16[128,2048]{1,0:T(8,128)(2,1)S(1)}, bf16[128,2048]{1,0:T(8,128)(2,1)}, u32[]{:S(2)}) copy-start(bf16[128,2048]{1,0:T(8,128)(2,1)} %param.17) | copy-start | bytes 1572868
  82.1 7.8 %copy-start.9 = (bf16[2048,64]{0,1:T(8,128)(2,1)S(1)}, bf16[2048,64]{0,1:T(8,128)(2,1)}, u32[]{:S(2)}) copy-start(bf16[2048,64]{0,1:T(8,128)(2,1)} %param.21) | copy-start | bytes 786436
  82.1 7.8 %copy-start.11 = (f32[2048]{0:T(1024)S(1)}, f32[2048]{0:T(1024)}, u32[]{:S(2)}) copy-start(f32[2048]{0:T(1024)} %param.18) | copy-start | bytes 24580
  82.1 32.6 %all-to-all-start.1 = ((bf16[16,32,1,16,128]{4,3,1,2,0:T(8,128)(2,1)}), bf16[16,32,1,16,128]{4,3,1,2,0:T(8,128)(2,1)S(1)}, u32[]{:S(2)}, u32[]{:S(2)}) async-start(bf16[16,32,1,16,128]{4,3,1,2,0:T(8,128)(2,1)} %broadcast_in_dim.22), calls=%async_computation.1 | async-start | bytes 4194304 | tf_op jit(solution)/shard_map/all_to_all | solution.py:30
  89.6 2.0 copy-start.7
  89.7 63.9 %all-gather.2.cloned.1.call-start = ((), (), s32[]{:S(2)}) async-start(), calls=%async_computation.4 | async-start | bytes 1148928 | tf_op jit(solution)/shard_map/all_gather | solution.py:18
  121.3 1.0 copy-start.8
  124.8 9.2 %copy-start.4 = (f32[128,4]{0,1:T(4,128)S(1)}, f32[128,4]{0,1:T(4,128)}, u32[]{:S(2)}) copy-start(f32[128,4]{0,1:T(4,128)} %param.27) | copy-start | bytes 6148
  124.8 9.2 %copy-start.5 = (s32[128,2]{0,1:T(2,128)S(1)}, s32[128,2]{0,1:T(2,128)}, u32[]{:S(2)}) copy-start(s32[128,2]{0,1:T(2,128)} %param.26) | copy-start | bytes 3076
  124.8 9.3 %copy-start.6 = (f32[128,2]{0,1:T(2,128)S(1)}, f32[128,2]{0,1:T(2,128)}, u32[]{:S(2)}) copy-start(f32[128,2]{0,1:T(2,128)} %param.28) | copy-start | bytes 3076
  124.8 9.4 %copy-start.10 = (bf16[2048,64]{0,1:T(8,128)(2,1)S(1)}, bf16[2048,64]{0,1:T(8,128)(2,1)}, u32[]{:S(2)}) copy-start(bf16[2048,64]{0,1:T(8,128)(2,1)} %param.19) | copy-start | bytes 786436
  124.8 48.0 %all-to-all-start.2 = ((bf16[16,32,1,16,128]{4,3,1,2,0:T(8,128)(2,1)}), bf16[16,32,1,16,128]{4,3,1,2,0:T(8,128)(2,1)}, u32[]{:S(2)}, u32[]{:S(2)}) async-start(bf16[16,32,1,16,128]{4,3,1,2,0:T(8,128)(2,1)} %broadcast_in_dim.23), calls=%async_computation.2 | async-start | bytes 4194304 | tf_op jit(solution)/shard_map/all_to_all | solution.py:30
  176.8 2.3 %copy-start.2 = (bf16[1,2048,128]{2,1,0:T(8,128)(2,1)S(1)}, bf16[1,2048,128]{2,1,0:T(8,128)(2,1)}, u32[]{:S(2)}) copy-start(bf16[1,2048,128]{2,1,0:T(8,128)(2,1)} %param.31) | copy-start | bytes 1572868
  179.1 35.7 %copy-start.3 = (bf16[1024,128]{1,0:T(8,128)(2,1)S(1)}, bf16[1024,128]{1,0:T(8,128)(2,1)}, u32[]{:S(2)}) copy-start(bf16[1024,128]{1,0:T(8,128)(2,1)} %param.23) | copy-start | bytes 786436
  182.1 33.6 %all-to-all-start.3 = ((bf16[32,1,16,128]{3,2,1,0:T(8,128)(2,1)}), bf16[32,1,16,128]{3,2,1,0:T(8,128)(2,1)S(1)}, u32[]{:S(2)}, u32[]{:S(2)}) async-start(bf16[32,1,16,128]{3,2,1,0:T(8,128)(2,1)} %fusion.22), calls=%async_computation.3 | async-start | bytes 262144 | tf_op jit(solution)/shard_map/all_to_all | solution.py:149
Sparse Core Ops, SparseCore 0:
  92.5 60.9 all-gather.1
where the time goes:
time: 227 us; the launch traced here: 225 us
  local copies, waits for them, and re-layouts  58.8 us (26%)
  blocking collectives  56.3 us (25%)
  waiting for transfers between devices  41.3 us (18%)
  starting transfers between devices  24.2 us (11%)
  other arithmetic  18.6 us (8%)
  between operations  14.3 us (6%)
  matrix products  11.5 us (5%)
    scatter x1, local copies, waits for them, and re-layouts, shards(): jnp.zeros((EXPERTS, CAP, width), jnp.bfloat16).at[flattened, position]  33.3 us
    all_to_all x1, blocking collectives, shards(): lax.all_to_all(narrow, 'ep', split_axis=0, concat_axis=0, tiled=True)  32.5 us
    all_gather x1, blocking collectives, shards(): lax.all_gather(attended, 'tp', axis=1, tiled=True)  23.8 us
    all_to_all x2, waiting for transfers between devices, sent_to_all(): return lax.all_to_all(copies, axis, split_axis=0, concat_axis=0, tiled=True)  22.4 us
    all_gather x1, waiting for transfers between devices, sent_together(): filled = lax.all_gather(both, axis, axis=dim, tiled=True)  18.9 us
    all_to_all x2, starting transfers between devices, sent_to_all(): return lax.all_to_all(copies, axis, split_axis=0, concat_axis=0, tiled=True)  16.7 us
    another operation x1, other arithmetic, work(): suffix = lax.cumsum(log_keep, axis=3, reverse=True) - log_keep  9.92 us
    transpose x2, local copies, waits for them, and re-layouts, laid_out(): return jnp.moveaxis(tiles, 0, dim).reshape(lengths)  7.81 us
  transfers between devices with their start and end apart: 4, of which 2 were waited for; matrix products, arithmetic and copies ran while one was open for 15% of the time, Pallas kernels for 0%

commit v1 on v0

v1 whole, which is shorter than its diff:
```python
import jax
import jax.numpy as jnp
from jax import lax
from jax.experimental import pallas as pl
from jax.experimental.pallas import tpu as pltpu
from jax.sharding import PartitionSpec as P


EXPERTS = 32
GROUPS = 4
GROUP_SIZE = 8
CAP = 16
BLOCK = 128
HEAD = 64
SLOTS = EXPERTS * CAP
MSG = 144

epsilon = 1e-06
f32 = jnp.float32
bf16 = jnp.bfloat16
i32 = jnp.int32

SMEM = pl.BlockSpec(memory_space=pltpu.SMEM)


def call(body, n_scalar, n_in, outs, flops, mib=16):
    return pl.pallas_call(
        body,
        out_shape=outs,
        in_specs=[SMEM] * n_scalar + [pl.BlockSpec()] * n_in,
        cost_estimate=pl.CostEstimate(flops=flops, bytes_accessed=1 << 20, transcendentals=0),
        compiler_params=pltpu.CompilerParams(vmem_limit_bytes=mib << 20),
    )


def nn(a, b):
    return lax.dot_general(a, b, (((1,), (0,)), ((), ())), preferred_element_type=f32)


def nt(a, b):
    return lax.dot_general(a, b, (((1,), (1,)), ((), ())), preferred_element_type=f32)


def iota(shape, dim):
    return lax.broadcasted_iota(i32, shape, dim)


def ones_where(mask):
    return jnp.where(mask, 1.0, 0.0).astype(f32)


def places(first, second):
    expert = iota((EXPERTS, BLOCK), 0)
    mark0 = ones_where(first == expert)
    mark1 = ones_where(second == expert)
    earlier = ones_where(iota((BLOCK, BLOCK), 0) < iota((BLOCK, BLOCK), 1)).astype(bf16)
    before = nn((mark0 + mark1).astype(bf16), earlier)
    place0 = jnp.sum(mark0 * before, axis=0, keepdims=True)
    place1 = jnp.sum(mark1 * before, axis=0, keepdims=True)
    return place0.astype(i32), place1.astype(i32)


def dispatch_body(tp_ref, rows_ref, gain_ref, ids_ref, out_ref):
    x = rows_ref[...].astype(f32)
    inv = lax.rsqrt(jnp.mean(x * x, axis=-1, keepdims=True) + epsilon)
    at = pl.multiple_of(tp_ref[0] * BLOCK, BLOCK)
    own = rows_ref[:, pl.ds(at, BLOCK)].astype(f32)
    own = (own * inv * gain_ref[:, pl.ds(at, BLOCK)]).astype(bf16)
    ids = ids_ref[...]
    first, second = ids[0:1, :], ids[1:2, :]
    place0, place1 = places(first, second)
    slot = iota((SLOTS, BLOCK), 0)
    hit = (slot == first * CAP + place0) | (slot == second * CAP + place1)
    out_ref[...] = nn(ones_where(hit).astype(bf16), own).astype(bf16)


def project_body(rows_ref, gain_ref, wq_ref, wk_ref, wv_ref, bias_ref, q_ref, msg_ref):
    x = rows_ref[...].astype(f32)
    inv = lax.rsqrt(jnp.mean(x * x, axis=-1, keepdims=True) + epsilon)
    normed = (x * inv * gain_ref[...]).astype(bf16)
    q = nt(normed, wq_ref[...]).astype(bf16)
    q_ref[...] = (q.astype(f32) * (HEAD**-0.5)).astype(bf16)
    kv = jnp.concatenate([wk_ref[...], wv_ref[...]], axis=0)
    msg_ref[0:BLOCK, :] = nt(kv, normed).astype(bf16)
    msg_ref[BLOCK:MSG, :] = jnp.broadcast_to(bias_ref[...], (MSG - BLOCK, BLOCK))


def copies_body(x_ref, out_ref):
    x = x_ref[...]
    for k in range(out_ref.shape[0]):
        out_ref[k] = x


def hidden_body(x_ref, gate_ref, up_ref, out_ref):
    parts = x_ref.shape[0]
    weights = jnp.concatenate([gate_ref[...], up_ref[...]], axis=1)
    rows = 256
    for m in range(SLOTS // rows):
        span = slice(m * rows, (m + 1) * rows)
        x = jnp.concatenate([x_ref[k, span, :] for k in range(parts)], axis=1)
        both = nn(x, weights)
        gate, up = both[:, :BLOCK], both[:, BLOCK:]
        hidden = (gate * jax.nn.sigmoid(gate) * up).astype(bf16)
        for k in range(parts):
            out_ref[k, span, :] = hidden


def down_body(x_ref, w_ref, out_ref):
    parts = x_ref.shape[0]
    rows = 256
    for m in range(SLOTS // rows):
        span = slice(m * rows, (m + 1) * rows)
        x = jnp.concatenate([x_ref[k, span, :] for k in range(parts)], axis=1)
        out_ref[span, :] = nn(x, w_ref[...]).astype(bf16)


def attend_body(pos_ref, q_ref, own_ref, other_ref, out_ref):
    here = pos_ref[0]
    core = here % 2
    chips = own_ref.shape[0] // MSG
    q = q_ref[...]
    wide = (2 * BLOCK, 2 * BLOCK)
    row, col = iota(wide, 0), iota(wide, 1)
    row = jnp.where(row >= BLOCK, row - BLOCK, row)
    tail = ones_where((col >= BLOCK) | (row >= col)).astype(bf16)
    t, s = iota((BLOCK, BLOCK), 0), iota((BLOCK, BLOCK), 1)

    def block(msg, number, later, total):
        scores = nn(q, msg[0:HEAD, :]) + msg[BLOCK : BLOCK + 1, :].astype(f32)
        causal = s + (number - here) * BLOCK < t
        keep = -(jnp.maximum(scores, 0.0) + jnp.log1p(jnp.exp(-jnp.abs(scores))))
        keep = jnp.where(causal, keep, 0.0)
        high = keep.astype(bf16)
        low = (keep - high.astype(f32)).astype(bf16)
        sums = nn(jnp.concatenate([high, low], axis=1), tail)
        weights = jnp.where(causal, jnp.exp(scores + sums[:, :BLOCK]), 0.0).astype(bf16)
        out = nt(weights, msg[HEAD:BLOCK, :])
        total = total + jnp.exp(later) * out
        return later + sums[:, BLOCK : BLOCK + HEAD], total

    def chip(k, carry):
        later, total = carry
        z = chips - 1 - k
        at = pl.multiple_of(z * MSG, MSG)
        own = own_ref[pl.ds(at, MSG), :]
        other = other_ref[pl.ds(at, MSG), :]
        upper = jnp.where(core == 1, own, other)
        lower = jnp.where(core == 1, other, own)
        later, total = block(upper, 2 * z + 1, later, total)
        return block(lower, 2 * z, later, total)

    zeros = jnp.zeros((BLOCK, HEAD), f32)
    _, total = lax.fori_loop(0, chips, chip, (zeros, zeros), unroll=2)
    out_ref[...] = jnp.transpose(total).astype(bf16)


def mix_body(x_ref, w_ref, out_ref):
    x = jnp.transpose(x_ref[...].astype(f32)).astype(bf16)
    out_ref[...] = nn(x, w_ref[...]).astype(bf16)


def combine_body(ids_ref, group_ref, pair_ref, back_ref, out_ref):
    ids = ids_ref[...]
    first, second = ids[0:1, :], ids[1:2, :]
    place0, place1 = places(first, second)
    shares = jnp.exp(group_ref[...])
    shares = shares / jnp.sum(shares, axis=0, keepdims=True)
    group = iota((GROUPS, BLOCK), 0)
    chosen0 = jnp.sum(jnp.where(first // GROUP_SIZE == group, shares, 0.0), axis=0, keepdims=True)
    chosen1 = jnp.sum(jnp.where(second // GROUP_SIZE == group, shares, 0.0), axis=0, keepdims=True)
    spread = pair_ref[0:1, :] - pair_ref[1:2, :]
    weight0 = chosen0 * jax.nn.sigmoid(spread)
    weight1 = chosen1 * jax.nn.sigmoid(-spread)
    slots = [(first * CAP + place0).astype(f32), (second * CAP + place1).astype(f32)]
    table = jnp.concatenate(slots + [weight0, weight1], axis=0)
    table = jnp.concatenate([table, jnp.zeros((BLOCK - 4, BLOCK), f32)], axis=0)
    table = jnp.transpose(table)
    slot = iota((BLOCK, SLOTS), 1)
    back = back_ref[...]
    pick0 = nn(ones_where(slot == table[:, 0:1].astype(i32)).astype(bf16), back)
    pick1 = nn(ones_where(slot == table[:, 1:2].astype(i32)).astype(bf16), back)
    out_ref[...] = (table[:, 2:3] * pick0 + table[:, 3:4] * pick1).astype(bf16)


def shards(
    attn_rows,
    attn_gain,
    query_weight,
    key_weight,
    value_weight,
    key_bias,
    out_weight,
    expert_rows,
    expert_gain,
    expert_ids,
    group_logits,
    pair_logits,
    gate_weight,
    up_weight,
    down_weight,
):
    ep, tp = lax.axis_size("ep"), lax.axis_size("tp")
    chips = ep // 2
    here = lax.axis_index("ep")
    same_core = [[z * 2 + c for z in range(chips)] for c in range(2)]
    partner = [(e, e ^ 1) for e in range(ep)]
    struct = jax.ShapeDtypeStruct

    def exchange(x, axis):
        return lax.all_to_all(x, axis, split_axis=0, concat_axis=0, tiled=True)

    slots = struct((SLOTS, BLOCK), bf16)
    copies = struct((tp, SLOTS, BLOCK), bf16)
    square = struct((BLOCK, BLOCK), bf16)
    ids = expert_ids.T
    column = lax.axis_index("tp").reshape(1)
    send = call(dispatch_body, 1, 3, slots, 1 << 27)(
        column, expert_rows, expert_gain[None, :], ids
    )
    routed = exchange(send.reshape(ep, CAP, BLOCK), "ep").reshape(SLOTS, BLOCK)
    outs = (struct((BLOCK, HEAD), bf16), struct((MSG, BLOCK), bf16))
    query, message = call(project_body, 0, 6, outs, 1 << 28)(
        attn_rows,
        attn_gain[None, :],
        query_weight.T,
        key_weight.T,
        value_weight.T,
        key_bias,
    )
    routed = call(copies_body, 0, 1, copies, 1 << 24)(routed)
    routed = exchange(routed, "tp")
    own = lax.all_gather(message, "ep", axis=0, tiled=True, axis_index_groups=same_core)
    other = lax.ppermute(own, "ep", partner)
    hidden = call(hidden_body, 0, 3, copies, 1 << 29)(routed, gate_weight[0], up_weight[0])
    hidden = exchange(hidden, "tp")
    attended = call(attend_body, 1, 3, struct((HEAD, BLOCK), bf16), 1 << 30)(
        here.reshape(1), query, own, other
    )
    result = call(down_body, 0, 2, slots, 1 << 28)(hidden, down_weight[0])
    back = exchange(result.reshape(ep, CAP, BLOCK), "ep").reshape(SLOTS, BLOCK)
    attended = lax.all_gather(attended, "tp", axis=0, tiled=True)
    mixed = call(mix_body, 0, 2, square, 1 << 26)(attended, out_weight)
    expert_out = call(combine_body, 0, 4, square, 1 << 27)(
        ids, group_logits.T, pair_logits.T, back
    )
    return (mixed, expert_out)


def solution(mesh):
    placed = (
        P("ep", None),
        P(),
        P(None, "tp"),
        P(None, "tp"),
        P(None, "tp"),
        P("tp", "ep"),
        P(None, "tp"),
        P("ep", None),
        P(),
        P("ep", None),
        P("ep", None),
        P("ep", None),
        P("ep", None, "tp"),
        P("ep", None, "tp"),
        P("ep", None, "tp"),
    )
    return jax.shard_map(
        shards,
        mesh=mesh,
        in_specs=placed,
        out_specs=(P("ep", "tp"), P("ep", "tp")),
        check_vma=False,
    )
```

time: 227 us -> 157 us (0.69)
  blocking collectives: 56.3 us -> 118 us
  local copies, waits for them, and re-layouts: 58.8 us -> 5.69 us
  waiting for transfers between devices: 41.3 us -> 0.01 us
  other arithmetic: 18.6 us -> 0 us
  Pallas kernels: 0 us -> 17.7 us
  between operations: 14.3 us -> 0.84 us
  matrix products: 11.5 us -> 0 us
  starting transfers between devices: 24.2 us -> 14 us
    scatter x1 -> x0, local copies, waits for them, and re-layouts: 33.3 us -> none  [shards(): jnp.zeros((EXPERTS, CAP, width), jnp.bfloat16).at[flattened, position]]
    all_to_all x1 -> x2, blocking collectives: 32.5 us -> 64.7 us  [exchange(): return lax.all_to_all(x, axis, split_axis=0, concat_axis=0, tiled=True)]
    all_gather x1 -> x2, blocking collectives: 23.8 us -> 53.2 us  [the longest x1 29.8 us: shards(): lax.all_gather(message, 'ep', axis=0, tiled=True, axis_index_groups=same_...]
    all_to_all x3 -> x2, waiting for transfers between devices: 22.4 us -> 0.01 us  [exchange(): return lax.all_to_all(x, axis, split_axis=0, concat_axis=0, tiled=True)]
    all_gather x1 -> x0, waiting for transfers between devices: 18.9 us -> none  [sent_together(): filled = lax.all_gather(both, axis, axis=dim, tiled=True)]
    pallas_call x0 -> x8, Pallas kernels: none -> 17.7 us  [the longest x1 12.1 us: shards(): call(attend_body, 1, 3, struct((HEAD, BLOCK), bf16), 1 << 30)]
    all_to_all x3 -> x2, starting transfers between devices: 24.2 us -> 12.1 us  [exchange(): return lax.all_to_all(x, axis, split_axis=0, concat_axis=0, tiled=True)]
    dot_general x9 -> x0, matrix products: 11.5 us -> none  [the longest x1 3 us: shards(): jnp.einsum('secf,efd->secd', collect(hidden, 'tp', 3), down_weight, prefe...]
  transfers between devices with their start and end apart: 4 -> 3, of which waited for: 2 -> 0; matrix products, arithmetic and copies ran while one was open for 15% -> 0% of each run, Pallas kernels for 0% -> 10%
where the time goes in v1:
time: 157 us; the launch traced here: 156 us
  blocking collectives  118 us (75%)
  Pallas kernels  17.7 us (11%)
  starting transfers between devices  14 us (9%)
  local copies, waits for them, and re-layouts  5.69 us (4%)
    all_to_all x2, blocking collectives, exchange(): return lax.all_to_all(x, axis, split_axis=0, concat_axis=0, tiled=True)  64.7 us
    all_gather x1, blocking collectives, shards(): lax.all_gather(message, 'ep', axis=0, tiled=True, axis_index_groups=same_...  29.8 us
    all_gather x1, blocking collectives, shards(): attended = lax.all_gather(attended, 'tp', axis=0, tiled=True)  23.5 us
    pallas_call x1, Pallas kernels, shards(): call(attend_body, 1, 3, struct((HEAD, BLOCK), bf16), 1 << 30)  12.1 us
    all_to_all x2, starting transfers between devices, exchange(): return lax.all_to_all(x, axis, split_axis=0, concat_axis=0, tiled=True)  12.1 us
    unnamed x34, local copies, waits for them, and re-layouts  5.69 us
  transfers between devices with their start and end apart: 3, of which 0 were waited for; matrix products, arithmetic and copies ran while one was open for 0% of the time, Pallas kernels for 10%

profile of v1, /device:TPU:6, one launch (start us, length us, event | category | flops | bytes accessed | tf_op | source)
XLA Modules:
  0.0 156.2 jit_solution(14965823498808312465)
XLA Ops:
  0.6 1.0 copy-done.4
  1.7 0.7 copy-done.10
  2.4 0.7 copy-done.12
  3.1 0.4 shard_map.161
  3.4 32.5 %all_to_all.20 = bf16[32,16,128]{2,1,0:T(8,128)(2,1)S(1)} all-to-all(bf16[32,16,128]{2,1,0:T(8,128)(2,1)S(1)} %bitcast.20), channel_id=1, replica_groups=mesh['ep'=32,'tp'=16] {'ep'}, dimensions={0} | all-to-all | bytes 262144 | tf_op jit(solution)/shard_map/all_to_all | solution.py:210
  35.9 0.4 shard_map.162
  36.3 32.2 %all_to_all.21.x_ref = bf16[16,512,128]{2,1,0:T(8,128)(2,1)S(1)} all-to-all(bf16[16,512,128]{2,1,0:T(8,128)(2,1)S(1)} %shard_map.162), channel_id=1, replica_groups=mesh['ep'=32,'tp'=16] {'tp'}, dimensions={0} | all-to-all | bytes 4194304 | tf_op jit(solution)/shard_map/all_to_all | solution.py:210
  68.5 0.9 shard_map.163
  69.4 1.3 copy-done
  70.8 0.0 copy-start.5
  70.8 6.6 %all-to-all-start.2 = ((bf16[16,512,128]{2,1,0:T(8,128)(2,1)}), bf16[16,512,128]{2,1,0:T(8,128)(2,1)S(1)}, u32[]{:S(2)}, u32[]{:S(2)}) async-start(bf16[16,512,128]{2,1,0:T(8,128)(2,1)} %copy-done), calls=%async_computation.2 | async-start | bytes 4194304 | tf_op jit(solution)/shard_map/all_to_all | solution.py:210
  77.4 0.9 copy-done.7
  78.3 0.9 copy-done.8
  79.3 0.6 shard_map.158
  79.9 29.8 %all_gather.6.own_ref = bf16[2304,128]{1,0:T(8,128)(2,1)S(1)} all-gather(bf16[144,128]{1,0:T(8,128)(2,1)S(1)} %get-tuple-element.5), channel_id=1, replica_groups={{0,32,64,96,128,160,192,224,256,288,320,352,384,416,448,480},{16,48,80,..., dimensions={0}, use_global_device_ids=true | all-gather | bytes 626688 | tf_op jit(solution)/shard_map/all_gather | solution.py:232
  109.6 1.9 %collective-permute-start = (bf16[2304,128]{1,0:T(8,128)(2,1)S(1)}, bf16[2304,128]{1,0:T(8,128)(2,1)}, u32[]{:S(2)}, u32[]{:S(2)}) collective-permute-start(bf16[2304,128]{1,0:T(8,128)(2,1)S(1)} %all_gather.6.own_ref), channel_id=1, source_target_pairs={{0,16},{16,0},{32,48},{48,32},{64,80},{80,64},{96,112},{112,96},{1... | collective-permute-start | bytes 1769480 | tf_op jit(solution)/shard_map/ppermute | solution.py:233
  111.6 1.3 shard_map.164
  112.9 5.5 %all-to-all-start.3 = ((bf16[32,16,128]{2,1,0:T(8,128)(2,1)}), bf16[32,16,128]{2,1,0:T(8,128)(2,1)S(1)}, u32[]{:S(2)}, u32[]{:S(2)}) async-start(bf16[32,16,128]{2,1,0:T(8,128)(2,1)} %bitcast.15), calls=%async_computation.3 | async-start | bytes 262144 | tf_op jit(solution)/shard_map/all_to_all | solution.py:210
  118.5 0.0 copy-start.9
  118.5 0.0 copy-start.13
  118.5 12.1 %shard_map.159 = bf16[64,128]{1,0:T(8,128)(2,1)S(1)} custom-call(s32[1]{0:T(128)} %bitcast.pos_ref, bf16[128,64]{1,0:T(8,128)(2,1)S(1)} %get-tuple-element.4.q_ref, bf16[2304,128]{1,0:T(8,128)(2,1)S(1)} %all_gather.6.own_ref, bf16[2304,128]{1,0:T(8,128)(2,1)} %collective-permute-done.other_ref), custom_call_target="tpu_custom_call" | custom-call | flops 1073741824 | bytes 1048576 | tf_op jit(solution)/shard_map/pallas_call | solution.py:236
  130.7 23.5 %all_gather.7.x_ref = bf16[1024,128]{1,0:T(8,128)(2,1)S(1)} all-gather(bf16[64,128]{1,0:T(8,128)(2,1)S(1)} %shard_map.159), channel_id=1, replica_groups=mesh['ep'=32,'tp'=16] {'tp'}, dimensions={0}, use_global_device_ids=true | all-gather | bytes 278528 | tf_op jit(solution)/shard_map/all_gather | solution.py:241
  154.1 0.9 shard_map.160
  155.1 1.1 shard_map.165
  (28 shorter events, 0.1 us)
Async XLA Ops:
  0.6 1.0 copy-start.4
  1.7 0.7 copy-start.10
  2.4 0.7 copy-start.12
  36.3 32.2 %copy-start.1 = (bf16[1,2048,128]{2,1,0:T(8,128)(2,1)S(1)}, bf16[1,2048,128]{2,1,0:T(8,128)(2,1)}, u32[]{:S(2)}) copy-start(bf16[1,2048,128]{2,1,0:T(8,128)(2,1)} %param.27) | copy-start | bytes 1572868
  36.3 32.2 %copy-start.2 = (bf16[1,2048,128]{2,1,0:T(8,128)(2,1)S(1)}, bf16[1,2048,128]{2,1,0:T(8,128)(2,1)}, u32[]{:S(2)}) copy-start(bf16[1,2048,128]{2,1,0:T(8,128)(2,1)} %param.28) | copy-start | bytes 1572868
  69.4 1.3 copy-start
  70.8 6.6 %copy-start.3 = (bf16[128,2048]{1,0:T(8,128)(2,1)S(1)}, bf16[128,2048]{1,0:T(8,128)(2,1)}, u32[]{:S(2)}) copy-start(bf16[128,2048]{1,0:T(8,128)(2,1)} %rows_ref.2) | copy-start | bytes 1572868
  70.8 6.6 %copy-start.6 = (bf16[2048,64]{0,1:T(8,128)(2,1)S(1)}, bf16[2048,64]{0,1:T(8,128)(2,1)}, u32[]{:S(2)}) copy-start(bf16[2048,64]{0,1:T(8,128)(2,1)} %param.17) | copy-start | bytes 786436
  70.8 6.6 %copy-start.11 = (f32[2048]{0:T(1024)S(1)}, f32[2048]{0:T(1024)}, u32[]{:S(2)}) copy-start(f32[2048]{0:T(1024)} %param.16) | copy-start | bytes 24580
  70.8 6.6 %copy-start.14 = (bf16[1,128]{1,0:T(2,128)(2,1)S(1)}, bf16[1,128]{1,0:T(2,128)(2,1)}, u32[]{:S(2)}) copy-start(bf16[1,128]{1,0:T(2,128)(2,1)} %bias_ref.1) | copy-start | bytes 772
  70.8 40.8 %copy-start.5 = (bf16[1,2048,128]{2,1,0:T(8,128)(2,1)S(1)}, bf16[1,2048,128]{2,1,0:T(8,128)(2,1)}, u32[]{:S(2)}) copy-start(bf16[1,2048,128]{2,1,0:T(8,128)(2,1)} %param.29) | copy-start | bytes 1572868
  70.8 40.8 %all-to-all-start.2 = ((bf16[16,512,128]{2,1,0:T(8,128)(2,1)}), bf16[16,512,128]{2,1,0:T(8,128)(2,1)S(1)}, u32[]{:S(2)}, u32[]{:S(2)}) async-start(bf16[16,512,128]{2,1,0:T(8,128)(2,1)} %copy-done), calls=%async_computation.2 | async-start | bytes 4194304 | tf_op jit(solution)/shard_map/all_to_all | solution.py:210
  77.4 1.0 copy-start.7
  78.3 0.9 copy-start.8
  109.6 8.8 %collective-permute-start = (bf16[2304,128]{1,0:T(8,128)(2,1)S(1)}, bf16[2304,128]{1,0:T(8,128)(2,1)}, u32[]{:S(2)}, u32[]{:S(2)}) collective-permute-start(bf16[2304,128]{1,0:T(8,128)(2,1)S(1)} %all_gather.6.own_ref), channel_id=1, source_target_pairs={{0,16},{16,0},{32,48},{48,32},{64,80},{80,64},{96,112},{112,96},{1... | collective-permute-start | bytes 1769480 | tf_op jit(solution)/shard_map/ppermute | solution.py:233
  112.9 42.1 %all-to-all-start.3 = ((bf16[32,16,128]{2,1,0:T(8,128)(2,1)}), bf16[32,16,128]{2,1,0:T(8,128)(2,1)S(1)}, u32[]{:S(2)}, u32[]{:S(2)}) async-start(bf16[32,16,128]{2,1,0:T(8,128)(2,1)} %bitcast.15), calls=%async_computation.3 | async-start | bytes 262144 | tf_op jit(solution)/shard_map/all_to_all | solution.py:210
  118.5 35.6 %copy-start.9 = (bf16[1024,128]{1,0:T(8,128)(2,1)S(1)}, bf16[1024,128]{1,0:T(8,128)(2,1)}, u32[]{:S(2)}) copy-start(bf16[1024,128]{1,0:T(8,128)(2,1)} %w_ref.1) | copy-start | bytes 786436
  118.5 36.5 %copy-start.13 = (s32[128,2]{0,1:T(2,128)S(1)}, s32[128,2]{0,1:T(2,128)}, u32[]{:S(2)}) copy-start(s32[128,2]{0,1:T(2,128)} %param.24) | copy-start | bytes 3076
  118.5 36.5 %copy-start.15 = (f32[128,4]{0,1:T(4,128)S(1)}, f32[128,4]{0,1:T(4,128)}, u32[]{:S(2)}) copy-start(f32[128,4]{0,1:T(4,128)} %param.25) | copy-start | bytes 6148
  118.5 36.5 %copy-start.16 = (f32[128,2]{0,1:T(2,128)S(1)}, f32[128,2]{0,1:T(2,128)}, u32[]{:S(2)}) copy-start(f32[128,2]{0,1:T(2,128)} %param.26) | copy-start | bytes 3076

commit v2 on v1

--- a/solution.py
+++ b/solution.py
@@ -13,7 +13,9 @@
 BLOCK = 128
 HEAD = 64
 SLOTS = EXPERTS * CAP
+ROWS = SLOTS // 2
 MSG = 144
+BEHIND = 4
 
 epsilon = 1e-06
 f32 = jnp.float32
@@ -23,14 +25,41 @@
 SMEM = pl.BlockSpec(memory_space=pltpu.SMEM)
 
 
-def call(body, n_scalar, n_in, outs, flops, mib=16):
-    return pl.pallas_call(
+def call(body, n_scalar, n_in, outs, flops, mib=16, hbm=(), **more):
+    def run(*args):
+        args = [
+            pltpu.with_memory_space_constraint(a, pltpu.HBM) if k in hbm else a
+            for k, a in enumerate(args)
+        ]
+        return kernel(*args)
+
+    kernel = pl.pallas_call(
         body,
         out_shape=outs,
         in_specs=[SMEM] * n_scalar + [pl.BlockSpec()] * n_in,
         cost_estimate=pl.CostEstimate(flops=flops, bytes_accessed=1 << 20, transcendentals=0),
         compiler_params=pltpu.CompilerParams(vmem_limit_bytes=mib << 20),
-    )
+        **more,
+    )
+    return run
+
+
+def call_out(body, n_scalar, n_in, out, flops, scratch):
+    copies = [pltpu.SemaphoreType.DMA((out.shape[0],))]
+    more = {"out_specs": pl.BlockSpec(memory_space=pltpu.HBM), "scratch_shapes": scratch + copies}
+    return call(body, n_scalar, n_in, out, flops, **more)
+
+
+def packed(*pieces):
+    def body(*refs):
+        at = 0
+        for ref in refs[:-1]:
+            refs[-1][at : at + ref.shape[0], :] = ref[...]
+            at += ref.shape[0]
+
+    rows = sum(p.shape[0] for p in pieces)
+    out = jax.ShapeDtypeStruct((rows, BLOCK), bf16)
+    return call(body, 0, len(pieces), out, 1 << 22)(*pieces)
 
 
 def nn(a, b):
@@ -58,6 +87,16 @@
     place0 = jnp.sum(mark0 * before, axis=0, keepdims=True)
     place1 = jnp.sum(mark1 * before, axis=0, keepdims=True)
     return place0.astype(i32), place1.astype(i32)
+
+
+def packed_seven(behind, middle, ahead):
+    def body(behind_ref, middle_ref, ahead_ref, out_ref):
+        out_ref[0 : 2 * MSG, :] = behind_ref[MSG:, :]
+        out_ref[2 * MSG : 5 * MSG, :] = middle_ref[...]
+        out_ref[5 * MSG :, :] = ahead_ref[: 2 * MSG, :]
+
+    out = jax.ShapeDtypeStruct((7 * MSG, BLOCK), bf16)
+    return call(body, 0, 3, out, 1 << 22)(behind, middle, ahead)
 
 
 def dispatch_body(tp_ref, rows_ref, gain_ref, ids_ref, out_ref):
@@ -85,38 +124,59 @@
     msg_ref[BLOCK:MSG, :] = jnp.broadcast_to(bias_ref[...], (MSG - BLOCK, BLOCK))
 
 
-def copies_body(x_ref, out_ref):
-    x = x_ref[...]
+def halves_body(x_ref, out_ref, sems):
+    copies = []
     for k in range(out_ref.shape[0]):
-        out_ref[k] = x
-
-
-def hidden_body(x_ref, gate_ref, up_ref, out_ref):
+        half = k % 2
+        source = x_ref.at[half * ROWS : (half + 1) * ROWS, :]
+        copies.append(pltpu.make_async_copy(source, out_ref.at[k], sems.at[k]))
+        copies[-1].start()
+    for copy in copies:
+        copy.wait()
+
+
+def hidden_body(tp_ref, x_ref, gate_ref, up_ref, other_ref, out_ref, hidden_ref, sems):
     parts = x_ref.shape[0]
-    weights = jnp.concatenate([gate_ref[...], up_ref[...]], axis=1)
-    rows = 256
-    for m in range(SLOTS // rows):
-        span = slice(m * rows, (m + 1) * rows)
-        x = jnp.concatenate([x_ref[k, span, :] for k in range(parts)], axis=1)
-        both = nn(x, weights)
+    even = tp_ref[0] % 2 == 0
+    depth = gate_ref.shape[0]
+    x = jnp.concatenate([x_ref[k] for k in range(parts)], axis=1)
+    own = nn(x, jnp.concatenate([gate_ref[...], up_ref[...]], axis=1))
+    other = nn(x, jnp.concatenate([other_ref[:depth, :], other_ref[depth:, :]], axis=1))
+
+    def gated(both):
         gate, up = both[:, :BLOCK], both[:, BLOCK:]
-        hidden = (gate * jax.nn.sigmoid(gate) * up).astype(bf16)
-        for k in range(parts):
-            out_ref[k, span, :] = hidden
+        return (gate * jax.nn.sigmoid(gate) * up).astype(bf16).astype(f32)
+
+    own, other = gated(own), gated(other)
+    first = jnp.where(even, own, other).astype(bf16)
+    second = jnp.where(even, other, own).astype(bf16)
+    hidden_ref[0:ROWS, :] = first
+    hidden_ref[ROWS:SLOTS, :] = second
+    copies = [pltpu.make_async_copy(hidden_ref, out_ref.at[k], sems.at[k]) for k in range(parts)]
+    for copy in copies:
+        copy.start()
+    for copy in copies:
+        copy.wait()
 
 
 def down_body(x_ref, w_ref, out_ref):
     parts = x_ref.shape[0]
-    rows = 256
-    for m in range(SLOTS // rows):
-        span = slice(m * rows, (m + 1) * rows)
-        x = jnp.concatenate([x_ref[k, span, :] for k in range(parts)], axis=1)
-        out_ref[span, :] = nn(x, w_ref[...]).astype(bf16)
+    for half in range(2):
+        x = jnp.concatenate(
+            [
+                x_ref[k, e * ROWS : (e + 1) * ROWS, :]
+                for k in range(half, parts, 2)
+                for e in range(2)
+            ],
+            axis=1,
+        )
+        out_ref[half * ROWS : (half + 1) * ROWS, :] = nn(x, w_ref[...]).astype(bf16)
 
 
 def attend_body(pos_ref, q_ref, own_ref, other_ref, out_ref):
     here = pos_ref[0]
     core = here % 2
+    chip_here = here // 2
     chips = own_ref.shape[0] // MSG
     q = q_ref[...]
     wide = (2 * BLOCK, 2 * BLOCK)
@@ -141,7 +201,7 @@
     def chip(k, carry):
         later, total = carry
         z = chips - 1 - k
-        at = pl.multiple_of(z * MSG, MSG)
+        at = pl.multiple_of(((z - chip_here + BEHIND + chips) % chips) * MSG, 16)
         own = own_ref[pl.ds(at, MSG), :]
         other = other_ref[pl.ds(at, MSG), :]
         upper = jnp.where(core == 1, own, other)
@@ -202,8 +262,9 @@
     ep, tp = lax.axis_size("ep"), lax.axis_size("tp")
     chips = ep // 2
     here = lax.axis_index("ep")
-    same_core = [[z * 2 + c for z in range(chips)] for c in range(2)]
-    partner = [(e, e ^ 1) for e in range(ep)]
+    side = tp // 4
+    along_x = [[y * 4 + x for x in range(4)] for y in range(side)]
+    along_y = [[y * 4 + x for y in range(side)] for x in range(4)]
     struct = jax.ShapeDtypeStruct
 
     def exchange(x, axis):
@@ -214,12 +275,17 @@
     square = struct((BLOCK, BLOCK), bf16)
     ids = expert_ids.T
     column = lax.axis_index("tp").reshape(1)
-    send = call(dispatch_body, 1, 3, slots, 1 << 27)(
+
+    def from_chip(x, step):
+        moves = [((((z + step) % chips) * 2 + c), z * 2 + c) for z in range(chips) for c in range(2)]
+        return lax.ppermute(x, "ep", moves)
+
+    send = call(dispatch_body, 1, 3, slots, 1 << 27, hbm=(1, 2, 3))(
         column, expert_rows, expert_gain[None, :], ids
     )
     routed = exchange(send.reshape(ep, CAP, BLOCK), "ep").reshape(SLOTS, BLOCK)
     outs = (struct((BLOCK, HEAD), bf16), struct((MSG, BLOCK), bf16))
-    query, message = call(project_body, 0, 6, outs, 1 << 28)(
+    query, message = call(project_body, 0, 6, outs, 1 << 28, hbm=range(6))(
         attn_rows,
         attn_gain[None, :],
         query_weight.T,
@@ -227,22 +293,35 @@
         value_weight.T,
         key_bias,
     )
-    routed = call(copies_body, 0, 1, copies, 1 << 24)(routed)
+    behind1 = from_chip(message, -1)
+    ahead1 = from_chip(message, 1)
+    swaps = [(k, k ^ 1) for k in range(tp)]
+    other_weights = lax.ppermute(
+        jnp.concatenate([gate_weight[0], up_weight[0]], axis=0), "tp", swaps
+    )
+    three = packed(behind1, message, ahead1)
+    behind3 = from_chip(three, -3)
+    ahead3 = from_chip(three, 3)
+    routed = call_out(halves_body, 0, 1, struct((tp, ROWS, BLOCK), bf16), 1 << 24, [])(routed)
     routed = exchange(routed, "tp")
-    own = lax.all_gather(message, "ep", axis=0, tiled=True, axis_index_groups=same_core)
-    other = lax.ppermute(own, "ep", partner)
-    hidden = call(hidden_body, 0, 3, copies, 1 << 29)(routed, gate_weight[0], up_weight[0])
+    seven = packed_seven(behind3, three, ahead3)
+    far = from_chip(seven, 8)
+    own_hidden = [pltpu.VMEM((SLOTS, BLOCK), bf16)]
+    hidden = call_out(hidden_body, 1, 4, copies, 1 << 29, own_hidden)(
+        column, routed, gate_weight[0], up_weight[0], other_weights
+    )
     hidden = exchange(hidden, "tp")
+    own = packed(behind3, three, ahead3, far)
+    other = lax.ppermute(own, "ep", [(e, e ^ 1) for e in range(ep)])
     attended = call(attend_body, 1, 3, struct((HEAD, BLOCK), bf16), 1 << 30)(
         here.reshape(1), query, own, other
     )
+    attended = lax.all_gather(attended, "tp", axis=0, tiled=True, axis_index_groups=along_x)
     result = call(down_body, 0, 2, slots, 1 << 28)(hidden, down_weight[0])
     back = exchange(result.reshape(ep, CAP, BLOCK), "ep").reshape(SLOTS, BLOCK)
-    attended = lax.all_gather(attended, "tp", axis=0, tiled=True)
+    attended = lax.all_gather(attended, "tp", axis=0, tiled=True, axis_index_groups=along_y)
     mixed = call(mix_body, 0, 2, square, 1 << 26)(attended, out_weight)
-    expert_out = call(combine_body, 0, 4, square, 1 << 27)(
-        ids, group_logits.T, pair_logits.T, back
-    )
+    expert_out = call(combine_body, 0, 4, square, 1 << 27)(ids, group_logits.T, pair_logits.T, back)
     return (mixed, expert_out)
 
 

time: 157 us -> 184 us (1.17)
  blocking collectives: 118 us -> 24.7 us
  starting transfers between devices: 14 us -> 76.6 us
  waiting for transfers between devices: 0.01 us -> 53.1 us
  Pallas kernels: 17.7 us -> 24.4 us
  local copies, waits for them, and re-layouts: 5.69 us -> 1.35 us
  other arithmetic: 0 us -> 2.26 us
    all_to_all x2 -> x0, blocking collectives: 64.7 us -> none  [exchange(): return lax.all_to_all(x, axis, split_axis=0, concat_axis=0, tiled=True)]
    all_to_all x2 -> x4, starting transfers between devices: 12.1 us -> 48 us  [exchange(): return lax.all_to_all(x, axis, split_axis=0, concat_axis=0, tiled=True)]
    ppermute x1 -> x7, waiting for transfers between devices: 0.01 us -> 29.9 us  [the longest x5 25.1 us: from_chip(): return lax.ppermute(x, 'ep', moves)]
    all_gather x2, blocking collectives: 53.2 us -> 24.7 us  [shards(): lax.all_gather(attended, 'tp', axis=0, tiled=True, axis_index_groups=alon...]
    ppermute x1 -> x7, starting transfers between devices: 1.91 us -> 28.5 us  [the longest x5 23.7 us: from_chip(): return lax.ppermute(x, 'ep', moves)]
    all_to_all x2 -> x4, waiting for transfers between devices: 0.01 us -> 23.2 us  [exchange(): return lax.all_to_all(x, axis, split_axis=0, concat_axis=0, tiled=True)]
    pallas_call x8 -> x11, Pallas kernels: 17.7 us -> 24.4 us  [run(): return kernel(*args)]
    unnamed x34 -> x16, local copies, waits for them, and re-layouts: 5.69 us -> 1.35 us
  transfers between devices with their start and end apart: 3 -> 11, of which waited for: 0 -> 7; matrix products, arithmetic and copies ran while one was open for 0% -> 1% of each run, Pallas kernels for 10% -> 10%
where the time goes in v2:
time: 184 us; the launch traced here: 183 us
  starting transfers between devices  76.6 us (42%)
  waiting for transfers between devices  53.1 us (29%)
  blocking collectives  24.7 us (13%)
  Pallas kernels  24.4 us (13%)
  other arithmetic  2.26 us (1%)
    all_to_all x4, starting transfers between devices, exchange(): return lax.all_to_all(x, axis, split_axis=0, concat_axis=0, tiled=True)  48 us
    ppermute x5, waiting for transfers between devices, from_chip(): return lax.ppermute(x, 'ep', moves)  25.1 us
    all_gather x2, blocking collectives, shards(): lax.all_gather(attended, 'tp', axis=0, tiled=True, axis_index_groups=alon...  24.7 us
    pallas_call x11, Pallas kernels, run(): return kernel(*args)  24.4 us
    ppermute x5, starting transfers between devices, from_chip(): return lax.ppermute(x, 'ep', moves)  23.7 us
    all_to_all x4, waiting for transfers between devices, exchange(): return lax.all_to_all(x, axis, split_axis=0, concat_axis=0, tiled=True)  23.2 us
    ppermute x1, waiting for transfers between devices, shards(): lax.ppermute(jnp.concatenate([gate_weight[0], up_weight[0]], axis=0), 'tp...  4.79 us
  transfers between devices with their start and end apart: 11, of which 7 were waited for; matrix products, arithmetic and copies ran while one was open for 1% of the time, Pallas kernels for 10%

profile of v2, /device:TPU:6, one launch (start us, length us, event | category | flops | bytes accessed | tf_op | source)
XLA Modules:
  0.0 183.2 jit_solution(9918450738456212990)
XLA Ops:
  0.6 2.1 %shard_map.164 = bf16[512,128]{1,0:T(8,128)(2,1)} custom-call(s32[1]{0:T(128)} %bitcast.8.tp_ref, bf16[128,2048]{1,0:T(8,128)(2,1)} %rows_ref.3, f32[1,2048]{1,0:T(1,128)} %bitcast.31, s32[2,128]{1,0:T(2,128)} %bitcast.24), custom_call_target="tpu_custom_call" | custom-call | flops 134217728 | bytes 1048576 | tf_op jit(solution)/shard_map/pallas_call | solution.py:34
  2.7 15.5 %all-to-all-start = ((bf16[32,16,128]{2,1,0:T(8,128)(2,1)}), bf16[32,16,128]{2,1,0:T(8,128)(2,1)S(1)}, u32[]{:S(2)}, u32[]{:S(2)}) async-start(bf16[32,16,128]{2,1,0:T(8,128)(2,1)} %bitcast.10), calls=%async_computation | async-start | bytes 262144 | tf_op jit(solution)/shard_map/all_to_all | solution.py:271
  18.2 2.3 %pad_maximum_fusion = bf16[4096,128]{1,0:T(8,128)(2,1)} fusion(bf16[2048,128]{1,0:T(8,128)(2,1)} %bitcast.19, bf16[2048,128]{1,0:T(8,128)(2,1)} %bitcast.17), kind=kLoop, calls=%fused_computation | loop fusion | flops 2097152 | bytes 2097152 | tf_op jit(solution)/shard_map/concatenate | solution.py:300
  20.5 2.9 %collective-permute-start.6 = (bf16[4096,128]{1,0:T(8,128)(2,1)}, bf16[4096,128]{1,0:T(8,128)(2,1)S(1)}, u32[]{:S(2)}, u32[]{:S(2)}) collective-permute-start(bf16[4096,128]{1,0:T(8,128)(2,1)} %pad_maximum_fusion), channel_id=1, source_target_pairs={{0,1},{1,0},{2,3},{3,2},{4,5},{5,4},{6,7},{7,6},{8,9},{9,8},{10,11... | collective-permute-start | bytes 3145736 | tf_op jit(solution)/shard_map/ppermute | solution.py:299
  23.3 12.1 %all-to-all-done = bf16[32,16,128]{2,1,0:T(8,128)(2,1)S(1)} async-done(((bf16[32,16,128]{2,1,0:T(8,128)(2,1)}), bf16[32,16,128]{2,1,0:T(8,128)(2,1)S(1)}, u32[]{:S(2)}, u32[]{:S(2)}) %all-to-all-start) | async-done | bytes 131104 | tf_op jit(solution)/shard_map/all_to_all | solution.py:271
  36.5 7.4 %all-to-all-start.1 = ((bf16[16,256,128]{2,1,0:T(8,128)(2,1)}), bf16[16,256,128]{2,1,0:T(8,128)(2,1)S(1)}, u32[]{:S(2)}, u32[]{:S(2)}) async-start(bf16[16,256,128]{2,1,0:T(8,128)(2,1)} %shard_map.165), calls=%async_computation.1 | async-start | bytes 2097152 | tf_op jit(solution)/shard_map/all_to_all | solution.py:271
  43.9 4.8 %collective-permute-done.6.other_ref = bf16[4096,128]{1,0:T(8,128)(2,1)S(1)} collective-permute-done((bf16[4096,128]{1,0:T(8,128)(2,1)}, bf16[4096,128]{1,0:T(8,128)(2,1)S(1)}, u32[]{:S(2)}, u32[]{:S(2)}) %collective-permute-start.6) | collective-permute-done | bytes 1048608 | tf_op jit(solution)/shard_map/ppermute | solution.py:299
  48.7 11.1 %all-to-all-done.1.x_ref = bf16[16,256,128]{2,1,0:T(8,128)(2,1)S(1)} async-done(((bf16[16,256,128]{2,1,0:T(8,128)(2,1)}), bf16[16,256,128]{2,1,0:T(8,128)(2,1)S(1)}, u32[]{:S(2)}, u32[]{:S(2)}) %all-to-all-start.1) | async-done | bytes 1048608 | tf_op jit(solution)/shard_map/all_to_all | solution.py:271
  59.8 3.6 %shard_map.166 = bf16[16,512,128]{2,1,0:T(8,128)(2,1)S(1)} custom-call(s32[1]{0:T(128)} %bitcast.8.tp_ref, bf16[16,256,128]{2,1,0:T(8,128)(2,1)S(1)} %all-to-all-done.1.x_ref, bf16[2048,128]{1,0:T(8,128)(2,1)S(1)} %bitcast.18, bf16[2048,128]{1,0:T(8,128)(2,1)S(1)} %bitcast.20, bf16[4096,128]{1,0:T(8,128)(2,1)S(1)} %collective-permute-done.6.other_ref), custom_call_target="tpu_custom_call" | custom-call | flops 536870912 | bytes 1048576 | tf_op jit(solution)/shard_map/pallas_call | solution.py:34
  64.8 8.1 %all-to-all-start.2 = ((bf16[16,512,128]{2,1,0:T(8,128)(2,1)}), bf16[16,512,128]{2,1,0:T(8,128)(2,1)S(1)}, u32[]{:S(2)}, u32[]{:S(2)}) async-start(bf16[16,512,128]{2,1,0:T(8,128)(2,1)} %copy-done), calls=%async_computation.2 | async-start | bytes 4194304 | tf_op jit(solution)/shard_map/all_to_all | solution.py:271
  72.9 1.9 %shard_map.158 = (bf16[128,64]{1,0:T(8,128)(2,1)S(1)}, bf16[144,128]{1,0:T(8,128)(2,1)S(1)}) custom-call(bf16[128,2048]{1,0:T(8,128)(2,1)} %rows_ref.2, f32[1,2048]{1,0:T(1,128)} %bitcast.32, bf16[64,2048]{1,0:T(8,128)(2,1)} %bitcast.28, bf16[64,2048]{1,0:T(8,128)(2,1)} %bitcast.29, bf16[64,2048]{1,0:T(8,128)(2,1)} %bitcast.30, bf16[1,128]{1,0:T(2,128)(2,1)} %bias_ref.1), custom_call_target="tpu_custom_call" | custom-call | flops 268435456 | bytes 1048576 | tf_op jit(solution)/shard_map/pallas_call | solution.py:34
  74.8 4.8 %collective-permute-start.1 = (bf16[144,128]{1,0:T(8,128)(2,1)S(1)}, bf16[144,128]{1,0:T(8,128)(2,1)S(1)}, u32[]{:S(2)}, u32[]{:S(2)}) collective-permute-start(bf16[144,128]{1,0:T(8,128)(2,1)S(1)} %get-tuple-element.5.refs_1_), channel_id=1, source_target_pairs={{32,0},{48,16},{64,32},{80,48},{96,64},{112,80},{128,96},{144,112}... | collective-permute-start | bytes 110600 | tf_op jit(solution)/shard_map/ppermute | solution.py:281
  79.6 1.9 %collective-permute-start = (bf16[144,128]{1,0:T(8,128)(2,1)S(1)}, bf16[144,128]{1,0:T(8,128)(2,1)S(1)}, u32[]{:S(2)}, u32[]{:S(2)}) collective-permute-start(bf16[144,128]{1,0:T(8,128)(2,1)S(1)} %get-tuple-element.5.refs_1_), channel_id=1, source_target_pairs={{480,0},{496,16},{0,32},{16,48},{32,64},{48,80},{64,96},{80,112},{... | collective-permute-start | bytes 110600 | tf_op jit(solution)/shard_map/ppermute | solution.py:281
  81.6 5.1 %collective-permute-done.refs_0_ = bf16[144,128]{1,0:T(8,128)(2,1)S(1)} collective-permute-done((bf16[144,128]{1,0:T(8,128)(2,1)S(1)}, bf16[144,128]{1,0:T(8,128)(2,1)S(1)}, u32[]{:S(2)}, u32[]{:S(2)}) %collective-permute-start) | collective-permute-done | bytes 36896 | tf_op jit(solution)/shard_map/ppermute | solution.py:281
  86.7 4.6 %collective-permute-start.3 = (bf16[432,128]{1,0:T(8,128)(2,1)S(1)}, bf16[432,128]{1,0:T(8,128)(2,1)S(1)}, u32[]{:S(2)}, u32[]{:S(2)}) collective-permute-start(bf16[432,128]{1,0:T(8,128)(2,1)S(1)} %shard_map.159.middle_ref.refs_1_), channel_id=1, source_target_pairs={{96,0},{112,16},{128,32},{144,48},{160,64},{176,80},{192,96},{208,... | collective-permute-start | bytes 331784 | tf_op jit(solution)/shard_map/ppermute | solution.py:281
  91.3 3.1 %collective-permute-start.2 = (bf16[432,128]{1,0:T(8,128)(2,1)S(1)}, bf16[432,128]{1,0:T(8,128)(2,1)S(1)}, u32[]{:S(2)}, u32[]{:S(2)}) collective-permute-start(bf16[432,128]{1,0:T(8,128)(2,1)S(1)} %shard_map.159.middle_ref.refs_1_), channel_id=1, source_target_pairs={{416,0},{432,16},{448,32},{464,48},{480,64},{496,80},{0,96},{16,11... | collective-permute-start | bytes 331784 | tf_op jit(solution)/shard_map/ppermute | solution.py:281
  96.1 5.1 %collective-permute-done.2.behind_ref.refs_0_ = bf16[432,128]{1,0:T(8,128)(2,1)S(1)} collective-permute-done((bf16[432,128]{1,0:T(8,128)(2,1)S(1)}, bf16[432,128]{1,0:T(8,128)(2,1)S(1)}, u32[]{:S(2)}, u32[]{:S(2)}) %collective-permute-start.2) | collective-permute-done | bytes 110624 | tf_op jit(solution)/shard_map/ppermute | solution.py:281
  101.2 9.4 %collective-permute-start.4 = (bf16[1008,128]{1,0:T(8,128)(2,1)S(1)}, bf16[1008,128]{1,0:T(8,128)(2,1)S(1)}, u32[]{:S(2)}, u32[]{:S(2)}) collective-permute-start(bf16[1008,128]{1,0:T(8,128)(2,1)S(1)} %shard_map.160), channel_id=1, source_target_pairs={{256,0},{272,16},{288,32},{304,48},{320,64},{336,80},{352,96},{368... | collective-permute-start | bytes 774152 | tf_op jit(solution)/shard_map/ppermute | solution.py:281
  110.6 13.2 %collective-permute-done.4.refs_3_ = bf16[1008,128]{1,0:T(8,128)(2,1)S(1)} collective-permute-done((bf16[1008,128]{1,0:T(8,128)(2,1)S(1)}, bf16[1008,128]{1,0:T(8,128)(2,1)S(1)}, u32[]{:S(2)}, u32[]{:S(2)}) %collective-permute-start.4) | collective-permute-done | bytes 258080 | tf_op jit(solution)/shard_map/ppermute | solution.py:281
  123.8 1.9 %collective-permute-start.5 = (bf16[2304,128]{1,0:T(8,128)(2,1)S(1)}, bf16[2304,128]{1,0:T(8,128)(2,1)}, u32[]{:S(2)}, u32[]{:S(2)}) collective-permute-start(bf16[2304,128]{1,0:T(8,128)(2,1)S(1)} %shard_map.161.own_ref), channel_id=1, source_target_pairs={{0,16},{16,0},{32,48},{48,32},{64,80},{80,64},{96,112},{112,96},{1... | collective-permute-start | bytes 1769480 | tf_op jit(solution)/shard_map/ppermute | solution.py:315
  127.1 17.0 %all-to-all-start.3 = ((bf16[32,16,128]{2,1,0:T(8,128)(2,1)}), bf16[32,16,128]{2,1,0:T(8,128)(2,1)S(1)}, u32[]{:S(2)}, u32[]{:S(2)}) async-start(bf16[32,16,128]{2,1,0:T(8,128)(2,1)} %bitcast.15), calls=%async_computation.3 | async-start | bytes 262144 | tf_op jit(solution)/shard_map/all_to_all | solution.py:271
  144.2 12.2 %shard_map.162 = bf16[64,128]{1,0:T(8,128)(2,1)S(1)} custom-call(s32[1]{0:T(128)} %bitcast.pos_ref, bf16[128,64]{1,0:T(8,128)(2,1)S(1)} %get-tuple-element.4.q_ref, bf16[2304,128]{1,0:T(8,128)(2,1)S(1)} %shard_map.161.own_ref, bf16[2304,128]{1,0:T(8,128)(2,1)} %collective-permute-done.5.other_ref), custom_call_target="tpu_custom_call" | custom-call | flops 1073741824 | bytes 1048576 | tf_op jit(solution)/shard_map/pallas_call | solution.py:34
  156.4 11.9 %all_gather.6 = bf16[256,128]{1,0:T(8,128)(2,1)S(1)} all-gather(bf16[64,128]{1,0:T(8,128)(2,1)S(1)} %shard_map.162), channel_id=1, replica_groups={{0,1,2,3},{4,5,6,7},{8,9,10,11},{12,13,14,15},{16,17,18,19},{20,21,22,2..., dimensions={0}, use_global_device_ids=true | all-gather | bytes 81920 | tf_op jit(solution)/shard_map/all_gather | solution.py:319
  168.3 12.9 %all_gather.7.x_ref = bf16[1024,128]{1,0:T(8,128)(2,1)S(1)} all-gather(bf16[256,128]{1,0:T(8,128)(2,1)S(1)} %all_gather.6), channel_id=1, replica_groups={{0,4,8,12},{1,5,9,13},{2,6,10,14},{3,7,11,15},{16,20,24,28},{17,21,25,2..., dimensions={0}, use_global_device_ids=true | all-gather | bytes 327680 | tf_op jit(solution)/shard_map/all_gather | solution.py:322
  (28 shorter events, 7.7 us)
Async XLA Ops:
  2.7 32.7 %all-to-all-start = ((bf16[32,16,128]{2,1,0:T(8,128)(2,1)}), bf16[32,16,128]{2,1,0:T(8,128)(2,1)S(1)}, u32[]{:S(2)}, u32[]{:S(2)}) async-start(bf16[32,16,128]{2,1,0:T(8,128)(2,1)} %bitcast.10), calls=%async_computation | async-start | bytes 262144 | tf_op jit(solution)/shard_map/all_to_all | solution.py:271
  20.5 39.4 %copy-start.1 = (bf16[1,2048,128]{2,1,0:T(8,128)(2,1)S(1)}, bf16[1,2048,128]{2,1,0:T(8,128)(2,1)}, u32[]{:S(2)}) copy-start(bf16[1,2048,128]{2,1,0:T(8,128)(2,1)} %param.27) | copy-start | bytes 1572868
  20.5 39.4 %copy-start.2 = (bf16[1,2048,128]{2,1,0:T(8,128)(2,1)S(1)}, bf16[1,2048,128]{2,1,0:T(8,128)(2,1)}, u32[]{:S(2)}) copy-start(bf16[1,2048,128]{2,1,0:T(8,128)(2,1)} %param.28) | copy-start | bytes 1572868
  20.5 28.3 %collective-permute-start.6 = (bf16[4096,128]{1,0:T(8,128)(2,1)}, bf16[4096,128]{1,0:T(8,128)(2,1)S(1)}, u32[]{:S(2)}, u32[]{:S(2)}) collective-permute-start(bf16[4096,128]{1,0:T(8,128)(2,1)} %pad_maximum_fusion), channel_id=1, source_target_pairs={{0,1},{1,0},{2,3},{3,2},{4,5},{5,4},{6,7},{7,6},{8,9},{9,8},{10,11... | collective-permute-start | bytes 3145736 | tf_op jit(solution)/shard_map/ppermute | solution.py:299
  36.5 23.3 %all-to-all-start.1 = ((bf16[16,256,128]{2,1,0:T(8,128)(2,1)}), bf16[16,256,128]{2,1,0:T(8,128)(2,1)S(1)}, u32[]{:S(2)}, u32[]{:S(2)}) async-start(bf16[16,256,128]{2,1,0:T(8,128)(2,1)} %shard_map.165), calls=%async_computation.1 | async-start | bytes 2097152 | tf_op jit(solution)/shard_map/all_to_all | solution.py:271
  63.4 1.3 copy-start
  64.8 61.0 %all-to-all-start.2 = ((bf16[16,512,128]{2,1,0:T(8,128)(2,1)}), bf16[16,512,128]{2,1,0:T(8,128)(2,1)S(1)}, u32[]{:S(2)}, u32[]{:S(2)}) async-start(bf16[16,512,128]{2,1,0:T(8,128)(2,1)} %copy-done), calls=%async_computation.2 | async-start | bytes 4194304 | tf_op jit(solution)/shard_map/all_to_all | solution.py:271
  72.9 52.9 %copy-start.3 = (bf16[1,2048,128]{2,1,0:T(8,128)(2,1)S(1)}, bf16[1,2048,128]{2,1,0:T(8,128)(2,1)}, u32[]{:S(2)}) copy-start(bf16[1,2048,128]{2,1,0:T(8,128)(2,1)} %param.29) | copy-start | bytes 1572868
  74.8 6.7 %collective-permute-start.1 = (bf16[144,128]{1,0:T(8,128)(2,1)S(1)}, bf16[144,128]{1,0:T(8,128)(2,1)S(1)}, u32[]{:S(2)}, u32[]{:S(2)}) collective-permute-start(bf16[144,128]{1,0:T(8,128)(2,1)S(1)} %get-tuple-element.5.refs_1_), channel_id=1, source_target_pairs={{32,0},{48,16},{64,32},{80,48},{96,64},{112,80},{128,96},{144,112}... | collective-permute-start | bytes 110600 | tf_op jit(solution)/shard_map/ppermute | solution.py:281
  79.6 7.1 %collective-permute-start = (bf16[144,128]{1,0:T(8,128)(2,1)S(1)}, bf16[144,128]{1,0:T(8,128)(2,1)S(1)}, u32[]{:S(2)}, u32[]{:S(2)}) collective-permute-start(bf16[144,128]{1,0:T(8,128)(2,1)S(1)} %get-tuple-element.5.refs_1_), channel_id=1, source_target_pairs={{480,0},{496,16},{0,32},{16,48},{32,64},{48,80},{64,96},{80,112},{... | collective-permute-start | bytes 110600 | tf_op jit(solution)/shard_map/ppermute | solution.py:281
  86.7 9.4 %collective-permute-start.3 = (bf16[432,128]{1,0:T(8,128)(2,1)S(1)}, bf16[432,128]{1,0:T(8,128)(2,1)S(1)}, u32[]{:S(2)}, u32[]{:S(2)}) collective-permute-start(bf16[432,128]{1,0:T(8,128)(2,1)S(1)} %shard_map.159.middle_ref.refs_1_), channel_id=1, source_target_pairs={{96,0},{112,16},{128,32},{144,48},{160,64},{176,80},{192,96},{208,... | collective-permute-start | bytes 331784 | tf_op jit(solution)/shard_map/ppermute | solution.py:281
  91.3 9.9 %collective-permute-start.2 = (bf16[432,128]{1,0:T(8,128)(2,1)S(1)}, bf16[432,128]{1,0:T(8,128)(2,1)S(1)}, u32[]{:S(2)}, u32[]{:S(2)}) collective-permute-start(bf16[432,128]{1,0:T(8,128)(2,1)S(1)} %shard_map.159.middle_ref.refs_1_), channel_id=1, source_target_pairs={{416,0},{432,16},{448,32},{464,48},{480,64},{496,80},{0,96},{16,11... | collective-permute-start | bytes 331784 | tf_op jit(solution)/shard_map/ppermute | solution.py:281
  101.2 22.6 %collective-permute-start.4 = (bf16[1008,128]{1,0:T(8,128)(2,1)S(1)}, bf16[1008,128]{1,0:T(8,128)(2,1)S(1)}, u32[]{:S(2)}, u32[]{:S(2)}) collective-permute-start(bf16[1008,128]{1,0:T(8,128)(2,1)S(1)} %shard_map.160), channel_id=1, source_target_pairs={{256,0},{272,16},{288,32},{304,48},{320,64},{336,80},{352,96},{368... | collective-permute-start | bytes 774152 | tf_op jit(solution)/shard_map/ppermute | solution.py:281
  123.8 20.3 %collective-permute-start.5 = (bf16[2304,128]{1,0:T(8,128)(2,1)S(1)}, bf16[2304,128]{1,0:T(8,128)(2,1)}, u32[]{:S(2)}, u32[]{:S(2)}) collective-permute-start(bf16[2304,128]{1,0:T(8,128)(2,1)S(1)} %shard_map.161.own_ref), channel_id=1, source_target_pairs={{0,16},{16,0},{32,48},{48,32},{64,80},{80,64},{96,112},{112,96},{1... | collective-permute-start | bytes 1769480 | tf_op jit(solution)/shard_map/ppermute | solution.py:315
  127.1 54.9 %all-to-all-start.3 = ((bf16[32,16,128]{2,1,0:T(8,128)(2,1)}), bf16[32,16,128]{2,1,0:T(8,128)(2,1)S(1)}, u32[]{:S(2)}, u32[]{:S(2)}) async-start(bf16[32,16,128]{2,1,0:T(8,128)(2,1)} %bitcast.15), calls=%async_computation.3 | async-start | bytes 262144 | tf_op jit(solution)/shard_map/all_to_all | solution.py:271
  144.1 37.0 %copy-start.4 = (bf16[1024,128]{1,0:T(8,128)(2,1)S(1)}, bf16[1024,128]{1,0:T(8,128)(2,1)}, u32[]{:S(2)}) copy-start(bf16[1024,128]{1,0:T(8,128)(2,1)} %w_ref.1) | copy-start | bytes 786436
  144.2 37.9 %copy-start.5 = (s32[128,2]{0,1:T(2,128)S(1)}, s32[128,2]{0,1:T(2,128)}, u32[]{:S(2)}) copy-start(s32[128,2]{0,1:T(2,128)} %param.24) | copy-start | bytes 3076
  144.2 37.9 %copy-start.6 = (f32[128,4]{0,1:T(4,128)S(1)}, f32[128,4]{0,1:T(4,128)}, u32[]{:S(2)}) copy-start(f32[128,4]{0,1:T(4,128)} %param.25) | copy-start | bytes 6148
  144.2 37.9 %copy-start.7 = (f32[128,2]{0,1:T(2,128)S(1)}, f32[128,2]{0,1:T(2,128)}, u32[]{:S(2)}) copy-start(f32[128,2]{0,1:T(2,128)} %param.26) | copy-start | bytes 3076

commit v3 on v2

--- a/solution.py
+++ b/solution.py
@@ -15,7 +15,7 @@
 SLOTS = EXPERTS * CAP
 ROWS = SLOTS // 2
 MSG = 144
-BEHIND = 4
+WIDTH = 4
 
 epsilon = 1e-06
 f32 = jnp.float32
@@ -47,19 +47,7 @@
 def call_out(body, n_scalar, n_in, out, flops, scratch):
     copies = [pltpu.SemaphoreType.DMA((out.shape[0],))]
     more = {"out_specs": pl.BlockSpec(memory_space=pltpu.HBM), "scratch_shapes": scratch + copies}
-    return call(body, n_scalar, n_in, out, flops, **more)
-
-
-def packed(*pieces):
-    def body(*refs):
-        at = 0
-        for ref in refs[:-1]:
-            refs[-1][at : at + ref.shape[0], :] = ref[...]
-            at += ref.shape[0]
-
-    rows = sum(p.shape[0] for p in pieces)
-    out = jax.ShapeDtypeStruct((rows, BLOCK), bf16)
-    return call(body, 0, len(pieces), out, 1 << 22)(*pieces)
+    return call(body, n_scalar, n_in, pltpu.HBM(out.shape, out.dtype), flops, **more)
 
 
 def nn(a, b):
@@ -87,16 +75,6 @@
     place0 = jnp.sum(mark0 * before, axis=0, keepdims=True)
     place1 = jnp.sum(mark1 * before, axis=0, keepdims=True)
     return place0.astype(i32), place1.astype(i32)
-
-
-def packed_seven(behind, middle, ahead):
-    def body(behind_ref, middle_ref, ahead_ref, out_ref):
-        out_ref[0 : 2 * MSG, :] = behind_ref[MSG:, :]
-        out_ref[2 * MSG : 5 * MSG, :] = middle_ref[...]
-        out_ref[5 * MSG :, :] = ahead_ref[: 2 * MSG, :]
-
-    out = jax.ShapeDtypeStruct((7 * MSG, BLOCK), bf16)
-    return call(body, 0, 3, out, 1 << 22)(behind, middle, ahead)
 
 
 def dispatch_body(tp_ref, rows_ref, gain_ref, ids_ref, out_ref):
@@ -135,13 +113,12 @@
         copy.wait()
 
 
-def hidden_body(tp_ref, x_ref, gate_ref, up_ref, other_ref, out_ref, hidden_ref, sems):
+def hidden_body(tp_ref, x_ref, g0_ref, u0_ref, g1_ref, u1_ref, out_ref, hidden_ref, sems):
     parts = x_ref.shape[0]
     even = tp_ref[0] % 2 == 0
-    depth = gate_ref.shape[0]
     x = jnp.concatenate([x_ref[k] for k in range(parts)], axis=1)
-    own = nn(x, jnp.concatenate([gate_ref[...], up_ref[...]], axis=1))
-    other = nn(x, jnp.concatenate([other_ref[:depth, :], other_ref[depth:, :]], axis=1))
+    own = nn(x, jnp.concatenate([g0_ref[...], u0_ref[...]], axis=1))
+    other = nn(x, jnp.concatenate([g1_ref[...], u1_ref[...]], axis=1))
 
     def gated(both):
         gate, up = both[:, :BLOCK], both[:, BLOCK:]
@@ -176,7 +153,6 @@
 def attend_body(pos_ref, q_ref, own_ref, other_ref, out_ref):
     here = pos_ref[0]
     core = here % 2
-    chip_here = here // 2
     chips = own_ref.shape[0] // MSG
     q = q_ref[...]
     wide = (2 * BLOCK, 2 * BLOCK)
@@ -185,32 +161,36 @@
     tail = ones_where((col >= BLOCK) | (row >= col)).astype(bf16)
     t, s = iota((BLOCK, BLOCK), 0), iota((BLOCK, BLOCK), 1)
 
-    def block(msg, number, later, total):
-        scores = nn(q, msg[0:HEAD, :]) + msg[BLOCK : BLOCK + 1, :].astype(f32)
-        causal = s + (number - here) * BLOCK < t
-        keep = -(jnp.maximum(scores, 0.0) + jnp.log1p(jnp.exp(-jnp.abs(scores))))
-        keep = jnp.where(causal, keep, 0.0)
-        high = keep.astype(bf16)
-        low = (keep - high.astype(f32)).astype(bf16)
-        sums = nn(jnp.concatenate([high, low], axis=1), tail)
-        weights = jnp.where(causal, jnp.exp(scores + sums[:, :BLOCK]), 0.0).astype(bf16)
-        out = nt(weights, msg[HEAD:BLOCK, :])
-        total = total + jnp.exp(later) * out
-        return later + sums[:, BLOCK : BLOCK + HEAD], total
-
-    def chip(k, carry):
+    offset = s - t
+
+    def step(k, carry):
         later, total = carry
-        z = chips - 1 - k
-        at = pl.multiple_of(((z - chip_here + BEHIND + chips) % chips) * MSG, 16)
-        own = own_ref[pl.ds(at, MSG), :]
-        other = other_ref[pl.ds(at, MSG), :]
-        upper = jnp.where(core == 1, own, other)
-        lower = jnp.where(core == 1, other, own)
-        later, total = block(upper, 2 * z + 1, later, total)
-        return block(lower, 2 * z, later, total)
+        messages, starts = [], []
+        for w in range(WIDTH):
+            z = chips - 1 - (k * WIDTH + w)
+            at = pl.multiple_of(((z % 4) * (chips // 4) + z // 4) * MSG, 16)
+            own = own_ref[pl.ds(at, MSG), :]
+            other = other_ref[pl.ds(at, MSG), :]
+            messages += [jnp.where(core == 1, own, other), jnp.where(core == 1, other, own)]
+            starts += [(here - 2 * z - 1) * BLOCK, (here - 2 * z) * BLOCK]
+        scores = [nn(q, m[0:HEAD, :]) + m[BLOCK : BLOCK + 1, :].astype(f32) for m in messages]
+        causal = [offset < start for start in starts]
+        logs = [jnp.log(1.0 + jnp.exp(-jnp.abs(x))) for x in scores]
+        keep = [-(jnp.maximum(x, 0.0) + y) for x, y in zip(scores, logs)]
+        keep = [jnp.where(c, x, 0.0) for c, x in zip(causal, keep)]
+        high = [x.astype(bf16) for x in keep]
+        low = [(x - y.astype(f32)).astype(bf16) for x, y in zip(keep, high)]
+        sums = [nn(jnp.concatenate([x, y], axis=1), tail) for x, y in zip(high, low)]
+        weights = [jnp.exp(x + y[:, :BLOCK]) for x, y in zip(scores, sums)]
+        weights = [jnp.where(c, x, 0.0).astype(bf16) for c, x in zip(causal, weights)]
+        outs = [nt(x, m[HEAD:BLOCK, :]) for x, m in zip(weights, messages)]
+        for x, y in zip(outs, sums):
+            total = total + jnp.exp(later) * x
+            later = later + y[:, BLOCK : BLOCK + HEAD]
+        return later, total
 
     zeros = jnp.zeros((BLOCK, HEAD), f32)
-    _, total = lax.fori_loop(0, chips, chip, (zeros, zeros), unroll=2)
+    _, total = lax.fori_loop(0, chips // WIDTH, step, (zeros, zeros))
     out_ref[...] = jnp.transpose(total).astype(bf16)
 
 
@@ -262,6 +242,9 @@
     ep, tp = lax.axis_size("ep"), lax.axis_size("tp")
     chips = ep // 2
     here = lax.axis_index("ep")
+    run = chips // 4
+    strided = [[(m + 4 * k) * 2 + c for k in range(run)] for m in range(4) for c in range(2)]
+    nearby = [[(m + 4 * k) * 2 + c for m in range(4)] for k in range(run) for c in range(2)]
     side = tp // 4
     along_x = [[y * 4 + x for x in range(4)] for y in range(side)]
     along_y = [[y * 4 + x for y in range(side)] for x in range(4)]
@@ -275,10 +258,6 @@
     square = struct((BLOCK, BLOCK), bf16)
     ids = expert_ids.T
     column = lax.axis_index("tp").reshape(1)
-
-    def from_chip(x, step):
-        moves = [((((z + step) % chips) * 2 + c), z * 2 + c) for z in range(chips) for c in range(2)]
-        return lax.ppermute(x, "ep", moves)
 
     send = call(dispatch_body, 1, 3, slots, 1 << 27, hbm=(1, 2, 3))(
         column, expert_rows, expert_gain[None, :], ids
@@ -293,25 +272,18 @@
         value_weight.T,
         key_bias,
     )
-    behind1 = from_chip(message, -1)
-    ahead1 = from_chip(message, 1)
     swaps = [(k, k ^ 1) for k in range(tp)]
-    other_weights = lax.ppermute(
-        jnp.concatenate([gate_weight[0], up_weight[0]], axis=0), "tp", swaps
-    )
-    three = packed(behind1, message, ahead1)
-    behind3 = from_chip(three, -3)
-    ahead3 = from_chip(three, 3)
+    other_gate = lax.ppermute(gate_weight[0], "tp", swaps)
+    other_up = lax.ppermute(up_weight[0], "tp", swaps)
+    keys = lax.all_gather(message, "ep", axis=0, tiled=True, axis_index_groups=strided)
     routed = call_out(halves_body, 0, 1, struct((tp, ROWS, BLOCK), bf16), 1 << 24, [])(routed)
     routed = exchange(routed, "tp")
-    seven = packed_seven(behind3, three, ahead3)
-    far = from_chip(seven, 8)
+    own = lax.all_gather(keys, "ep", axis=0, tiled=True, axis_index_groups=nearby)
     own_hidden = [pltpu.VMEM((SLOTS, BLOCK), bf16)]
-    hidden = call_out(hidden_body, 1, 4, copies, 1 << 29, own_hidden)(
-        column, routed, gate_weight[0], up_weight[0], other_weights
+    hidden = call_out(hidden_body, 1, 5, copies, 1 << 29, own_hidden)(
+        column, routed, gate_weight[0], up_weight[0], other_gate, other_up
     )
     hidden = exchange(hidden, "tp")
-    own = packed(behind3, three, ahead3, far)
     other = lax.ppermute(own, "ep", [(e, e ^ 1) for e in range(ep)])
     attended = call(attend_body, 1, 3, struct((HEAD, BLOCK), bf16), 1 << 30)(
         here.reshape(1), query, own, other

time: 184 us -> 165 us (0.90)
  blocking collectives: 24.7 us -> 90.5 us
  starting transfers between devices: 76.6 us -> 29.4 us
  waiting for transfers between devices: 53.1 us -> 28.2 us
  Pallas kernels: 24.4 us -> 14.3 us
  other arithmetic: 2.26 us -> 0 us
    all_gather x0 -> x2, blocking collectives: none -> 33.1 us  [the longest x1 17.7 us: shards(): lax.all_gather(message, 'ep', axis=0, tiled=True, axis_index_groups=strided)]
    all_to_all x0 -> x1, blocking collectives: none -> 32.5 us  [exchange(): return lax.all_to_all(x, axis, split_axis=0, concat_axis=0, tiled=True)]
    all_to_all x4 -> x3, starting transfers between devices: 48 us -> 21.6 us  [exchange(): return lax.all_to_all(x, axis, split_axis=0, concat_axis=0, tiled=True)]
    all_to_all x4 -> x3, waiting for transfers between devices: 23.2 us -> 0.01 us  [exchange(): return lax.all_to_all(x, axis, split_axis=0, concat_axis=0, tiled=True)]
    ppermute x6 -> x2, starting transfers between devices: 26.6 us -> 5.84 us  [the longest x1 3.08 us: shards(): other_up = lax.ppermute(up_weight[0], 'tp', swaps)]
    pallas_call x11 -> x8, Pallas kernels: 24.4 us -> 14.3 us  [run(): return kernel(*args)]
    concatenate x1 -> x0, other arithmetic: 2.26 us -> none  [shards(): jnp.concatenate([gate_weight[0], up_weight[0]], axis=0)]
    ppermute x6 -> x2, waiting for transfers between devices: 29.9 us -> 28.2 us  [the longest x1 19.2 us: shards(): other_gate = lax.ppermute(gate_weight[0], 'tp', swaps)]
  transfers between devices with their start and end apart: 11 -> 6, of which waited for: 7 -> 2; matrix products, arithmetic and copies ran while one was open for 1% -> 0% of each run, Pallas kernels for 10% -> 5%
where the time goes in v3:
time: 165 us; the launch traced here: 163 us
  blocking collectives  90.5 us (55%)
  starting transfers between devices  29.4 us (18%)
  waiting for transfers between devices  28.2 us (17%)
  Pallas kernels  14.3 us (9%)
    all_to_all x1, blocking collectives, exchange(): return lax.all_to_all(x, axis, split_axis=0, concat_axis=0, tiled=True)  32.5 us
    all_gather x2, blocking collectives, shards(): lax.all_gather(attended, 'tp', axis=0, tiled=True, axis_index_groups=alon...  24.9 us
    all_to_all x3, starting transfers between devices, exchange(): return lax.all_to_all(x, axis, split_axis=0, concat_axis=0, tiled=True)  21.6 us
    ppermute x1, waiting for transfers between devices, shards(): other_gate = lax.ppermute(gate_weight[0], 'tp', swaps)  19.2 us
    all_gather x1, blocking collectives, shards(): lax.all_gather(message, 'ep', axis=0, tiled=True, axis_index_groups=strided)  17.7 us
    all_gather x1, blocking collectives, shards(): lax.all_gather(keys, 'ep', axis=0, tiled=True, axis_index_groups=nearby)  15.3 us
    pallas_call x8, Pallas kernels, run(): return kernel(*args)  14.3 us
    ppermute x1, waiting for transfers between devices, shards(): other_up = lax.ppermute(up_weight[0], 'tp', swaps)  8.97 us
  transfers between devices with their start and end apart: 6, of which 2 were waited for; matrix products, arithmetic and copies ran while one was open for 0% of the time, Pallas kernels for 5%

profile of v3, /device:TPU:6, one launch (start us, length us, event | category | flops | bytes accessed | tf_op | source)
XLA Modules:
  0.0 163.2 jit_solution(10012131457029925377)
XLA Ops:
  0.7 1.5 shard_map.161
  2.2 32.5 %all_to_all.20 = bf16[32,16,128]{2,1,0:T(8,128)(2,1)S(1)} all-to-all(bf16[32,16,128]{2,1,0:T(8,128)(2,1)S(1)} %bitcast.18), channel_id=1, replica_groups=mesh['ep'=32,'tp'=16] {'ep'}, dimensions={0} | all-to-all | bytes 262144 | tf_op jit(solution)/shard_map/all_to_all | solution.py:254
  34.6 1.1 shard_map.162
  35.8 7.4 %all-to-all-start.1 = ((bf16[16,256,128]{2,1,0:T(8,128)(2,1)}), bf16[16,256,128]{2,1,0:T(8,128)(2,1)S(1)}, u32[]{:S(2)}, u32[]{:S(2)}) async-start(bf16[16,256,128]{2,1,0:T(8,128)(2,1)} %shard_map.162), calls=%async_computation.1 | async-start | bytes 2097152 | tf_op jit(solution)/shard_map/all_to_all | solution.py:254
  43.2 2.8 %collective-permute-start.1 = (bf16[2048,128]{1,0:T(8,128)(2,1)S(1)}, bf16[2048,128]{1,0:T(8,128)(2,1)S(1)}, u32[]{:S(2)}, u32[]{:S(2)}) collective-permute-start(bf16[2048,128]{1,0:T(8,128)(2,1)S(1)} %bitcast.20), channel_id=1, source_target_pairs={{0,1},{1,0},{2,3},{3,2},{4,5},{5,4},{6,7},{7,6},{8,9},{9,8},{10,11... | collective-permute-start | bytes 1572872 | tf_op jit(solution)/shard_map/ppermute | solution.py:276
  46.0 3.1 %collective-permute-start.2 = (bf16[2048,128]{1,0:T(8,128)(2,1)S(1)}, bf16[2048,128]{1,0:T(8,128)(2,1)S(1)}, u32[]{:S(2)}, u32[]{:S(2)}) collective-permute-start(bf16[2048,128]{1,0:T(8,128)(2,1)S(1)} %bitcast.22), channel_id=1, source_target_pairs={{0,1},{1,0},{2,3},{3,2},{4,5},{5,4},{6,7},{7,6},{8,9},{9,8},{10,11... | collective-permute-start | bytes 1572872 | tf_op jit(solution)/shard_map/ppermute | solution.py:277
  49.1 19.2 %collective-permute-done.1.g1_ref = bf16[2048,128]{1,0:T(8,128)(2,1)S(1)} collective-permute-done((bf16[2048,128]{1,0:T(8,128)(2,1)S(1)}, bf16[2048,128]{1,0:T(8,128)(2,1)S(1)}, u32[]{:S(2)}, u32[]{:S(2)}) %collective-permute-start.1) | collective-permute-done | bytes 524320 | tf_op jit(solution)/shard_map/ppermute | solution.py:276
  68.3 9.0 %collective-permute-done.2.u1_ref = bf16[2048,128]{1,0:T(8,128)(2,1)S(1)} collective-permute-done((bf16[2048,128]{1,0:T(8,128)(2,1)S(1)}, bf16[2048,128]{1,0:T(8,128)(2,1)S(1)}, u32[]{:S(2)}, u32[]{:S(2)}) %collective-permute-start.2) | collective-permute-done | bytes 524320 | tf_op jit(solution)/shard_map/ppermute | solution.py:277
  77.2 2.2 %shard_map.163 = bf16[16,512,128]{2,1,0:T(8,128)(2,1)} custom-call(s32[1]{0:T(128)} %bitcast.8.tp_ref, bf16[16,256,128]{2,1,0:T(8,128)(2,1)S(1)} %all-to-all-done.1.x_ref, bf16[2048,128]{1,0:T(8,128)(2,1)S(1)} %bitcast.21, bf16[2048,128]{1,0:T(8,128)(2,1)S(1)} %bitcast.23, bf16[2048,128]{1,0:T(8,128)(2,1)S(1)} %collective-permute-done.1.g1_ref, ...), custom_call_target="tpu_custom_call" | custom-call | flops 536870912 | bytes 1048576 | tf_op jit(solution)/shard_map/pallas_call | solution.py:34
  79.4 7.6 %all-to-all-start.2 = ((bf16[16,512,128]{2,1,0:T(8,128)(2,1)}), bf16[16,512,128]{2,1,0:T(8,128)(2,1)S(1)}, u32[]{:S(2)}, u32[]{:S(2)}) async-start(bf16[16,512,128]{2,1,0:T(8,128)(2,1)} %shard_map.163), calls=%async_computation.2 | async-start | bytes 4194304 | tf_op jit(solution)/shard_map/all_to_all | solution.py:254
  87.0 1.9 %shard_map.158 = (bf16[128,64]{1,0:T(8,128)(2,1)S(1)}, bf16[144,128]{1,0:T(8,128)(2,1)S(1)}) custom-call(bf16[128,2048]{1,0:T(8,128)(2,1)} %rows_ref.2, f32[1,2048]{1,0:T(1,128)} %bitcast.33, bf16[64,2048]{1,0:T(8,128)(2,1)} %bitcast.29, bf16[64,2048]{1,0:T(8,128)(2,1)} %bitcast.30, bf16[64,2048]{1,0:T(8,128)(2,1)} %bitcast.31, bf16[1,128]{1,0:T(2,128)(2,1)} %bias_ref.1), custom_call_target="tpu_custom_call" | custom-call | flops 268435456 | bytes 1048576 | tf_op jit(solution)/shard_map/pallas_call | solution.py:34
  88.9 17.7 %all_gather.12 = bf16[576,128]{1,0:T(8,128)(2,1)S(1)} all-gather(bf16[144,128]{1,0:T(8,128)(2,1)S(1)} %get-tuple-element.5), channel_id=1, replica_groups={{0,128,256,384},{16,144,272,400},{32,160,288,416},{48,176,304,432},{64,..., dimensions={0}, use_global_device_ids=true | all-gather | bytes 184320 | tf_op jit(solution)/shard_map/all_gather | solution.py:278
  106.7 15.3 %all_gather.13.own_ref = bf16[2304,128]{1,0:T(8,128)(2,1)S(1)} all-gather(bf16[576,128]{1,0:T(8,128)(2,1)S(1)} %all_gather.12), channel_id=1, replica_groups={{0,32,64,96},{16,48,80,112},{128,160,192,224},{144,176,208,240},{256,28..., dimensions={0}, use_global_device_ids=true | all-gather | bytes 737280 | tf_op jit(solution)/shard_map/all_gather | solution.py:281
  122.0 1.9 %collective-permute-start = (bf16[2304,128]{1,0:T(8,128)(2,1)S(1)}, bf16[2304,128]{1,0:T(8,128)(2,1)}, u32[]{:S(2)}, u32[]{:S(2)}) collective-permute-start(bf16[2304,128]{1,0:T(8,128)(2,1)S(1)} %all_gather.13.own_ref), channel_id=1, source_target_pairs={{0,16},{16,0},{32,48},{48,32},{64,80},{80,64},{96,112},{112,96},{1... | collective-permute-start | bytes 1769480 | tf_op jit(solution)/shard_map/ppermute | solution.py:287
  123.9 1.4 shard_map.164
  125.3 6.6 %all-to-all-start.3 = ((bf16[32,16,128]{2,1,0:T(8,128)(2,1)}), bf16[32,16,128]{2,1,0:T(8,128)(2,1)S(1)}, u32[]{:S(2)}, u32[]{:S(2)}) async-start(bf16[32,16,128]{2,1,0:T(8,128)(2,1)} %bitcast.15), calls=%async_computation.3 | async-start | bytes 262144 | tf_op jit(solution)/shard_map/all_to_all | solution.py:254
  131.9 0.0 copy-start.3
  131.9 0.0 copy-start.4
  132.0 0.0 copy-start.5
  132.0 4.2 %shard_map.159 = bf16[64,128]{1,0:T(8,128)(2,1)S(1)} custom-call(s32[1]{0:T(128)} %bitcast.pos_ref, bf16[128,64]{1,0:T(8,128)(2,1)S(1)} %get-tuple-element.4.q_ref, bf16[2304,128]{1,0:T(8,128)(2,1)S(1)} %all_gather.13.own_ref, bf16[2304,128]{1,0:T(8,128)(2,1)} %collective-permute-done.other_ref), custom_call_target="tpu_custom_call" | custom-call | flops 1073741824 | bytes 1048576 | tf_op jit(solution)/shard_map/pallas_call | solution.py:34
  136.2 11.9 %all_gather.14 = bf16[256,128]{1,0:T(8,128)(2,1)S(1)} all-gather(bf16[64,128]{1,0:T(8,128)(2,1)S(1)} %shard_map.159), channel_id=1, replica_groups={{0,1,2,3},{4,5,6,7},{8,9,10,11},{12,13,14,15},{16,17,18,19},{20,21,22,2..., dimensions={0}, use_global_device_ids=true | all-gather | bytes 81920 | tf_op jit(solution)/shard_map/all_gather | solution.py:291
  148.0 13.1 %all_gather.15.x_ref = bf16[1024,128]{1,0:T(8,128)(2,1)S(1)} all-gather(bf16[256,128]{1,0:T(8,128)(2,1)S(1)} %all_gather.14), channel_id=1, replica_groups={{0,4,8,12},{1,5,9,13},{2,6,10,14},{3,7,11,15},{16,20,24,28},{17,21,25,2..., dimensions={0}, use_global_device_ids=true | all-gather | bytes 327680 | tf_op jit(solution)/shard_map/all_gather | solution.py:294
  161.1 0.9 shard_map.160
  162.0 1.1 shard_map.165
  (15 shorter events, 0.0 us)
Async XLA Ops:
  0.6 42.6 %copy-start.1 = (bf16[1,2048,128]{2,1,0:T(8,128)(2,1)S(1)}, bf16[1,2048,128]{2,1,0:T(8,128)(2,1)}, u32[]{:S(2)}) copy-start(bf16[1,2048,128]{2,1,0:T(8,128)(2,1)} %param.27) | copy-start | bytes 1572868
  0.6 45.3 %copy-start.2 = (bf16[1,2048,128]{2,1,0:T(8,128)(2,1)S(1)}, bf16[1,2048,128]{2,1,0:T(8,128)(2,1)}, u32[]{:S(2)}) copy-start(bf16[1,2048,128]{2,1,0:T(8,128)(2,1)} %param.28) | copy-start | bytes 1572868
  35.8 41.5 %all-to-all-start.1 = ((bf16[16,256,128]{2,1,0:T(8,128)(2,1)}), bf16[16,256,128]{2,1,0:T(8,128)(2,1)S(1)}, u32[]{:S(2)}, u32[]{:S(2)}) async-start(bf16[16,256,128]{2,1,0:T(8,128)(2,1)} %shard_map.162), calls=%async_computation.1 | async-start | bytes 2097152 | tf_op jit(solution)/shard_map/all_to_all | solution.py:254
  43.2 25.1 %collective-permute-start.1 = (bf16[2048,128]{1,0:T(8,128)(2,1)S(1)}, bf16[2048,128]{1,0:T(8,128)(2,1)S(1)}, u32[]{:S(2)}, u32[]{:S(2)}) collective-permute-start(bf16[2048,128]{1,0:T(8,128)(2,1)S(1)} %bitcast.20), channel_id=1, source_target_pairs={{0,1},{1,0},{2,3},{3,2},{4,5},{5,4},{6,7},{7,6},{8,9},{9,8},{10,11... | collective-permute-start | bytes 1572872 | tf_op jit(solution)/shard_map/ppermute | solution.py:276
  46.0 31.2 %collective-permute-start.2 = (bf16[2048,128]{1,0:T(8,128)(2,1)S(1)}, bf16[2048,128]{1,0:T(8,128)(2,1)S(1)}, u32[]{:S(2)}, u32[]{:S(2)}) collective-permute-start(bf16[2048,128]{1,0:T(8,128)(2,1)S(1)} %bitcast.22), channel_id=1, source_target_pairs={{0,1},{1,0},{2,3},{3,2},{4,5},{5,4},{6,7},{7,6},{8,9},{9,8},{10,11... | collective-permute-start | bytes 1572872 | tf_op jit(solution)/shard_map/ppermute | solution.py:277
  79.4 44.5 %all-to-all-start.2 = ((bf16[16,512,128]{2,1,0:T(8,128)(2,1)}), bf16[16,512,128]{2,1,0:T(8,128)(2,1)S(1)}, u32[]{:S(2)}, u32[]{:S(2)}) async-start(bf16[16,512,128]{2,1,0:T(8,128)(2,1)} %shard_map.163), calls=%async_computation.2 | async-start | bytes 4194304 | tf_op jit(solution)/shard_map/all_to_all | solution.py:254
  87.0 36.9 %copy-start = (bf16[1,2048,128]{2,1,0:T(8,128)(2,1)S(1)}, bf16[1,2048,128]{2,1,0:T(8,128)(2,1)}, u32[]{:S(2)}) copy-start(bf16[1,2048,128]{2,1,0:T(8,128)(2,1)} %param.29) | copy-start | bytes 1572868
  122.0 9.9 %collective-permute-start = (bf16[2304,128]{1,0:T(8,128)(2,1)S(1)}, bf16[2304,128]{1,0:T(8,128)(2,1)}, u32[]{:S(2)}, u32[]{:S(2)}) collective-permute-start(bf16[2304,128]{1,0:T(8,128)(2,1)S(1)} %all_gather.13.own_ref), channel_id=1, source_target_pairs={{0,16},{16,0},{32,48},{48,32},{64,80},{80,64},{96,112},{112,96},{1... | collective-permute-start | bytes 1769480 | tf_op jit(solution)/shard_map/ppermute | solution.py:287
  125.3 36.7 %all-to-all-start.3 = ((bf16[32,16,128]{2,1,0:T(8,128)(2,1)}), bf16[32,16,128]{2,1,0:T(8,128)(2,1)S(1)}, u32[]{:S(2)}, u32[]{:S(2)}) async-start(bf16[32,16,128]{2,1,0:T(8,128)(2,1)} %bitcast.15), calls=%async_computation.3 | async-start | bytes 262144 | tf_op jit(solution)/shard_map/all_to_all | solution.py:254
  131.9 29.2 %copy-start.3 = (bf16[1024,128]{1,0:T(8,128)(2,1)S(1)}, bf16[1024,128]{1,0:T(8,128)(2,1)}, u32[]{:S(2)}) copy-start(bf16[1024,128]{1,0:T(8,128)(2,1)} %w_ref.1) | copy-start | bytes 786436
  131.9 30.1 %copy-start.4 = (s32[128,2]{0,1:T(2,128)S(1)}, s32[128,2]{0,1:T(2,128)}, u32[]{:S(2)}) copy-start(s32[128,2]{0,1:T(2,128)} %param.24) | copy-start | bytes 3076
  132.0 30.1 %copy-start.5 = (f32[128,4]{0,1:T(4,128)S(1)}, f32[128,4]{0,1:T(4,128)}, u32[]{:S(2)}) copy-start(f32[128,4]{0,1:T(4,128)} %param.25) | copy-start | bytes 6148
  132.0 30.1 %copy-start.6 = (f32[128,2]{0,1:T(2,128)S(1)}, f32[128,2]{0,1:T(2,128)}, u32[]{:S(2)}) copy-start(f32[128,2]{0,1:T(2,128)} %param.26) | copy-start | bytes 3076

commit v4 on v3

--- a/solution.py
+++ b/solution.py
@@ -44,8 +44,8 @@
     return run
 
 
-def call_out(body, n_scalar, n_in, out, flops, scratch):
-    copies = [pltpu.SemaphoreType.DMA((out.shape[0],))]
+def call_out(body, n_scalar, n_in, out, flops, scratch, copies):
+    copies = [pltpu.SemaphoreType.DMA((copies,))]
     more = {"out_specs": pl.BlockSpec(memory_space=pltpu.HBM), "scratch_shapes": scratch + copies}
     return call(body, n_scalar, n_in, pltpu.HBM(out.shape, out.dtype), flops, **more)
 
@@ -116,22 +116,27 @@
 def hidden_body(tp_ref, x_ref, g0_ref, u0_ref, g1_ref, u1_ref, out_ref, hidden_ref, sems):
     parts = x_ref.shape[0]
     even = tp_ref[0] % 2 == 0
-    x = jnp.concatenate([x_ref[k] for k in range(parts)], axis=1)
-    own = nn(x, jnp.concatenate([g0_ref[...], u0_ref[...]], axis=1))
-    other = nn(x, jnp.concatenate([g1_ref[...], u1_ref[...]], axis=1))
+    own_weights = jnp.concatenate([g0_ref[...], u0_ref[...]], axis=1)
+    other_weights = jnp.concatenate([g1_ref[...], u1_ref[...]], axis=1)
 
     def gated(both):
         gate, up = both[:, :BLOCK], both[:, BLOCK:]
-        return (gate * jax.nn.sigmoid(gate) * up).astype(bf16).astype(f32)
-
-    own, other = gated(own), gated(other)
-    first = jnp.where(even, own, other).astype(bf16)
-    second = jnp.where(even, other, own).astype(bf16)
-    hidden_ref[0:ROWS, :] = first
-    hidden_ref[ROWS:SLOTS, :] = second
-    copies = [pltpu.make_async_copy(hidden_ref, out_ref.at[k], sems.at[k]) for k in range(parts)]
-    for copy in copies:
-        copy.start()
+        return gate * jax.nn.sigmoid(gate) * up
+
+    copies = []
+    for m in range(2):
+        x = [x_ref[k, m * BLOCK : (m + 1) * BLOCK, :] for k in range(parts)]
+        x = jnp.concatenate(x, axis=1)
+        own, other = gated(nn(x, own_weights)), gated(nn(x, other_weights))
+        span = slice(m * ROWS, (m + 1) * ROWS)
+        hidden_ref[m * ROWS : m * ROWS + BLOCK, :] = jnp.where(even, own, other).astype(bf16)
+        hidden_ref[m * ROWS + BLOCK : (m + 1) * ROWS, :] = jnp.where(even, other, own).astype(bf16)
+        for k in range(parts):
+            target = out_ref.at[k, span, :]
+            copies.append(
+                pltpu.make_async_copy(hidden_ref.at[span, :], target, sems.at[m * parts + k])
+            )
+            copies[-1].start()
     for copy in copies:
         copy.wait()
 
@@ -139,15 +144,18 @@
 def down_body(x_ref, w_ref, out_ref):
     parts = x_ref.shape[0]
     for half in range(2):
-        x = jnp.concatenate(
-            [
-                x_ref[k, e * ROWS : (e + 1) * ROWS, :]
-                for k in range(half, parts, 2)
-                for e in range(2)
-            ],
-            axis=1,
-        )
-        out_ref[half * ROWS : (half + 1) * ROWS, :] = nn(x, w_ref[...]).astype(bf16)
+        for m in range(2):
+            at = m * ROWS
+            x = jnp.concatenate(
+                [
+                    x_ref[k, at + e * BLOCK : at + (e + 1) * BLOCK, :]
+                    for k in range(half, parts, 2)
+                    for e in range(2)
+                ],
+                axis=1,
+            )
+            at = half * ROWS + m * BLOCK
+            out_ref[at : at + BLOCK, :] = nn(x, w_ref[...]).astype(bf16)
 
 
 def attend_body(pos_ref, q_ref, own_ref, other_ref, out_ref):
@@ -245,9 +253,6 @@
     run = chips // 4
     strided = [[(m + 4 * k) * 2 + c for k in range(run)] for m in range(4) for c in range(2)]
     nearby = [[(m + 4 * k) * 2 + c for m in range(4)] for k in range(run) for c in range(2)]
-    side = tp // 4
-    along_x = [[y * 4 + x for x in range(4)] for y in range(side)]
-    along_y = [[y * 4 + x for y in range(side)] for x in range(4)]
     struct = jax.ShapeDtypeStruct
 
     def exchange(x, axis):
@@ -276,11 +281,11 @@
     other_gate = lax.ppermute(gate_weight[0], "tp", swaps)
     other_up = lax.ppermute(up_weight[0], "tp", swaps)
     keys = lax.all_gather(message, "ep", axis=0, tiled=True, axis_index_groups=strided)
-    routed = call_out(halves_body, 0, 1, struct((tp, ROWS, BLOCK), bf16), 1 << 24, [])(routed)
+    routed = call_out(halves_body, 0, 1, struct((tp, ROWS, BLOCK), bf16), 1 << 24, [], tp)(routed)
     routed = exchange(routed, "tp")
     own = lax.all_gather(keys, "ep", axis=0, tiled=True, axis_index_groups=nearby)
     own_hidden = [pltpu.VMEM((SLOTS, BLOCK), bf16)]
-    hidden = call_out(hidden_body, 1, 5, copies, 1 << 29, own_hidden)(
+    hidden = call_out(hidden_body, 1, 5, copies, 1 << 29, own_hidden, 2 * tp)(
         column, routed, gate_weight[0], up_weight[0], other_gate, other_up
     )
     hidden = exchange(hidden, "tp")
@@ -288,10 +293,9 @@
     attended = call(attend_body, 1, 3, struct((HEAD, BLOCK), bf16), 1 << 30)(
         here.reshape(1), query, own, other
     )
-    attended = lax.all_gather(attended, "tp", axis=0, tiled=True, axis_index_groups=along_x)
     result = call(down_body, 0, 2, slots, 1 << 28)(hidden, down_weight[0])
     back = exchange(result.reshape(ep, CAP, BLOCK), "ep").reshape(SLOTS, BLOCK)
-    attended = lax.all_gather(attended, "tp", axis=0, tiled=True, axis_index_groups=along_y)
+    attended = lax.all_gather(attended, "tp", axis=0, tiled=True)
     mixed = call(mix_body, 0, 2, square, 1 << 26)(attended, out_weight)
     expert_out = call(combine_body, 0, 4, square, 1 << 27)(ids, group_logits.T, pair_logits.T, back)
     return (mixed, expert_out)

time: 165 us -> 163 us (0.988)
    all_gather x2 -> x1, blocking collectives: 24.9 us -> 23.9 us  [shards(): attended = lax.all_gather(attended, 'tp', axis=0, tiled=True)]
where the time goes in v4:
time: 163 us; the launch traced here: 162 us
  blocking collectives  88.9 us (55%)
  starting transfers between devices  29.9 us (18%)
  waiting for transfers between devices  28.2 us (17%)
  Pallas kernels  14.3 us (9%)
    all_to_all x1, blocking collectives, exchange(): return lax.all_to_all(x, axis, split_axis=0, concat_axis=0, tiled=True)  32.5 us
    all_gather x1, blocking collectives, shards(): attended = lax.all_gather(attended, 'tp', axis=0, tiled=True)  23.9 us
    all_to_all x3, starting transfers between devices, exchange(): return lax.all_to_all(x, axis, split_axis=0, concat_axis=0, tiled=True)  22.1 us
    ppermute x1, waiting for transfers between devices, shards(): other_gate = lax.ppermute(gate_weight[0], 'tp', swaps)  19.2 us
    all_gather x1, blocking collectives, shards(): lax.all_gather(message, 'ep', axis=0, tiled=True, axis_index_groups=strided)  17.5 us
    all_gather x1, blocking collectives, shards(): lax.all_gather(keys, 'ep', axis=0, tiled=True, axis_index_groups=nearby)  15.1 us
    pallas_call x8, Pallas kernels, run(): return kernel(*args)  14.3 us
    ppermute x1, waiting for transfers between devices, shards(): other_up = lax.ppermute(up_weight[0], 'tp', swaps)  8.97 us
  transfers between devices with their start and end apart: 6, of which 2 were waited for; matrix products, arithmetic and copies ran while one was open for 0% of the time, Pallas kernels for 5%

profile of v4, /device:TPU:6, one launch (start us, length us, event | category | flops | bytes accessed | tf_op | source)
XLA Modules:
  0.0 162.2 jit_solution(1339824522824002841)
XLA Ops:
  0.7 1.5 shard_map.161
  2.2 32.5 %all_to_all.20 = bf16[32,16,128]{2,1,0:T(8,128)(2,1)S(1)} all-to-all(bf16[32,16,128]{2,1,0:T(8,128)(2,1)S(1)} %bitcast.18), channel_id=1, replica_groups=mesh['ep'=32,'tp'=16] {'ep'}, dimensions={0} | all-to-all | bytes 262144 | tf_op jit(solution)/shard_map/all_to_all | solution.py:259
  34.6 1.1 shard_map.162
  35.8 7.4 %all-to-all-start.1 = ((bf16[16,256,128]{2,1,0:T(8,128)(2,1)}), bf16[16,256,128]{2,1,0:T(8,128)(2,1)S(1)}, u32[]{:S(2)}, u32[]{:S(2)}) async-start(bf16[16,256,128]{2,1,0:T(8,128)(2,1)} %shard_map.162), calls=%async_computation.1 | async-start | bytes 2097152 | tf_op jit(solution)/shard_map/all_to_all | solution.py:259
  43.2 2.8 %collective-permute-start.1 = (bf16[2048,128]{1,0:T(8,128)(2,1)S(1)}, bf16[2048,128]{1,0:T(8,128)(2,1)S(1)}, u32[]{:S(2)}, u32[]{:S(2)}) collective-permute-start(bf16[2048,128]{1,0:T(8,128)(2,1)S(1)} %bitcast.20), channel_id=1, source_target_pairs={{0,1},{1,0},{2,3},{3,2},{4,5},{5,4},{6,7},{7,6},{8,9},{9,8},{10,11... | collective-permute-start | bytes 1572872 | tf_op jit(solution)/shard_map/ppermute | solution.py:281
  46.0 3.1 %collective-permute-start.2 = (bf16[2048,128]{1,0:T(8,128)(2,1)S(1)}, bf16[2048,128]{1,0:T(8,128)(2,1)S(1)}, u32[]{:S(2)}, u32[]{:S(2)}) collective-permute-start(bf16[2048,128]{1,0:T(8,128)(2,1)S(1)} %bitcast.22), channel_id=1, source_target_pairs={{0,1},{1,0},{2,3},{3,2},{4,5},{5,4},{6,7},{7,6},{8,9},{9,8},{10,11... | collective-permute-start | bytes 1572872 | tf_op jit(solution)/shard_map/ppermute | solution.py:282
  49.1 19.2 %collective-permute-done.1.g1_ref = bf16[2048,128]{1,0:T(8,128)(2,1)S(1)} collective-permute-done((bf16[2048,128]{1,0:T(8,128)(2,1)S(1)}, bf16[2048,128]{1,0:T(8,128)(2,1)S(1)}, u32[]{:S(2)}, u32[]{:S(2)}) %collective-permute-start.1) | collective-permute-done | bytes 524320 | tf_op jit(solution)/shard_map/ppermute | solution.py:281
  68.3 9.0 %collective-permute-done.2.u1_ref = bf16[2048,128]{1,0:T(8,128)(2,1)S(1)} collective-permute-done((bf16[2048,128]{1,0:T(8,128)(2,1)S(1)}, bf16[2048,128]{1,0:T(8,128)(2,1)S(1)}, u32[]{:S(2)}, u32[]{:S(2)}) %collective-permute-start.2) | collective-permute-done | bytes 524320 | tf_op jit(solution)/shard_map/ppermute | solution.py:282
  77.2 2.2 %shard_map.163 = bf16[16,512,128]{2,1,0:T(8,128)(2,1)} custom-call(s32[1]{0:T(128)} %bitcast.8.tp_ref, bf16[16,256,128]{2,1,0:T(8,128)(2,1)S(1)} %all-to-all-done.1.x_ref, bf16[2048,128]{1,0:T(8,128)(2,1)S(1)} %bitcast.21, bf16[2048,128]{1,0:T(8,128)(2,1)S(1)} %bitcast.23, bf16[2048,128]{1,0:T(8,128)(2,1)S(1)} %collective-permute-done.1.g1_ref, ...), custom_call_target="tpu_custom_call" | custom-call | flops 536870912 | bytes 1048576 | tf_op jit(solution)/shard_map/pallas_call | solution.py:34
  79.4 7.6 %all-to-all-start.2 = ((bf16[16,512,128]{2,1,0:T(8,128)(2,1)}), bf16[16,512,128]{2,1,0:T(8,128)(2,1)S(1)}, u32[]{:S(2)}, u32[]{:S(2)}) async-start(bf16[16,512,128]{2,1,0:T(8,128)(2,1)} %shard_map.163), calls=%async_computation.2 | async-start | bytes 4194304 | tf_op jit(solution)/shard_map/all_to_all | solution.py:259
  87.0 1.9 %shard_map.158 = (bf16[128,64]{1,0:T(8,128)(2,1)S(1)}, bf16[144,128]{1,0:T(8,128)(2,1)S(1)}) custom-call(bf16[128,2048]{1,0:T(8,128)(2,1)} %rows_ref.2, f32[1,2048]{1,0:T(1,128)} %bitcast.33, bf16[64,2048]{1,0:T(8,128)(2,1)} %bitcast.29, bf16[64,2048]{1,0:T(8,128)(2,1)} %bitcast.30, bf16[64,2048]{1,0:T(8,128)(2,1)} %bitcast.31, bf16[1,128]{1,0:T(2,128)(2,1)} %bias_ref.1), custom_call_target="tpu_custom_call" | custom-call | flops 268435456 | bytes 1048576 | tf_op jit(solution)/shard_map/pallas_call | solution.py:34
  88.9 17.5 %all_gather.9 = bf16[576,128]{1,0:T(8,128)(2,1)S(1)} all-gather(bf16[144,128]{1,0:T(8,128)(2,1)S(1)} %get-tuple-element.5), channel_id=1, replica_groups={{0,128,256,384},{16,144,272,400},{32,160,288,416},{48,176,304,432},{64,..., dimensions={0}, use_global_device_ids=true | all-gather | bytes 184320 | tf_op jit(solution)/shard_map/all_gather | solution.py:283
  106.5 15.1 %all_gather.10.own_ref = bf16[2304,128]{1,0:T(8,128)(2,1)S(1)} all-gather(bf16[576,128]{1,0:T(8,128)(2,1)S(1)} %all_gather.9), channel_id=1, replica_groups={{0,32,64,96},{16,48,80,112},{128,160,192,224},{144,176,208,240},{256,28..., dimensions={0}, use_global_device_ids=true | all-gather | bytes 737280 | tf_op jit(solution)/shard_map/all_gather | solution.py:286
  121.5 1.9 %collective-permute-start = (bf16[2304,128]{1,0:T(8,128)(2,1)S(1)}, bf16[2304,128]{1,0:T(8,128)(2,1)}, u32[]{:S(2)}, u32[]{:S(2)}) collective-permute-start(bf16[2304,128]{1,0:T(8,128)(2,1)S(1)} %all_gather.10.own_ref), channel_id=1, source_target_pairs={{0,16},{16,0},{32,48},{48,32},{64,80},{80,64},{96,112},{112,96},{1... | collective-permute-start | bytes 1769480 | tf_op jit(solution)/shard_map/ppermute | solution.py:292
  123.5 1.4 shard_map.164
  124.8 7.2 %all-to-all-start.3 = ((bf16[32,16,128]{2,1,0:T(8,128)(2,1)}), bf16[32,16,128]{2,1,0:T(8,128)(2,1)S(1)}, u32[]{:S(2)}, u32[]{:S(2)}) async-start(bf16[32,16,128]{2,1,0:T(8,128)(2,1)} %bitcast.15), calls=%async_computation.3 | async-start | bytes 262144 | tf_op jit(solution)/shard_map/all_to_all | solution.py:259
  132.0 0.0 copy-start.3
  132.0 0.0 copy-start.4
  132.0 0.0 copy-start.5
  132.1 0.0 copy-start.6
  132.1 4.2 %shard_map.159 = bf16[64,128]{1,0:T(8,128)(2,1)S(1)} custom-call(s32[1]{0:T(128)} %bitcast.pos_ref, bf16[128,64]{1,0:T(8,128)(2,1)S(1)} %get-tuple-element.4.q_ref, bf16[2304,128]{1,0:T(8,128)(2,1)S(1)} %all_gather.10.own_ref, bf16[2304,128]{1,0:T(8,128)(2,1)} %collective-permute-done.other_ref), custom_call_target="tpu_custom_call" | custom-call | flops 1073741824 | bytes 1048576 | tf_op jit(solution)/shard_map/pallas_call | solution.py:34
  136.3 23.9 %all_gather.11.x_ref = bf16[1024,128]{1,0:T(8,128)(2,1)S(1)} all-gather(bf16[64,128]{1,0:T(8,128)(2,1)S(1)} %shard_map.159), channel_id=1, replica_groups=mesh['ep'=32,'tp'=16] {'tp'}, dimensions={0}, use_global_device_ids=true | all-gather | bytes 278528 | tf_op jit(solution)/shard_map/all_gather | solution.py:298
  160.1 0.9 shard_map.160
  161.0 1.1 shard_map.165
  (14 shorter events, 0.0 us)
Async XLA Ops:
  0.6 42.6 %copy-start.1 = (bf16[1,2048,128]{2,1,0:T(8,128)(2,1)S(1)}, bf16[1,2048,128]{2,1,0:T(8,128)(2,1)}, u32[]{:S(2)}) copy-start(bf16[1,2048,128]{2,1,0:T(8,128)(2,1)} %param.27) | copy-start | bytes 1572868
  0.6 45.3 %copy-start.2 = (bf16[1,2048,128]{2,1,0:T(8,128)(2,1)S(1)}, bf16[1,2048,128]{2,1,0:T(8,128)(2,1)}, u32[]{:S(2)}) copy-start(bf16[1,2048,128]{2,1,0:T(8,128)(2,1)} %param.28) | copy-start | bytes 1572868
  35.8 41.5 %all-to-all-start.1 = ((bf16[16,256,128]{2,1,0:T(8,128)(2,1)}), bf16[16,256,128]{2,1,0:T(8,128)(2,1)S(1)}, u32[]{:S(2)}, u32[]{:S(2)}) async-start(bf16[16,256,128]{2,1,0:T(8,128)(2,1)} %shard_map.162), calls=%async_computation.1 | async-start | bytes 2097152 | tf_op jit(solution)/shard_map/all_to_all | solution.py:259
  43.2 25.1 %collective-permute-start.1 = (bf16[2048,128]{1,0:T(8,128)(2,1)S(1)}, bf16[2048,128]{1,0:T(8,128)(2,1)S(1)}, u32[]{:S(2)}, u32[]{:S(2)}) collective-permute-start(bf16[2048,128]{1,0:T(8,128)(2,1)S(1)} %bitcast.20), channel_id=1, source_target_pairs={{0,1},{1,0},{2,3},{3,2},{4,5},{5,4},{6,7},{7,6},{8,9},{9,8},{10,11... | collective-permute-start | bytes 1572872 | tf_op jit(solution)/shard_map/ppermute | solution.py:281
  46.0 31.2 %collective-permute-start.2 = (bf16[2048,128]{1,0:T(8,128)(2,1)S(1)}, bf16[2048,128]{1,0:T(8,128)(2,1)S(1)}, u32[]{:S(2)}, u32[]{:S(2)}) collective-permute-start(bf16[2048,128]{1,0:T(8,128)(2,1)S(1)} %bitcast.22), channel_id=1, source_target_pairs={{0,1},{1,0},{2,3},{3,2},{4,5},{5,4},{6,7},{7,6},{8,9},{9,8},{10,11... | collective-permute-start | bytes 1572872 | tf_op jit(solution)/shard_map/ppermute | solution.py:282
  79.4 44.0 %all-to-all-start.2 = ((bf16[16,512,128]{2,1,0:T(8,128)(2,1)}), bf16[16,512,128]{2,1,0:T(8,128)(2,1)S(1)}, u32[]{:S(2)}, u32[]{:S(2)}) async-start(bf16[16,512,128]{2,1,0:T(8,128)(2,1)} %shard_map.163), calls=%async_computation.2 | async-start | bytes 4194304 | tf_op jit(solution)/shard_map/all_to_all | solution.py:259
  87.0 36.5 %copy-start = (bf16[1,2048,128]{2,1,0:T(8,128)(2,1)S(1)}, bf16[1,2048,128]{2,1,0:T(8,128)(2,1)}, u32[]{:S(2)}) copy-start(bf16[1,2048,128]{2,1,0:T(8,128)(2,1)} %param.29) | copy-start | bytes 1572868
  121.5 10.5 %collective-permute-start = (bf16[2304,128]{1,0:T(8,128)(2,1)S(1)}, bf16[2304,128]{1,0:T(8,128)(2,1)}, u32[]{:S(2)}, u32[]{:S(2)}) collective-permute-start(bf16[2304,128]{1,0:T(8,128)(2,1)S(1)} %all_gather.10.own_ref), channel_id=1, source_target_pairs={{0,16},{16,0},{32,48},{48,32},{64,80},{80,64},{96,112},{112,96},{1... | collective-permute-start | bytes 1769480 | tf_op jit(solution)/shard_map/ppermute | solution.py:292
  124.8 36.2 %all-to-all-start.3 = ((bf16[32,16,128]{2,1,0:T(8,128)(2,1)}), bf16[32,16,128]{2,1,0:T(8,128)(2,1)S(1)}, u32[]{:S(2)}, u32[]{:S(2)}) async-start(bf16[32,16,128]{2,1,0:T(8,128)(2,1)} %bitcast.15), calls=%async_computation.3 | async-start | bytes 262144 | tf_op jit(solution)/shard_map/all_to_all | solution.py:259
  132.0 28.1 %copy-start.3 = (bf16[1024,128]{1,0:T(8,128)(2,1)S(1)}, bf16[1024,128]{1,0:T(8,128)(2,1)}, u32[]{:S(2)}) copy-start(bf16[1024,128]{1,0:T(8,128)(2,1)} %w_ref.1) | copy-start | bytes 786436
  132.0 29.0 %copy-start.4 = (s32[128,2]{0,1:T(2,128)S(1)}, s32[128,2]{0,1:T(2,128)}, u32[]{:S(2)}) copy-start(s32[128,2]{0,1:T(2,128)} %param.24) | copy-start | bytes 3076
  132.0 29.0 %copy-start.5 = (f32[128,4]{0,1:T(4,128)S(1)}, f32[128,4]{0,1:T(4,128)}, u32[]{:S(2)}) copy-start(f32[128,4]{0,1:T(4,128)} %param.25) | copy-start | bytes 6148
  132.1 29.0 %copy-start.6 = (f32[128,2]{0,1:T(2,128)S(1)}, f32[128,2]{0,1:T(2,128)}, u32[]{:S(2)}) copy-start(f32[128,2]{0,1:T(2,128)} %param.26) | copy-start | bytes 3076

commit v5 on v4

--- a/solution.py
+++ b/solution.py
@@ -158,10 +158,11 @@
             out_ref[at : at + BLOCK, :] = nn(x, w_ref[...]).astype(bf16)
 
 
-def attend_body(pos_ref, q_ref, own_ref, other_ref, out_ref):
+def attend_body(pos_ref, q_ref, own_ref, other_ref, far_ref, far_other_ref, out_ref):
     here = pos_ref[0]
     core = here % 2
-    chips = own_ref.shape[0] // MSG
+    chips = 2 * own_ref.shape[0] // MSG
+    odd = (here // 2) % 2
     q = q_ref[...]
     wide = (2 * BLOCK, 2 * BLOCK)
     row, col = iota(wide, 0), iota(wide, 1)
@@ -176,9 +177,10 @@
         messages, starts = [], []
         for w in range(WIDTH):
             z = chips - 1 - (k * WIDTH + w)
-            at = pl.multiple_of(((z % 4) * (chips // 4) + z // 4) * MSG, 16)
-            own = own_ref[pl.ds(at, MSG), :]
-            other = other_ref[pl.ds(at, MSG), :]
+            at = pl.ds(pl.multiple_of((z // 2) * MSG, 16), MSG)
+            near = odd == (WIDTH - 1 - w) % 2
+            own = jnp.where(near, own_ref[at, :], far_ref[at, :])
+            other = jnp.where(near, other_ref[at, :], far_other_ref[at, :])
             messages += [jnp.where(core == 1, own, other), jnp.where(core == 1, other, own)]
             starts += [(here - 2 * z - 1) * BLOCK, (here - 2 * z) * BLOCK]
         scores = [nn(q, m[0:HEAD, :]) + m[BLOCK : BLOCK + 1, :].astype(f32) for m in messages]
@@ -252,7 +254,10 @@
     here = lax.axis_index("ep")
     run = chips // 4
     strided = [[(m + 4 * k) * 2 + c for k in range(run)] for m in range(4) for c in range(2)]
-    nearby = [[(m + 4 * k) * 2 + c for m in range(4)] for k in range(run) for c in range(2)]
+    pairs = [[(z + 2 * b) * 2 + c for b in range(2)] for z in range(chips) if z % 4 < 2 for c in range(2)]
+    side = tp // 4
+    along_x = [[y * 4 + x for x in range(4)] for y in range(side)]
+    along_y = [[y * 4 + x for y in range(side)] for x in range(4)]
     struct = jax.ShapeDtypeStruct
 
     def exchange(x, axis):
@@ -280,22 +285,26 @@
     swaps = [(k, k ^ 1) for k in range(tp)]
     other_gate = lax.ppermute(gate_weight[0], "tp", swaps)
     other_up = lax.ppermute(up_weight[0], "tp", swaps)
-    keys = lax.all_gather(message, "ep", axis=0, tiled=True, axis_index_groups=strided)
+    keys = lax.all_gather(message, "ep", axis=0, tiled=True, axis_index_groups=pairs)
+    own = lax.all_gather(keys, "ep", axis=0, tiled=True, axis_index_groups=strided)
+    far = lax.ppermute(own, "ep", [(e, e ^ 2) for e in range(ep)])
     routed = call_out(halves_body, 0, 1, struct((tp, ROWS, BLOCK), bf16), 1 << 24, [], tp)(routed)
     routed = exchange(routed, "tp")
-    own = lax.all_gather(keys, "ep", axis=0, tiled=True, axis_index_groups=nearby)
     own_hidden = [pltpu.VMEM((SLOTS, BLOCK), bf16)]
     hidden = call_out(hidden_body, 1, 5, copies, 1 << 29, own_hidden, 2 * tp)(
         column, routed, gate_weight[0], up_weight[0], other_gate, other_up
     )
     hidden = exchange(hidden, "tp")
-    other = lax.ppermute(own, "ep", [(e, e ^ 1) for e in range(ep)])
-    attended = call(attend_body, 1, 3, struct((HEAD, BLOCK), bf16), 1 << 30)(
-        here.reshape(1), query, own, other
-    )
+    cores = [(e, e ^ 1) for e in range(ep)]
+    own_other = lax.ppermute(own, "ep", cores)
+    far_other = lax.ppermute(far, "ep", cores)
+    attended = call(attend_body, 1, 5, struct((HEAD, BLOCK), bf16), 1 << 30)(
+        here.reshape(1), query, own, own_other, far, far_other
+    )
+    attended = lax.all_gather(attended, "tp", axis=0, tiled=True, axis_index_groups=along_x)
     result = call(down_body, 0, 2, slots, 1 << 28)(hidden, down_weight[0])
     back = exchange(result.reshape(ep, CAP, BLOCK), "ep").reshape(SLOTS, BLOCK)
-    attended = lax.all_gather(attended, "tp", axis=0, tiled=True)
+    attended = lax.all_gather(attended, "tp", axis=0, tiled=True, axis_index_groups=along_y)
     mixed = call(mix_body, 0, 2, square, 1 << 26)(attended, out_weight)
     expert_out = call(combine_body, 0, 4, square, 1 << 27)(ids, group_logits.T, pair_logits.T, back)
     return (mixed, expert_out)

time: 163 us -> 165 us (1.012)
  blocking collectives: 88.9 us -> 82.9 us
  waiting for transfers between devices: 28.2 us -> 32.9 us
  starting transfers between devices: 29.9 us -> 33.8 us
    all_gather x3 -> x4, blocking collectives: 56.5 us -> 50.4 us  [the longest x2 24.3 us: shards(): lax.all_gather(attended, 'tp', axis=0, tiled=True, axis_index_groups=alon...]
    ppermute x1 -> x3, waiting for transfers between devices: 0.01 us -> 4.7 us  [the longest x1 4.69 us: shards(): far = lax.ppermute(own, 'ep', [(e, e ^ 2) for e in range(ep)])]
    ppermute x1 -> x3, starting transfers between devices: 1.91 us -> 5.81 us  [the longest x1 1.98 us: shards(): far = lax.ppermute(own, 'ep', [(e, e ^ 2) for e in range(ep)])]
  transfers between devices with their start and end apart: 6 -> 8, of which waited for: 2 -> 3; matrix products, arithmetic and copies ran while one was open for 0% -> 0% of each run, Pallas kernels for 5% -> 5%
where the time goes in v5:
time: 165 us
  blocking collectives  82.9 us (50%)
  starting transfers between devices  33.8 us (20%)
  waiting for transfers between devices  32.9 us (20%)
  Pallas kernels  14.2 us (9%)
    all_to_all x1, blocking collectives, exchange(): return lax.all_to_all(x, axis, split_axis=0, concat_axis=0, tiled=True)  32.5 us
    all_gather x2, blocking collectives, shards(): lax.all_gather(attended, 'tp', axis=0, tiled=True, axis_index_groups=alon...  24.3 us
    all_to_all x3, starting transfers between devices, exchange(): return lax.all_to_all(x, axis, split_axis=0, concat_axis=0, tiled=True)  22.1 us
    all_gather x1, blocking collectives, shards(): lax.all_gather(keys, 'ep', axis=0, tiled=True, axis_index_groups=strided)  20.6 us
    ppermute x1, waiting for transfers between devices, shards(): other_gate = lax.ppermute(gate_weight[0], 'tp', swaps)  19.2 us
    pallas_call x8, Pallas kernels, run(): return kernel(*args)  14.2 us
    ppermute x1, waiting for transfers between devices, shards(): other_up = lax.ppermute(up_weight[0], 'tp', swaps)  8.97 us
    all_gather x1, blocking collectives, shards(): lax.all_gather(message, 'ep', axis=0, tiled=True, axis_index_groups=pairs)  5.57 us
  transfers between devices with their start and end apart: 8, of which 3 were waited for; matrix products, arithmetic and copies ran while one was open for 0% of the time, Pallas kernels for 5%

profile of v5, /device:TPU:6, one launch (start us, length us, event | category | flops | bytes accessed | tf_op | source)
XLA Modules:
  0.0 164.7 jit_solution(10949297856251430606)
XLA Ops:
  0.7 1.5 shard_map.161
  2.2 32.5 %all_to_all.20 = bf16[32,16,128]{2,1,0:T(8,128)(2,1)S(1)} all-to-all(bf16[32,16,128]{2,1,0:T(8,128)(2,1)S(1)} %bitcast.18), channel_id=1, replica_groups=mesh['ep'=32,'tp'=16] {'ep'}, dimensions={0} | all-to-all | bytes 262144 | tf_op jit(solution)/shard_map/all_to_all | solution.py:264
  34.6 1.1 shard_map.162
  35.8 7.4 %all-to-all-start.1 = ((bf16[16,256,128]{2,1,0:T(8,128)(2,1)}), bf16[16,256,128]{2,1,0:T(8,128)(2,1)S(1)}, u32[]{:S(2)}, u32[]{:S(2)}) async-start(bf16[16,256,128]{2,1,0:T(8,128)(2,1)} %shard_map.162), calls=%async_computation.1 | async-start | bytes 2097152 | tf_op jit(solution)/shard_map/all_to_all | solution.py:264
  43.2 2.8 %collective-permute-start.3 = (bf16[2048,128]{1,0:T(8,128)(2,1)S(1)}, bf16[2048,128]{1,0:T(8,128)(2,1)S(1)}, u32[]{:S(2)}, u32[]{:S(2)}) collective-permute-start(bf16[2048,128]{1,0:T(8,128)(2,1)S(1)} %bitcast.20), channel_id=1, source_target_pairs={{0,1},{1,0},{2,3},{3,2},{4,5},{5,4},{6,7},{7,6},{8,9},{9,8},{10,11... | collective-permute-start | bytes 1572872 | tf_op jit(solution)/shard_map/ppermute | solution.py:286
  46.0 3.1 %collective-permute-start.4 = (bf16[2048,128]{1,0:T(8,128)(2,1)S(1)}, bf16[2048,128]{1,0:T(8,128)(2,1)S(1)}, u32[]{:S(2)}, u32[]{:S(2)}) collective-permute-start(bf16[2048,128]{1,0:T(8,128)(2,1)S(1)} %bitcast.22), channel_id=1, source_target_pairs={{0,1},{1,0},{2,3},{3,2},{4,5},{5,4},{6,7},{7,6},{8,9},{9,8},{10,11... | collective-permute-start | bytes 1572872 | tf_op jit(solution)/shard_map/ppermute | solution.py:287
  49.1 19.2 %collective-permute-done.3.g1_ref = bf16[2048,128]{1,0:T(8,128)(2,1)S(1)} collective-permute-done((bf16[2048,128]{1,0:T(8,128)(2,1)S(1)}, bf16[2048,128]{1,0:T(8,128)(2,1)S(1)}, u32[]{:S(2)}, u32[]{:S(2)}) %collective-permute-start.3) | collective-permute-done | bytes 524320 | tf_op jit(solution)/shard_map/ppermute | solution.py:286
  68.3 9.0 %collective-permute-done.4.u1_ref = bf16[2048,128]{1,0:T(8,128)(2,1)S(1)} collective-permute-done((bf16[2048,128]{1,0:T(8,128)(2,1)S(1)}, bf16[2048,128]{1,0:T(8,128)(2,1)S(1)}, u32[]{:S(2)}, u32[]{:S(2)}) %collective-permute-start.4) | collective-permute-done | bytes 524320 | tf_op jit(solution)/shard_map/ppermute | solution.py:287
  77.2 2.2 %shard_map.163 = bf16[16,512,128]{2,1,0:T(8,128)(2,1)} custom-call(s32[1]{0:T(128)} %bitcast.8.tp_ref, bf16[16,256,128]{2,1,0:T(8,128)(2,1)S(1)} %all-to-all-done.1.x_ref, bf16[2048,128]{1,0:T(8,128)(2,1)S(1)} %bitcast.21, bf16[2048,128]{1,0:T(8,128)(2,1)S(1)} %bitcast.23, bf16[2048,128]{1,0:T(8,128)(2,1)S(1)} %collective-permute-done.3.g1_ref, ...), custom_call_target="tpu_custom_call" | custom-call | flops 536870912 | bytes 1048576 | tf_op jit(solution)/shard_map/pallas_call | solution.py:34
  79.4 7.7 %all-to-all-start.2 = ((bf16[16,512,128]{2,1,0:T(8,128)(2,1)}), bf16[16,512,128]{2,1,0:T(8,128)(2,1)S(1)}, u32[]{:S(2)}, u32[]{:S(2)}) async-start(bf16[16,512,128]{2,1,0:T(8,128)(2,1)} %shard_map.163), calls=%async_computation.2 | async-start | bytes 4194304 | tf_op jit(solution)/shard_map/all_to_all | solution.py:264
  87.1 1.9 %shard_map.158 = (bf16[128,64]{1,0:T(8,128)(2,1)S(1)}, bf16[144,128]{1,0:T(8,128)(2,1)S(1)}) custom-call(bf16[128,2048]{1,0:T(8,128)(2,1)} %rows_ref.2, f32[1,2048]{1,0:T(1,128)} %bitcast.33, bf16[64,2048]{1,0:T(8,128)(2,1)} %bitcast.29, bf16[64,2048]{1,0:T(8,128)(2,1)} %bitcast.30, bf16[64,2048]{1,0:T(8,128)(2,1)} %bitcast.31, bf16[1,128]{1,0:T(2,128)(2,1)} %bias_ref.1), custom_call_target="tpu_custom_call" | custom-call | flops 268435456 | bytes 1048576 | tf_op jit(solution)/shard_map/pallas_call | solution.py:34
  89.0 5.6 %all_gather.12 = bf16[288,128]{1,0:T(8,128)(2,1)S(1)} all-gather(bf16[144,128]{1,0:T(8,128)(2,1)S(1)} %get-tuple-element.5), channel_id=1, replica_groups={{0,64},{16,80},{32,96},{48,112},{128,192},{144,208},{160,224},{176,240}..., dimensions={0}, use_global_device_ids=true | all-gather | bytes 110592 | tf_op jit(solution)/shard_map/all_gather | solution.py:288
  94.6 20.6 %all_gather.13.own_ref = bf16[1152,128]{1,0:T(8,128)(2,1)S(1)} all-gather(bf16[288,128]{1,0:T(8,128)(2,1)S(1)} %all_gather.12), channel_id=1, replica_groups={{0,128,256,384},{16,144,272,400},{32,160,288,416},{48,176,304,432},{64,..., dimensions={0}, use_global_device_ids=true | all-gather | bytes 368640 | tf_op jit(solution)/shard_map/all_gather | solution.py:289
  115.1 2.0 %collective-permute-start.1 = (bf16[1152,128]{1,0:T(8,128)(2,1)S(1)}, bf16[1152,128]{1,0:T(8,128)(2,1)S(1)}, u32[]{:S(2)}, u32[]{:S(2)}) collective-permute-start(bf16[1152,128]{1,0:T(8,128)(2,1)S(1)} %all_gather.13.own_ref), channel_id=1, source_target_pairs={{0,32},{16,48},{32,0},{48,16},{64,96},{80,112},{96,64},{112,80},{1... | collective-permute-start | bytes 884744 | tf_op jit(solution)/shard_map/ppermute | solution.py:290
  117.1 1.9 %collective-permute-start = (bf16[1152,128]{1,0:T(8,128)(2,1)S(1)}, bf16[1152,128]{1,0:T(8,128)(2,1)S(1)}, u32[]{:S(2)}, u32[]{:S(2)}) collective-permute-start(bf16[1152,128]{1,0:T(8,128)(2,1)S(1)} %all_gather.13.own_ref), channel_id=1, source_target_pairs={{0,16},{16,0},{32,48},{48,32},{64,80},{80,64},{96,112},{112,96},{1... | collective-permute-start | bytes 884744 | tf_op jit(solution)/shard_map/ppermute | solution.py:299
  119.0 4.7 %collective-permute-done.1.far_ref = bf16[1152,128]{1,0:T(8,128)(2,1)S(1)} collective-permute-done((bf16[1152,128]{1,0:T(8,128)(2,1)S(1)}, bf16[1152,128]{1,0:T(8,128)(2,1)S(1)}, u32[]{:S(2)}, u32[]{:S(2)}) %collective-permute-start.1) | collective-permute-done | bytes 294944 | tf_op jit(solution)/shard_map/ppermute | solution.py:290
  123.7 1.9 %collective-permute-start.2 = (bf16[1152,128]{1,0:T(8,128)(2,1)S(1)}, bf16[1152,128]{1,0:T(8,128)(2,1)}, u32[]{:S(2)}, u32[]{:S(2)}) collective-permute-start(bf16[1152,128]{1,0:T(8,128)(2,1)S(1)} %collective-permute-done.1.far_ref), channel_id=1, source_target_pairs={{0,16},{16,0},{32,48},{48,32},{64,80},{80,64},{96,112},{112,96},{1... | collective-permute-start | bytes 884744 | tf_op jit(solution)/shard_map/ppermute | solution.py:300
  125.7 1.4 shard_map.164
  127.1 7.0 %all-to-all-start.3 = ((bf16[32,16,128]{2,1,0:T(8,128)(2,1)}), bf16[32,16,128]{2,1,0:T(8,128)(2,1)S(1)}, u32[]{:S(2)}, u32[]{:S(2)}) async-start(bf16[32,16,128]{2,1,0:T(8,128)(2,1)} %bitcast.15), calls=%async_computation.3 | async-start | bytes 262144 | tf_op jit(solution)/shard_map/all_to_all | solution.py:264
  134.2 4.1 %shard_map.159 = bf16[64,128]{1,0:T(8,128)(2,1)S(1)} custom-call(s32[1]{0:T(128)} %bitcast.pos_ref, bf16[128,64]{1,0:T(8,128)(2,1)S(1)} %get-tuple-element.4.q_ref, bf16[1152,128]{1,0:T(8,128)(2,1)S(1)} %all_gather.13.own_ref, bf16[1152,128]{1,0:T(8,128)(2,1)S(1)} %collective-permute-done.other_ref, bf16[1152,128]{1,0:T(8,128)(2,1)S(1)} %collective-permute-done.1.far_ref, ...), custom_call_target="tpu_custom_call" | custom-call | flops 1073741824 | bytes 1048576 | tf_op jit(solution)/shard_map/pallas_call | solution.py:34
  138.3 11.9 %all_gather.14 = bf16[256,128]{1,0:T(8,128)(2,1)S(1)} all-gather(bf16[64,128]{1,0:T(8,128)(2,1)S(1)} %shard_map.159), channel_id=1, replica_groups={{0,1,2,3},{4,5,6,7},{8,9,10,11},{12,13,14,15},{16,17,18,19},{20,21,22,2..., dimensions={0}, use_global_device_ids=true | all-gather | bytes 81920 | tf_op jit(solution)/shard_map/all_gather | solution.py:304
  150.2 12.4 %all_gather.15.x_ref = bf16[1024,128]{1,0:T(8,128)(2,1)S(1)} all-gather(bf16[256,128]{1,0:T(8,128)(2,1)S(1)} %all_gather.14), channel_id=1, replica_groups={{0,4,8,12},{1,5,9,13},{2,6,10,14},{3,7,11,15},{16,20,24,28},{17,21,25,2..., dimensions={0}, use_global_device_ids=true | all-gather | bytes 327680 | tf_op jit(solution)/shard_map/all_gather | solution.py:307
  162.6 0.9 shard_map.160
  163.5 1.1 shard_map.165
  (19 shorter events, 0.1 us)
Async XLA Ops:
  0.6 42.6 %copy-start.1 = (bf16[1,2048,128]{2,1,0:T(8,128)(2,1)S(1)}, bf16[1,2048,128]{2,1,0:T(8,128)(2,1)}, u32[]{:S(2)}) copy-start(bf16[1,2048,128]{2,1,0:T(8,128)(2,1)} %param.27) | copy-start | bytes 1572868
  0.6 45.3 %copy-start.2 = (bf16[1,2048,128]{2,1,0:T(8,128)(2,1)S(1)}, bf16[1,2048,128]{2,1,0:T(8,128)(2,1)}, u32[]{:S(2)}) copy-start(bf16[1,2048,128]{2,1,0:T(8,128)(2,1)} %param.28) | copy-start | bytes 1572868
  35.8 41.5 %all-to-all-start.1 = ((bf16[16,256,128]{2,1,0:T(8,128)(2,1)}), bf16[16,256,128]{2,1,0:T(8,128)(2,1)S(1)}, u32[]{:S(2)}, u32[]{:S(2)}) async-start(bf16[16,256,128]{2,1,0:T(8,128)(2,1)} %shard_map.162), calls=%async_computation.1 | async-start | bytes 2097152 | tf_op jit(solution)/shard_map/all_to_all | solution.py:264
  43.2 25.1 %collective-permute-start.3 = (bf16[2048,128]{1,0:T(8,128)(2,1)S(1)}, bf16[2048,128]{1,0:T(8,128)(2,1)S(1)}, u32[]{:S(2)}, u32[]{:S(2)}) collective-permute-start(bf16[2048,128]{1,0:T(8,128)(2,1)S(1)} %bitcast.20), channel_id=1, source_target_pairs={{0,1},{1,0},{2,3},{3,2},{4,5},{5,4},{6,7},{7,6},{8,9},{9,8},{10,11... | collective-permute-start | bytes 1572872 | tf_op jit(solution)/shard_map/ppermute | solution.py:286
  46.0 31.2 %collective-permute-start.4 = (bf16[2048,128]{1,0:T(8,128)(2,1)S(1)}, bf16[2048,128]{1,0:T(8,128)(2,1)S(1)}, u32[]{:S(2)}, u32[]{:S(2)}) collective-permute-start(bf16[2048,128]{1,0:T(8,128)(2,1)S(1)} %bitcast.22), channel_id=1, source_target_pairs={{0,1},{1,0},{2,3},{3,2},{4,5},{5,4},{6,7},{7,6},{8,9},{9,8},{10,11... | collective-permute-start | bytes 1572872 | tf_op jit(solution)/shard_map/ppermute | solution.py:287
  79.4 46.3 %copy-start = (bf16[1,2048,128]{2,1,0:T(8,128)(2,1)S(1)}, bf16[1,2048,128]{2,1,0:T(8,128)(2,1)}, u32[]{:S(2)}) copy-start(bf16[1,2048,128]{2,1,0:T(8,128)(2,1)} %param.29) | copy-start | bytes 1572868
  79.4 46.2 %all-to-all-start.2 = ((bf16[16,512,128]{2,1,0:T(8,128)(2,1)}), bf16[16,512,128]{2,1,0:T(8,128)(2,1)S(1)}, u32[]{:S(2)}, u32[]{:S(2)}) async-start(bf16[16,512,128]{2,1,0:T(8,128)(2,1)} %shard_map.163), calls=%async_computation.2 | async-start | bytes 4194304 | tf_op jit(solution)/shard_map/all_to_all | solution.py:264
  115.1 8.6 %collective-permute-start.1 = (bf16[1152,128]{1,0:T(8,128)(2,1)S(1)}, bf16[1152,128]{1,0:T(8,128)(2,1)S(1)}, u32[]{:S(2)}, u32[]{:S(2)}) collective-permute-start(bf16[1152,128]{1,0:T(8,128)(2,1)S(1)} %all_gather.13.own_ref), channel_id=1, source_target_pairs={{0,32},{16,48},{32,0},{48,16},{64,96},{80,112},{96,64},{112,80},{1... | collective-permute-start | bytes 884744 | tf_op jit(solution)/shard_map/ppermute | solution.py:290
  117.1 17.0 %collective-permute-start = (bf16[1152,128]{1,0:T(8,128)(2,1)S(1)}, bf16[1152,128]{1,0:T(8,128)(2,1)S(1)}, u32[]{:S(2)}, u32[]{:S(2)}) collective-permute-start(bf16[1152,128]{1,0:T(8,128)(2,1)S(1)} %all_gather.13.own_ref), channel_id=1, source_target_pairs={{0,16},{16,0},{32,48},{48,32},{64,80},{80,64},{96,112},{112,96},{1... | collective-permute-start | bytes 884744 | tf_op jit(solution)/shard_map/ppermute | solution.py:299
  123.7 10.4 %collective-permute-start.2 = (bf16[1152,128]{1,0:T(8,128)(2,1)S(1)}, bf16[1152,128]{1,0:T(8,128)(2,1)}, u32[]{:S(2)}, u32[]{:S(2)}) collective-permute-start(bf16[1152,128]{1,0:T(8,128)(2,1)S(1)} %collective-permute-done.1.far_ref), channel_id=1, source_target_pairs={{0,16},{16,0},{32,48},{48,32},{64,80},{80,64},{96,112},{112,96},{1... | collective-permute-start | bytes 884744 | tf_op jit(solution)/shard_map/ppermute | solution.py:300
  127.1 36.5 %all-to-all-start.3 = ((bf16[32,16,128]{2,1,0:T(8,128)(2,1)}), bf16[32,16,128]{2,1,0:T(8,128)(2,1)S(1)}, u32[]{:S(2)}, u32[]{:S(2)}) async-start(bf16[32,16,128]{2,1,0:T(8,128)(2,1)} %bitcast.15), calls=%async_computation.3 | async-start | bytes 262144 | tf_op jit(solution)/shard_map/all_to_all | solution.py:264
  134.1 28.5 %copy-start.3 = (bf16[1024,128]{1,0:T(8,128)(2,1)S(1)}, bf16[1024,128]{1,0:T(8,128)(2,1)}, u32[]{:S(2)}) copy-start(bf16[1024,128]{1,0:T(8,128)(2,1)} %w_ref.1) | copy-start | bytes 786436
  134.1 29.4 %copy-start.4 = (s32[128,2]{0,1:T(2,128)S(1)}, s32[128,2]{0,1:T(2,128)}, u32[]{:S(2)}) copy-start(s32[128,2]{0,1:T(2,128)} %param.24) | copy-start | bytes 3076
  134.1 29.4 %copy-start.5 = (f32[128,4]{0,1:T(4,128)S(1)}, f32[128,4]{0,1:T(4,128)}, u32[]{:S(2)}) copy-start(f32[128,4]{0,1:T(4,128)} %param.25) | copy-start | bytes 6148
  134.1 29.4 %copy-start.6 = (f32[128,2]{0,1:T(2,128)S(1)}, f32[128,2]{0,1:T(2,128)}, u32[]{:S(2)}) copy-start(f32[128,2]{0,1:T(2,128)} %param.26) | copy-start | bytes 3076

commit v6 on v5

--- a/solution.py
+++ b/solution.py
@@ -16,6 +16,7 @@
 ROWS = SLOTS // 2
 MSG = 144
 WIDTH = 4
+OFFSETS = (0, 1, 3, 2)
 
 epsilon = 1e-06
 f32 = jnp.float32
@@ -204,9 +205,19 @@
     out_ref[...] = jnp.transpose(total).astype(bf16)
 
 
-def mix_body(x_ref, w_ref, out_ref):
+def pack_body(*refs):
+    for k, ref in enumerate(refs[:-1]):
+        refs[-1][k * HEAD : (k + 1) * HEAD, :] = ref[...]
+
+
+def mix_body(tp_ref, x_ref, w_ref, out_ref):
+    column = tp_ref[0] % 4
+    weights = []
+    for k in range(x_ref.shape[0] // HEAD):
+        head = k - k % 4 + (column + OFFSETS[k % 4]) % 4
+        weights.append(w_ref[pl.ds(pl.multiple_of(head * HEAD, HEAD), HEAD), :])
     x = jnp.transpose(x_ref[...].astype(f32)).astype(bf16)
-    out_ref[...] = nn(x, w_ref[...]).astype(bf16)
+    out_ref[...] = nn(x, jnp.concatenate(weights, axis=0)).astype(bf16)
 
 
 def combine_body(ids_ref, group_ref, pair_ref, back_ref, out_ref):
@@ -256,7 +267,6 @@
     strided = [[(m + 4 * k) * 2 + c for k in range(run)] for m in range(4) for c in range(2)]
     pairs = [[(z + 2 * b) * 2 + c for b in range(2)] for z in range(chips) if z % 4 < 2 for c in range(2)]
     side = tp // 4
-    along_x = [[y * 4 + x for x in range(4)] for y in range(side)]
     along_y = [[y * 4 + x for y in range(side)] for x in range(4)]
     struct = jax.ShapeDtypeStruct
 
@@ -301,11 +311,16 @@
     attended = call(attend_body, 1, 5, struct((HEAD, BLOCK), bf16), 1 << 30)(
         here.reshape(1), query, own, own_other, far, far_other
     )
-    attended = lax.all_gather(attended, "tp", axis=0, tiled=True, axis_index_groups=along_x)
+    heads = [attended]
+    for d in OFFSETS[1:]:
+        moves = [(k - k % 4 + (k + d) % 4, k) for k in range(tp)]
+        heads.append(lax.ppermute(attended, "tp", moves))
+    stacked = struct((len(heads) * HEAD, BLOCK), bf16)
+    attended = call(pack_body, 0, len(heads), stacked, 1 << 20)(*heads)
     result = call(down_body, 0, 2, slots, 1 << 28)(hidden, down_weight[0])
     back = exchange(result.reshape(ep, CAP, BLOCK), "ep").reshape(SLOTS, BLOCK)
     attended = lax.all_gather(attended, "tp", axis=0, tiled=True, axis_index_groups=along_y)
-    mixed = call(mix_body, 0, 2, square, 1 << 26)(attended, out_weight)
+    mixed = call(mix_body, 1, 2, square, 1 << 26)(column, attended, out_weight)
     expert_out = call(combine_body, 0, 4, square, 1 << 27)(ids, group_logits.T, pair_logits.T, back)
     return (mixed, expert_out)
 

time: 165 us -> 167 us (1.012)
  blocking collectives: 82.9 us -> 71.3 us
  starting transfers between devices: 33.8 us -> 42.1 us
  waiting for transfers between devices: 32.9 us -> 37.8 us
    all_gather x2 -> x1, blocking collectives: 24.3 us -> 12.7 us  [shards(): lax.all_gather(attended, 'tp', axis=0, tiled=True, axis_index_groups=alon...]
    ppermute x0 -> x3, starting transfers between devices: none -> 8.46 us  [shards(): heads.append(lax.ppermute(attended, 'tp', moves))]
    ppermute x0 -> x3, waiting for transfers between devices: none -> 4.9 us  [shards(): heads.append(lax.ppermute(attended, 'tp', moves))]
    pallas_call x8 -> x9, Pallas kernels: 14.2 us -> 14.2 us  [run(): return kernel(*args)]
  transfers between devices with their start and end apart: 8 -> 11, of which waited for: 3 -> 4; matrix products, arithmetic and copies ran while one was open for 0% -> 0% of each run, Pallas kernels for 5% -> 5%
where the time goes in v6:
time: 167 us; the launch traced here: 166 us
  blocking collectives  71.3 us (43%)
  starting transfers between devices  42.1 us (25%)
  waiting for transfers between devices  37.8 us (23%)
  Pallas kernels  14.2 us (9%)
    all_to_all x1, blocking collectives, exchange(): return lax.all_to_all(x, axis, split_axis=0, concat_axis=0, tiled=True)  32.5 us
    all_to_all x3, starting transfers between devices, exchange(): return lax.all_to_all(x, axis, split_axis=0, concat_axis=0, tiled=True)  22 us
    all_gather x1, blocking collectives, shards(): lax.all_gather(keys, 'ep', axis=0, tiled=True, axis_index_groups=strided)  20.6 us
    ppermute x1, waiting for transfers between devices, shards(): other_gate = lax.ppermute(gate_weight[0], 'tp', swaps)  19.2 us
    pallas_call x9, Pallas kernels, run(): return kernel(*args)  14.2 us
    all_gather x1, blocking collectives, shards(): lax.all_gather(attended, 'tp', axis=0, tiled=True, axis_index_groups=alon...  12.7 us
    ppermute x1, waiting for transfers between devices, shards(): other_up = lax.ppermute(up_weight[0], 'tp', swaps)  8.97 us
    ppermute x3, starting transfers between devices, shards(): heads.append(lax.ppermute(attended, 'tp', moves))  8.46 us
  transfers between devices with their start and end apart: 11, of which 4 were waited for; matrix products, arithmetic and copies ran while one was open for 0% of the time, Pallas kernels for 5%

profile of v6, /device:TPU:6, one launch (start us, length us, event | category | flops | bytes accessed | tf_op | source)
XLA Modules:
  0.0 166.3 jit_solution(3834785306040036013)
XLA Ops:
  0.7 1.5 shard_map.162
  2.2 32.5 %all_to_all.20 = bf16[32,16,128]{2,1,0:T(8,128)(2,1)S(1)} all-to-all(bf16[32,16,128]{2,1,0:T(8,128)(2,1)S(1)} %bitcast.18), channel_id=1, replica_groups=mesh['ep'=32,'tp'=16] {'ep'}, dimensions={0} | all-to-all | bytes 262144 | tf_op jit(solution)/shard_map/all_to_all | solution.py:274
  35.8 7.4 %all-to-all-start.1 = ((bf16[16,256,128]{2,1,0:T(8,128)(2,1)}), bf16[16,256,128]{2,1,0:T(8,128)(2,1)S(1)}, u32[]{:S(2)}, u32[]{:S(2)}) async-start(bf16[16,256,128]{2,1,0:T(8,128)(2,1)} %shard_map.163), calls=%async_computation.1 | async-start | bytes 2097152 | tf_op jit(solution)/shard_map/all_to_all | solution.py:274
  43.2 2.8 %collective-permute-start.6 = (bf16[2048,128]{1,0:T(8,128)(2,1)S(1)}, bf16[2048,128]{1,0:T(8,128)(2,1)S(1)}, u32[]{:S(2)}, u32[]{:S(2)}) collective-permute-start(bf16[2048,128]{1,0:T(8,128)(2,1)S(1)} %bitcast.20), channel_id=1, source_target_pairs={{0,1},{1,0},{2,3},{3,2},{4,5},{5,4},{6,7},{7,6},{8,9},{9,8},{10,11... | collective-permute-start | bytes 1572872 | tf_op jit(solution)/shard_map/ppermute | solution.py:296
  46.0 3.1 %collective-permute-start.7 = (bf16[2048,128]{1,0:T(8,128)(2,1)S(1)}, bf16[2048,128]{1,0:T(8,128)(2,1)S(1)}, u32[]{:S(2)}, u32[]{:S(2)}) collective-permute-start(bf16[2048,128]{1,0:T(8,128)(2,1)S(1)} %bitcast.22), channel_id=1, source_target_pairs={{0,1},{1,0},{2,3},{3,2},{4,5},{5,4},{6,7},{7,6},{8,9},{9,8},{10,11... | collective-permute-start | bytes 1572872 | tf_op jit(solution)/shard_map/ppermute | solution.py:297
  49.1 19.2 %collective-permute-done.6.g1_ref = bf16[2048,128]{1,0:T(8,128)(2,1)S(1)} collective-permute-done((bf16[2048,128]{1,0:T(8,128)(2,1)S(1)}, bf16[2048,128]{1,0:T(8,128)(2,1)S(1)}, u32[]{:S(2)}, u32[]{:S(2)}) %collective-permute-start.6) | collective-permute-done | bytes 524320 | tf_op jit(solution)/shard_map/ppermute | solution.py:296
  68.3 9.0 %collective-permute-done.7.u1_ref = bf16[2048,128]{1,0:T(8,128)(2,1)S(1)} collective-permute-done((bf16[2048,128]{1,0:T(8,128)(2,1)S(1)}, bf16[2048,128]{1,0:T(8,128)(2,1)S(1)}, u32[]{:S(2)}, u32[]{:S(2)}) %collective-permute-start.7) | collective-permute-done | bytes 524320 | tf_op jit(solution)/shard_map/ppermute | solution.py:297
  77.2 2.2 %shard_map.164 = bf16[16,512,128]{2,1,0:T(8,128)(2,1)} custom-call(s32[1]{0:T(128)} %bitcast.tp_ref, bf16[16,256,128]{2,1,0:T(8,128)(2,1)S(1)} %all-to-all-done.1.x_ref, bf16[2048,128]{1,0:T(8,128)(2,1)S(1)} %bitcast.21, bf16[2048,128]{1,0:T(8,128)(2,1)S(1)} %bitcast.23, bf16[2048,128]{1,0:T(8,128)(2,1)S(1)} %collective-permute-done.6.g1_ref, ...), custom_call_target="tpu_custom_call" | custom-call | flops 536870912 | bytes 1048576 | tf_op jit(solution)/shard_map/pallas_call | solution.py:35
  79.4 7.7 %all-to-all-start.2 = ((bf16[16,512,128]{2,1,0:T(8,128)(2,1)}), bf16[16,512,128]{2,1,0:T(8,128)(2,1)S(1)}, u32[]{:S(2)}, u32[]{:S(2)}) async-start(bf16[16,512,128]{2,1,0:T(8,128)(2,1)} %shard_map.164), calls=%async_computation.2 | async-start | bytes 4194304 | tf_op jit(solution)/shard_map/all_to_all | solution.py:274
  87.1 1.9 %shard_map.158 = (bf16[128,64]{1,0:T(8,128)(2,1)S(1)}, bf16[144,128]{1,0:T(8,128)(2,1)S(1)}) custom-call(bf16[128,2048]{1,0:T(8,128)(2,1)} %rows_ref.2, f32[1,2048]{1,0:T(1,128)} %bitcast.33, bf16[64,2048]{1,0:T(8,128)(2,1)} %bitcast.29, bf16[64,2048]{1,0:T(8,128)(2,1)} %bitcast.30, bf16[64,2048]{1,0:T(8,128)(2,1)} %bitcast.31, bf16[1,128]{1,0:T(2,128)(2,1)} %bias_ref.1), custom_call_target="tpu_custom_call" | custom-call | flops 268435456 | bytes 1048576 | tf_op jit(solution)/shard_map/pallas_call | solution.py:35
  89.0 5.6 %all_gather.9 = bf16[288,128]{1,0:T(8,128)(2,1)S(1)} all-gather(bf16[144,128]{1,0:T(8,128)(2,1)S(1)} %get-tuple-element.5), channel_id=1, replica_groups={{0,64},{16,80},{32,96},{48,112},{128,192},{144,208},{160,224},{176,240}..., dimensions={0}, use_global_device_ids=true | all-gather | bytes 110592 | tf_op jit(solution)/shard_map/all_gather | solution.py:298
  94.6 20.6 %all_gather.10.own_ref = bf16[1152,128]{1,0:T(8,128)(2,1)S(1)} all-gather(bf16[288,128]{1,0:T(8,128)(2,1)S(1)} %all_gather.9), channel_id=1, replica_groups={{0,128,256,384},{16,144,272,400},{32,160,288,416},{48,176,304,432},{64,..., dimensions={0}, use_global_device_ids=true | all-gather | bytes 368640 | tf_op jit(solution)/shard_map/all_gather | solution.py:299
  115.1 2.0 %collective-permute-start.1 = (bf16[1152,128]{1,0:T(8,128)(2,1)S(1)}, bf16[1152,128]{1,0:T(8,128)(2,1)S(1)}, u32[]{:S(2)}, u32[]{:S(2)}) collective-permute-start(bf16[1152,128]{1,0:T(8,128)(2,1)S(1)} %all_gather.10.own_ref), channel_id=1, source_target_pairs={{0,32},{16,48},{32,0},{48,16},{64,96},{80,112},{96,64},{112,80},{1... | collective-permute-start | bytes 884744 | tf_op jit(solution)/shard_map/ppermute | solution.py:300
  117.1 1.9 %collective-permute-start = (bf16[1152,128]{1,0:T(8,128)(2,1)S(1)}, bf16[1152,128]{1,0:T(8,128)(2,1)S(1)}, u32[]{:S(2)}, u32[]{:S(2)}) collective-permute-start(bf16[1152,128]{1,0:T(8,128)(2,1)S(1)} %all_gather.10.own_ref), channel_id=1, source_target_pairs={{0,16},{16,0},{32,48},{48,32},{64,80},{80,64},{96,112},{112,96},{1... | collective-permute-start | bytes 884744 | tf_op jit(solution)/shard_map/ppermute | solution.py:309
  119.1 4.7 %collective-permute-done.1.far_ref = bf16[1152,128]{1,0:T(8,128)(2,1)S(1)} collective-permute-done((bf16[1152,128]{1,0:T(8,128)(2,1)S(1)}, bf16[1152,128]{1,0:T(8,128)(2,1)S(1)}, u32[]{:S(2)}, u32[]{:S(2)}) %collective-permute-start.1) | collective-permute-done | bytes 294944 | tf_op jit(solution)/shard_map/ppermute | solution.py:300
  123.7 1.9 %collective-permute-start.2 = (bf16[1152,128]{1,0:T(8,128)(2,1)S(1)}, bf16[1152,128]{1,0:T(8,128)(2,1)}, u32[]{:S(2)}, u32[]{:S(2)}) collective-permute-start(bf16[1152,128]{1,0:T(8,128)(2,1)S(1)} %collective-permute-done.1.far_ref), channel_id=1, source_target_pairs={{0,16},{16,0},{32,48},{48,32},{64,80},{80,64},{96,112},{112,96},{1... | collective-permute-start | bytes 884744 | tf_op jit(solution)/shard_map/ppermute | solution.py:310
  125.7 1.3 shard_map.165
  127.0 6.9 %all-to-all-start.3 = ((bf16[32,16,128]{2,1,0:T(8,128)(2,1)}), bf16[32,16,128]{2,1,0:T(8,128)(2,1)S(1)}, u32[]{:S(2)}, u32[]{:S(2)}) async-start(bf16[32,16,128]{2,1,0:T(8,128)(2,1)} %bitcast.15), calls=%async_computation.3 | async-start | bytes 262144 | tf_op jit(solution)/shard_map/all_to_all | solution.py:274
  134.0 4.1 %shard_map.159.refs_0_ = bf16[64,128]{1,0:T(8,128)(2,1)S(1)} custom-call(s32[1]{0:T(128)} %bitcast.1.pos_ref, bf16[128,64]{1,0:T(8,128)(2,1)S(1)} %get-tuple-element.4.q_ref, bf16[1152,128]{1,0:T(8,128)(2,1)S(1)} %all_gather.10.own_ref, bf16[1152,128]{1,0:T(8,128)(2,1)S(1)} %collective-permute-done.other_ref, ...), custom_call_target="tpu_custom_call" | custom-call | flops 1073741824 | bytes 1048576 | tf_op jit(solution)/shard_map/pallas_call | solution.py:35
  138.1 2.4 %collective-permute-start.5 = (bf16[64,128]{1,0:T(8,128)(2,1)S(1)}, bf16[64,128]{1,0:T(8,128)(2,1)S(1)}, u32[]{:S(2)}, u32[]{:S(2)}) collective-permute-start(bf16[64,128]{1,0:T(8,128)(2,1)S(1)} %shard_map.159.refs_0_), channel_id=1, source_target_pairs={{2,0},{3,1},{0,2},{1,3},{6,4},{7,5},{4,6},{5,7},{10,8},{11,9},{8,1... | collective-permute-start | bytes 49160 | tf_op jit(solution)/shard_map/ppermute | solution.py:317
  140.5 4.2 %collective-permute-start.4 = (bf16[64,128]{1,0:T(8,128)(2,1)S(1)}, bf16[64,128]{1,0:T(8,128)(2,1)S(1)}, u32[]{:S(2)}, u32[]{:S(2)}) collective-permute-start(bf16[64,128]{1,0:T(8,128)(2,1)S(1)} %shard_map.159.refs_0_), channel_id=1, source_target_pairs={{3,0},{0,1},{1,2},{2,3},{7,4},{4,5},{5,6},{6,7},{11,8},{8,9},{9,10... | collective-permute-start | bytes 49160 | tf_op jit(solution)/shard_map/ppermute | solution.py:317
  144.7 1.9 %collective-permute-start.3 = (bf16[64,128]{1,0:T(8,128)(2,1)S(1)}, bf16[64,128]{1,0:T(8,128)(2,1)S(1)}, u32[]{:S(2)}, u32[]{:S(2)}) collective-permute-start(bf16[64,128]{1,0:T(8,128)(2,1)S(1)} %shard_map.159.refs_0_), channel_id=1, source_target_pairs={{1,0},{2,1},{3,2},{0,3},{5,4},{6,5},{7,6},{4,7},{9,8},{10,9},{11,1... | collective-permute-start | bytes 49160 | tf_op jit(solution)/shard_map/ppermute | solution.py:317
  146.6 4.9 %collective-permute-done.3.refs_1_ = bf16[64,128]{1,0:T(8,128)(2,1)S(1)} collective-permute-done((bf16[64,128]{1,0:T(8,128)(2,1)S(1)}, bf16[64,128]{1,0:T(8,128)(2,1)S(1)}, u32[]{:S(2)}, u32[]{:S(2)}) %collective-permute-start.3) | collective-permute-done | bytes 16416 | tf_op jit(solution)/shard_map/ppermute | solution.py:317
  151.5 12.7 %all_gather.11.x_ref = bf16[1024,128]{1,0:T(8,128)(2,1)S(1)} all-gather(bf16[256,128]{1,0:T(8,128)(2,1)S(1)} %shard_map.160), channel_id=1, replica_groups={{0,4,8,12},{1,5,9,13},{2,6,10,14},{3,7,11,15},{16,20,24,28},{17,21,25,2..., dimensions={0}, use_global_device_ids=true | all-gather | bytes 327680 | tf_op jit(solution)/shard_map/all_gather | solution.py:322
  (25 shorter events, 3.2 us)
Async XLA Ops:
  0.6 42.6 %copy-start.1 = (bf16[1,2048,128]{2,1,0:T(8,128)(2,1)S(1)}, bf16[1,2048,128]{2,1,0:T(8,128)(2,1)}, u32[]{:S(2)}) copy-start(bf16[1,2048,128]{2,1,0:T(8,128)(2,1)} %param.27) | copy-start | bytes 1572868
  0.6 45.3 %copy-start.2 = (bf16[1,2048,128]{2,1,0:T(8,128)(2,1)S(1)}, bf16[1,2048,128]{2,1,0:T(8,128)(2,1)}, u32[]{:S(2)}) copy-start(bf16[1,2048,128]{2,1,0:T(8,128)(2,1)} %param.28) | copy-start | bytes 1572868
  35.8 41.5 %all-to-all-start.1 = ((bf16[16,256,128]{2,1,0:T(8,128)(2,1)}), bf16[16,256,128]{2,1,0:T(8,128)(2,1)S(1)}, u32[]{:S(2)}, u32[]{:S(2)}) async-start(bf16[16,256,128]{2,1,0:T(8,128)(2,1)} %shard_map.163), calls=%async_computation.1 | async-start | bytes 2097152 | tf_op jit(solution)/shard_map/all_to_all | solution.py:274
  43.2 25.1 %collective-permute-start.6 = (bf16[2048,128]{1,0:T(8,128)(2,1)S(1)}, bf16[2048,128]{1,0:T(8,128)(2,1)S(1)}, u32[]{:S(2)}, u32[]{:S(2)}) collective-permute-start(bf16[2048,128]{1,0:T(8,128)(2,1)S(1)} %bitcast.20), channel_id=1, source_target_pairs={{0,1},{1,0},{2,3},{3,2},{4,5},{5,4},{6,7},{7,6},{8,9},{9,8},{10,11... | collective-permute-start | bytes 1572872 | tf_op jit(solution)/shard_map/ppermute | solution.py:296
  46.0 31.2 %collective-permute-start.7 = (bf16[2048,128]{1,0:T(8,128)(2,1)S(1)}, bf16[2048,128]{1,0:T(8,128)(2,1)S(1)}, u32[]{:S(2)}, u32[]{:S(2)}) collective-permute-start(bf16[2048,128]{1,0:T(8,128)(2,1)S(1)} %bitcast.22), channel_id=1, source_target_pairs={{0,1},{1,0},{2,3},{3,2},{4,5},{5,4},{6,7},{7,6},{8,9},{9,8},{10,11... | collective-permute-start | bytes 1572872 | tf_op jit(solution)/shard_map/ppermute | solution.py:297
  79.4 46.3 %copy-start = (bf16[1,2048,128]{2,1,0:T(8,128)(2,1)S(1)}, bf16[1,2048,128]{2,1,0:T(8,128)(2,1)}, u32[]{:S(2)}) copy-start(bf16[1,2048,128]{2,1,0:T(8,128)(2,1)} %param.29) | copy-start | bytes 1572868
  79.4 46.2 %all-to-all-start.2 = ((bf16[16,512,128]{2,1,0:T(8,128)(2,1)}), bf16[16,512,128]{2,1,0:T(8,128)(2,1)S(1)}, u32[]{:S(2)}, u32[]{:S(2)}) async-start(bf16[16,512,128]{2,1,0:T(8,128)(2,1)} %shard_map.164), calls=%async_computation.2 | async-start | bytes 4194304 | tf_op jit(solution)/shard_map/all_to_all | solution.py:274
  115.1 8.6 %collective-permute-start.1 = (bf16[1152,128]{1,0:T(8,128)(2,1)S(1)}, bf16[1152,128]{1,0:T(8,128)(2,1)S(1)}, u32[]{:S(2)}, u32[]{:S(2)}) collective-permute-start(bf16[1152,128]{1,0:T(8,128)(2,1)S(1)} %all_gather.10.own_ref), channel_id=1, source_target_pairs={{0,32},{16,48},{32,0},{48,16},{64,96},{80,112},{96,64},{112,80},{1... | collective-permute-start | bytes 884744 | tf_op jit(solution)/shard_map/ppermute | solution.py:300
  117.1 16.8 %collective-permute-start = (bf16[1152,128]{1,0:T(8,128)(2,1)S(1)}, bf16[1152,128]{1,0:T(8,128)(2,1)S(1)}, u32[]{:S(2)}, u32[]{:S(2)}) collective-permute-start(bf16[1152,128]{1,0:T(8,128)(2,1)S(1)} %all_gather.10.own_ref), channel_id=1, source_target_pairs={{0,16},{16,0},{32,48},{48,32},{64,80},{80,64},{96,112},{112,96},{1... | collective-permute-start | bytes 884744 | tf_op jit(solution)/shard_map/ppermute | solution.py:309
  123.7 10.2 %collective-permute-start.2 = (bf16[1152,128]{1,0:T(8,128)(2,1)S(1)}, bf16[1152,128]{1,0:T(8,128)(2,1)}, u32[]{:S(2)}, u32[]{:S(2)}) collective-permute-start(bf16[1152,128]{1,0:T(8,128)(2,1)S(1)} %collective-permute-done.1.far_ref), channel_id=1, source_target_pairs={{0,16},{16,0},{32,48},{48,32},{64,80},{80,64},{96,112},{112,96},{1... | collective-permute-start | bytes 884744 | tf_op jit(solution)/shard_map/ppermute | solution.py:310
  127.0 38.1 %all-to-all-start.3 = ((bf16[32,16,128]{2,1,0:T(8,128)(2,1)}), bf16[32,16,128]{2,1,0:T(8,128)(2,1)S(1)}, u32[]{:S(2)}, u32[]{:S(2)}) async-start(bf16[32,16,128]{2,1,0:T(8,128)(2,1)} %bitcast.15), calls=%async_computation.3 | async-start | bytes 262144 | tf_op jit(solution)/shard_map/all_to_all | solution.py:274
  133.9 30.3 %copy-start.3 = (bf16[1024,128]{1,0:T(8,128)(2,1)S(1)}, bf16[1024,128]{1,0:T(8,128)(2,1)}, u32[]{:S(2)}) copy-start(bf16[1024,128]{1,0:T(8,128)(2,1)} %w_ref.1) | copy-start | bytes 786436
  133.9 31.2 %copy-start.4 = (s32[128,2]{0,1:T(2,128)S(1)}, s32[128,2]{0,1:T(2,128)}, u32[]{:S(2)}) copy-start(s32[128,2]{0,1:T(2,128)} %param.24) | copy-start | bytes 3076
  134.0 31.1 %copy-start.5 = (f32[128,4]{0,1:T(4,128)S(1)}, f32[128,4]{0,1:T(4,128)}, u32[]{:S(2)}) copy-start(f32[128,4]{0,1:T(4,128)} %param.25) | copy-start | bytes 6148
  134.0 31.1 %copy-start.6 = (f32[128,2]{0,1:T(2,128)S(1)}, f32[128,2]{0,1:T(2,128)}, u32[]{:S(2)}) copy-start(f32[128,2]{0,1:T(2,128)} %param.26) | copy-start | bytes 3076
  138.1 8.5 %collective-permute-start.5 = (bf16[64,128]{1,0:T(8,128)(2,1)S(1)}, bf16[64,128]{1,0:T(8,128)(2,1)S(1)}, u32[]{:S(2)}, u32[]{:S(2)}) collective-permute-start(bf16[64,128]{1,0:T(8,128)(2,1)S(1)} %shard_map.159.refs_0_), channel_id=1, source_target_pairs={{2,0},{3,1},{0,2},{1,3},{6,4},{7,5},{4,6},{5,7},{10,8},{11,9},{8,1... | collective-permute-start | bytes 49160 | tf_op jit(solution)/shard_map/ppermute | solution.py:317
  140.5 6.1 %collective-permute-start.4 = (bf16[64,128]{1,0:T(8,128)(2,1)S(1)}, bf16[64,128]{1,0:T(8,128)(2,1)S(1)}, u32[]{:S(2)}, u32[]{:S(2)}) collective-permute-start(bf16[64,128]{1,0:T(8,128)(2,1)S(1)} %shard_map.159.refs_0_), channel_id=1, source_target_pairs={{3,0},{0,1},{1,2},{2,3},{7,4},{4,5},{5,6},{6,7},{11,8},{8,9},{9,10... | collective-permute-start | bytes 49160 | tf_op jit(solution)/shard_map/ppermute | solution.py:317
  144.7 6.8 %collective-permute-start.3 = (bf16[64,128]{1,0:T(8,128)(2,1)S(1)}, bf16[64,128]{1,0:T(8,128)(2,1)S(1)}, u32[]{:S(2)}, u32[]{:S(2)}) collective-permute-start(bf16[64,128]{1,0:T(8,128)(2,1)S(1)} %shard_map.159.refs_0_), channel_id=1, source_target_pairs={{1,0},{2,1},{3,2},{0,3},{5,4},{6,5},{7,6},{4,7},{9,8},{10,9},{11,1... | collective-permute-start | bytes 49160 | tf_op jit(solution)/shard_map/ppermute | solution.py:317

commit v7 on v6

--- a/solution.py
+++ b/solution.py
@@ -144,19 +144,17 @@
 
 def down_body(x_ref, w_ref, out_ref):
     parts = x_ref.shape[0]
+    rows = []
     for half in range(2):
         for m in range(2):
             at = m * ROWS
-            x = jnp.concatenate(
-                [
-                    x_ref[k, at + e * BLOCK : at + (e + 1) * BLOCK, :]
-                    for k in range(half, parts, 2)
-                    for e in range(2)
-                ],
-                axis=1,
-            )
-            at = half * ROWS + m * BLOCK
-            out_ref[at : at + BLOCK, :] = nn(x, w_ref[...]).astype(bf16)
+            pieces = [
+                x_ref[k, at + e * BLOCK : at + (e + 1) * BLOCK, :]
+                for k in range(half, parts, 2)
+                for e in range(2)
+            ]
+            rows.append(jnp.concatenate(pieces, axis=1))
+    out_ref[...] = nn(jnp.concatenate(rows, axis=0), w_ref[...]).astype(bf16)
 
 
 def attend_body(pos_ref, q_ref, own_ref, other_ref, far_ref, far_other_ref, out_ref):
@@ -220,7 +218,7 @@
     out_ref[...] = nn(x, jnp.concatenate(weights, axis=0)).astype(bf16)
 
 
-def combine_body(ids_ref, group_ref, pair_ref, back_ref, out_ref):
+def plan_body(ids_ref, group_ref, pair_ref, pick_ref, table_ref):
     ids = ids_ref[...]
     first, second = ids[0:1, :], ids[1:2, :]
     place0, place1 = places(first, second)
@@ -237,10 +235,16 @@
     table = jnp.concatenate([table, jnp.zeros((BLOCK - 4, BLOCK), f32)], axis=0)
     table = jnp.transpose(table)
     slot = iota((BLOCK, SLOTS), 1)
-    back = back_ref[...]
-    pick0 = nn(ones_where(slot == table[:, 0:1].astype(i32)).astype(bf16), back)
-    pick1 = nn(ones_where(slot == table[:, 1:2].astype(i32)).astype(bf16), back)
-    out_ref[...] = (table[:, 2:3] * pick0 + table[:, 3:4] * pick1).astype(bf16)
+    for k in range(2):
+        hit = ones_where(slot == table[:, k : k + 1].astype(i32))
+        pick_ref[k * BLOCK : (k + 1) * BLOCK, :] = hit.astype(bf16)
+    table_ref[...] = table
+
+
+def combine_body(pick_ref, table_ref, back_ref, out_ref):
+    both = nn(pick_ref[...], back_ref[...])
+    out = table_ref[:, 2:3] * both[:BLOCK] + table_ref[:, 3:4] * both[BLOCK:]
+    out_ref[...] = out.astype(bf16)
 
 
 def shards(
@@ -319,9 +323,11 @@
     attended = call(pack_body, 0, len(heads), stacked, 1 << 20)(*heads)
     result = call(down_body, 0, 2, slots, 1 << 28)(hidden, down_weight[0])
     back = exchange(result.reshape(ep, CAP, BLOCK), "ep").reshape(SLOTS, BLOCK)
+    tables = (struct((2 * BLOCK, SLOTS), bf16), struct((BLOCK, BLOCK), f32))
+    picks, table = call(plan_body, 0, 3, tables, 1 << 26)(ids, group_logits.T, pair_logits.T)
     attended = lax.all_gather(attended, "tp", axis=0, tiled=True, axis_index_groups=along_y)
     mixed = call(mix_body, 1, 2, square, 1 << 26)(column, attended, out_weight)
-    expert_out = call(combine_body, 0, 4, square, 1 << 27)(ids, group_logits.T, pair_logits.T, back)
+    expert_out = call(combine_body, 0, 3, square, 1 << 27)(picks, table, back)
     return (mixed, expert_out)
 
 

time: 167 us -> 167 us (level)
    pallas_call x9 -> x10, Pallas kernels: 14.2 us -> 14.3 us  [run(): return kernel(*args)]
where the time goes in v7:
time: 167 us
  blocking collectives  71.2 us (43%)
  starting transfers between devices  42.9 us (26%)
  waiting for transfers between devices  37.5 us (22%)
  Pallas kernels  14.3 us (9%)
    all_to_all x1, blocking collectives, exchange(): return lax.all_to_all(x, axis, split_axis=0, concat_axis=0, tiled=True)  32.5 us
    all_to_all x3, starting transfers between devices, exchange(): return lax.all_to_all(x, axis, split_axis=0, concat_axis=0, tiled=True)  22.1 us
    all_gather x1, blocking collectives, shards(): lax.all_gather(keys, 'ep', axis=0, tiled=True, axis_index_groups=strided)  20.6 us
    ppermute x1, waiting for transfers between devices, shards(): other_gate = lax.ppermute(gate_weight[0], 'tp', swaps)  19.2 us
    pallas_call x10, Pallas kernels, run(): return kernel(*args)  14.3 us
    all_gather x1, blocking collectives, shards(): lax.all_gather(attended, 'tp', axis=0, tiled=True, axis_index_groups=alon...  12.5 us
    ppermute x3, starting transfers between devices, shards(): heads.append(lax.ppermute(attended, 'tp', moves))  9.17 us
    ppermute x1, waiting for transfers between devices, shards(): other_up = lax.ppermute(up_weight[0], 'tp', swaps)  8.97 us
  transfers between devices with their start and end apart: 11, of which 4 were waited for; matrix products, arithmetic and copies ran while one was open for 0% of the time, Pallas kernels for 5%

profile of v7, /device:TPU:6, one launch (start us, length us, event | category | flops | bytes accessed | tf_op | source)
XLA Modules:
  0.0 166.8 jit_solution(5653375262707329397)
XLA Ops:
  0.7 1.5 shard_map.163
  2.2 32.5 %all_to_all.20 = bf16[32,16,128]{2,1,0:T(8,128)(2,1)S(1)} all-to-all(bf16[32,16,128]{2,1,0:T(8,128)(2,1)S(1)} %bitcast.18), channel_id=1, replica_groups=mesh['ep'=32,'tp'=16] {'ep'}, dimensions={0} | all-to-all | bytes 262144 | tf_op jit(solution)/shard_map/all_to_all | solution.py:278
  35.8 7.4 %all-to-all-start.1 = ((bf16[16,256,128]{2,1,0:T(8,128)(2,1)}), bf16[16,256,128]{2,1,0:T(8,128)(2,1)S(1)}, u32[]{:S(2)}, u32[]{:S(2)}) async-start(bf16[16,256,128]{2,1,0:T(8,128)(2,1)} %shard_map.164), calls=%async_computation.1 | async-start | bytes 2097152 | tf_op jit(solution)/shard_map/all_to_all | solution.py:278
  43.2 2.8 %collective-permute-start.6 = (bf16[2048,128]{1,0:T(8,128)(2,1)S(1)}, bf16[2048,128]{1,0:T(8,128)(2,1)S(1)}, u32[]{:S(2)}, u32[]{:S(2)}) collective-permute-start(bf16[2048,128]{1,0:T(8,128)(2,1)S(1)} %bitcast.20), channel_id=1, source_target_pairs={{0,1},{1,0},{2,3},{3,2},{4,5},{5,4},{6,7},{7,6},{8,9},{9,8},{10,11... | collective-permute-start | bytes 1572872 | tf_op jit(solution)/shard_map/ppermute | solution.py:300
  46.0 3.1 %collective-permute-start.7 = (bf16[2048,128]{1,0:T(8,128)(2,1)S(1)}, bf16[2048,128]{1,0:T(8,128)(2,1)S(1)}, u32[]{:S(2)}, u32[]{:S(2)}) collective-permute-start(bf16[2048,128]{1,0:T(8,128)(2,1)S(1)} %bitcast.22), channel_id=1, source_target_pairs={{0,1},{1,0},{2,3},{3,2},{4,5},{5,4},{6,7},{7,6},{8,9},{9,8},{10,11... | collective-permute-start | bytes 1572872 | tf_op jit(solution)/shard_map/ppermute | solution.py:301
  49.1 19.2 %collective-permute-done.6.g1_ref = bf16[2048,128]{1,0:T(8,128)(2,1)S(1)} collective-permute-done((bf16[2048,128]{1,0:T(8,128)(2,1)S(1)}, bf16[2048,128]{1,0:T(8,128)(2,1)S(1)}, u32[]{:S(2)}, u32[]{:S(2)}) %collective-permute-start.6) | collective-permute-done | bytes 524320 | tf_op jit(solution)/shard_map/ppermute | solution.py:300
  68.3 9.0 %collective-permute-done.7.u1_ref = bf16[2048,128]{1,0:T(8,128)(2,1)S(1)} collective-permute-done((bf16[2048,128]{1,0:T(8,128)(2,1)S(1)}, bf16[2048,128]{1,0:T(8,128)(2,1)S(1)}, u32[]{:S(2)}, u32[]{:S(2)}) %collective-permute-start.7) | collective-permute-done | bytes 524320 | tf_op jit(solution)/shard_map/ppermute | solution.py:301
  77.3 2.2 %shard_map.165 = bf16[16,512,128]{2,1,0:T(8,128)(2,1)} custom-call(s32[1]{0:T(128)} %bitcast.tp_ref, bf16[16,256,128]{2,1,0:T(8,128)(2,1)S(1)} %all-to-all-done.1.x_ref, bf16[2048,128]{1,0:T(8,128)(2,1)S(1)} %bitcast.21, bf16[2048,128]{1,0:T(8,128)(2,1)S(1)} %bitcast.23, bf16[2048,128]{1,0:T(8,128)(2,1)S(1)} %collective-permute-done.6.g1_ref, ...), custom_call_target="tpu_custom_call" | custom-call | flops 536870912 | bytes 1048576 | tf_op jit(solution)/shard_map/pallas_call | solution.py:35
  79.5 7.7 %all-to-all-start.2 = ((bf16[16,512,128]{2,1,0:T(8,128)(2,1)}), bf16[16,512,128]{2,1,0:T(8,128)(2,1)S(1)}, u32[]{:S(2)}, u32[]{:S(2)}) async-start(bf16[16,512,128]{2,1,0:T(8,128)(2,1)} %shard_map.165), calls=%async_computation.2 | async-start | bytes 4194304 | tf_op jit(solution)/shard_map/all_to_all | solution.py:278
  87.1 1.9 %shard_map.158 = (bf16[128,64]{1,0:T(8,128)(2,1)S(1)}, bf16[144,128]{1,0:T(8,128)(2,1)S(1)}) custom-call(bf16[128,2048]{1,0:T(8,128)(2,1)} %rows_ref.2, f32[1,2048]{1,0:T(1,128)} %bitcast.33, bf16[64,2048]{1,0:T(8,128)(2,1)} %bitcast.29, bf16[64,2048]{1,0:T(8,128)(2,1)} %bitcast.30, bf16[64,2048]{1,0:T(8,128)(2,1)} %bitcast.31, bf16[1,128]{1,0:T(2,128)(2,1)} %bias_ref.1), custom_call_target="tpu_custom_call" | custom-call | flops 268435456 | bytes 1048576 | tf_op jit(solution)/shard_map/pallas_call | solution.py:35
  89.0 5.6 %all_gather.9 = bf16[288,128]{1,0:T(8,128)(2,1)S(1)} all-gather(bf16[144,128]{1,0:T(8,128)(2,1)S(1)} %get-tuple-element.7), channel_id=1, replica_groups={{0,64},{16,80},{32,96},{48,112},{128,192},{144,208},{160,224},{176,240}..., dimensions={0}, use_global_device_ids=true | all-gather | bytes 110592 | tf_op jit(solution)/shard_map/all_gather | solution.py:302
  94.6 20.6 %all_gather.10.own_ref = bf16[1152,128]{1,0:T(8,128)(2,1)S(1)} all-gather(bf16[288,128]{1,0:T(8,128)(2,1)S(1)} %all_gather.9), channel_id=1, replica_groups={{0,128,256,384},{16,144,272,400},{32,160,288,416},{48,176,304,432},{64,..., dimensions={0}, use_global_device_ids=true | all-gather | bytes 368640 | tf_op jit(solution)/shard_map/all_gather | solution.py:303
  115.2 2.0 %collective-permute-start.1 = (bf16[1152,128]{1,0:T(8,128)(2,1)S(1)}, bf16[1152,128]{1,0:T(8,128)(2,1)S(1)}, u32[]{:S(2)}, u32[]{:S(2)}) collective-permute-start(bf16[1152,128]{1,0:T(8,128)(2,1)S(1)} %all_gather.10.own_ref), channel_id=1, source_target_pairs={{0,32},{16,48},{32,0},{48,16},{64,96},{80,112},{96,64},{112,80},{1... | collective-permute-start | bytes 884744 | tf_op jit(solution)/shard_map/ppermute | solution.py:304
  117.2 1.9 %collective-permute-start = (bf16[1152,128]{1,0:T(8,128)(2,1)S(1)}, bf16[1152,128]{1,0:T(8,128)(2,1)S(1)}, u32[]{:S(2)}, u32[]{:S(2)}) collective-permute-start(bf16[1152,128]{1,0:T(8,128)(2,1)S(1)} %all_gather.10.own_ref), channel_id=1, source_target_pairs={{0,16},{16,0},{32,48},{48,32},{64,80},{80,64},{96,112},{112,96},{1... | collective-permute-start | bytes 884744 | tf_op jit(solution)/shard_map/ppermute | solution.py:313
  119.1 4.7 %collective-permute-done.1.far_ref = bf16[1152,128]{1,0:T(8,128)(2,1)S(1)} collective-permute-done((bf16[1152,128]{1,0:T(8,128)(2,1)S(1)}, bf16[1152,128]{1,0:T(8,128)(2,1)S(1)}, u32[]{:S(2)}, u32[]{:S(2)}) %collective-permute-start.1) | collective-permute-done | bytes 294944 | tf_op jit(solution)/shard_map/ppermute | solution.py:304
  123.8 1.9 %collective-permute-start.2 = (bf16[1152,128]{1,0:T(8,128)(2,1)S(1)}, bf16[1152,128]{1,0:T(8,128)(2,1)}, u32[]{:S(2)}, u32[]{:S(2)}) collective-permute-start(bf16[1152,128]{1,0:T(8,128)(2,1)S(1)} %collective-permute-done.1.far_ref), channel_id=1, source_target_pairs={{0,16},{16,0},{32,48},{48,32},{64,80},{80,64},{96,112},{112,96},{1... | collective-permute-start | bytes 884744 | tf_op jit(solution)/shard_map/ppermute | solution.py:314
  125.7 1.4 shard_map.166
  127.1 7.0 %all-to-all-start.3 = ((bf16[32,16,128]{2,1,0:T(8,128)(2,1)}), bf16[32,16,128]{2,1,0:T(8,128)(2,1)S(1)}, u32[]{:S(2)}, u32[]{:S(2)}) async-start(bf16[32,16,128]{2,1,0:T(8,128)(2,1)} %bitcast.15), calls=%async_computation.3 | async-start | bytes 262144 | tf_op jit(solution)/shard_map/all_to_all | solution.py:278
  134.1 4.2 %shard_map.159.refs_0_ = bf16[64,128]{1,0:T(8,128)(2,1)S(1)} custom-call(s32[1]{0:T(128)} %bitcast.1.pos_ref, bf16[128,64]{1,0:T(8,128)(2,1)S(1)} %get-tuple-element.6.q_ref, bf16[1152,128]{1,0:T(8,128)(2,1)S(1)} %all_gather.10.own_ref, bf16[1152,128]{1,0:T(8,128)(2,1)S(1)} %collective-permute-done.other_ref, ...), custom_call_target="tpu_custom_call" | custom-call | flops 1073741824 | bytes 1048576 | tf_op jit(solution)/shard_map/pallas_call | solution.py:35
  138.3 2.3 %collective-permute-start.3 = (bf16[64,128]{1,0:T(8,128)(2,1)S(1)}, bf16[64,128]{1,0:T(8,128)(2,1)S(1)}, u32[]{:S(2)}, u32[]{:S(2)}) collective-permute-start(bf16[64,128]{1,0:T(8,128)(2,1)S(1)} %shard_map.159.refs_0_), channel_id=1, source_target_pairs={{1,0},{2,1},{3,2},{0,3},{5,4},{6,5},{7,6},{4,7},{9,8},{10,9},{11,1... | collective-permute-start | bytes 49160 | tf_op jit(solution)/shard_map/ppermute | solution.py:321
  140.6 4.8 %collective-permute-start.4 = (bf16[64,128]{1,0:T(8,128)(2,1)S(1)}, bf16[64,128]{1,0:T(8,128)(2,1)S(1)}, u32[]{:S(2)}, u32[]{:S(2)}) collective-permute-start(bf16[64,128]{1,0:T(8,128)(2,1)S(1)} %shard_map.159.refs_0_), channel_id=1, source_target_pairs={{3,0},{0,1},{1,2},{2,3},{7,4},{4,5},{5,6},{6,7},{11,8},{8,9},{9,10... | collective-permute-start | bytes 49160 | tf_op jit(solution)/shard_map/ppermute | solution.py:321
  145.3 2.1 %collective-permute-start.5 = (bf16[64,128]{1,0:T(8,128)(2,1)S(1)}, bf16[64,128]{1,0:T(8,128)(2,1)S(1)}, u32[]{:S(2)}, u32[]{:S(2)}) collective-permute-start(bf16[64,128]{1,0:T(8,128)(2,1)S(1)} %shard_map.159.refs_0_), channel_id=1, source_target_pairs={{2,0},{3,1},{0,2},{1,3},{6,4},{7,5},{4,6},{5,7},{10,8},{11,9},{8,1... | collective-permute-start | bytes 49160 | tf_op jit(solution)/shard_map/ppermute | solution.py:321
  147.9 4.6 %collective-permute-done.5.refs_3_ = bf16[64,128]{1,0:T(8,128)(2,1)S(1)} collective-permute-done((bf16[64,128]{1,0:T(8,128)(2,1)S(1)}, bf16[64,128]{1,0:T(8,128)(2,1)S(1)}, u32[]{:S(2)}, u32[]{:S(2)}) %collective-permute-start.5) | collective-permute-done | bytes 16416 | tf_op jit(solution)/shard_map/ppermute | solution.py:321
  152.5 12.5 %all_gather.11.x_ref = bf16[1024,128]{1,0:T(8,128)(2,1)S(1)} all-gather(bf16[256,128]{1,0:T(8,128)(2,1)S(1)} %shard_map.160), channel_id=1, replica_groups={{0,4,8,12},{1,5,9,13},{2,6,10,14},{3,7,11,15},{16,20,24,28},{17,21,25,2..., dimensions={0}, use_global_device_ids=true | all-gather | bytes 327680 | tf_op jit(solution)/shard_map/all_gather | solution.py:328
  (26 shorter events, 3.3 us)
Async XLA Ops:
  0.6 42.6 %copy-start.1 = (bf16[1,2048,128]{2,1,0:T(8,128)(2,1)S(1)}, bf16[1,2048,128]{2,1,0:T(8,128)(2,1)}, u32[]{:S(2)}) copy-start(bf16[1,2048,128]{2,1,0:T(8,128)(2,1)} %param.27) | copy-start | bytes 1572868
  0.6 45.4 %copy-start.2 = (bf16[1,2048,128]{2,1,0:T(8,128)(2,1)S(1)}, bf16[1,2048,128]{2,1,0:T(8,128)(2,1)}, u32[]{:S(2)}) copy-start(bf16[1,2048,128]{2,1,0:T(8,128)(2,1)} %param.28) | copy-start | bytes 1572868
  35.8 41.5 %all-to-all-start.1 = ((bf16[16,256,128]{2,1,0:T(8,128)(2,1)}), bf16[16,256,128]{2,1,0:T(8,128)(2,1)S(1)}, u32[]{:S(2)}, u32[]{:S(2)}) async-start(bf16[16,256,128]{2,1,0:T(8,128)(2,1)} %shard_map.164), calls=%async_computation.1 | async-start | bytes 2097152 | tf_op jit(solution)/shard_map/all_to_all | solution.py:278
  43.2 25.1 %collective-permute-start.6 = (bf16[2048,128]{1,0:T(8,128)(2,1)S(1)}, bf16[2048,128]{1,0:T(8,128)(2,1)S(1)}, u32[]{:S(2)}, u32[]{:S(2)}) collective-permute-start(bf16[2048,128]{1,0:T(8,128)(2,1)S(1)} %bitcast.20), channel_id=1, source_target_pairs={{0,1},{1,0},{2,3},{3,2},{4,5},{5,4},{6,7},{7,6},{8,9},{9,8},{10,11... | collective-permute-start | bytes 1572872 | tf_op jit(solution)/shard_map/ppermute | solution.py:300
  46.0 31.2 %collective-permute-start.7 = (bf16[2048,128]{1,0:T(8,128)(2,1)S(1)}, bf16[2048,128]{1,0:T(8,128)(2,1)S(1)}, u32[]{:S(2)}, u32[]{:S(2)}) collective-permute-start(bf16[2048,128]{1,0:T(8,128)(2,1)S(1)} %bitcast.22), channel_id=1, source_target_pairs={{0,1},{1,0},{2,3},{3,2},{4,5},{5,4},{6,7},{7,6},{8,9},{9,8},{10,11... | collective-permute-start | bytes 1572872 | tf_op jit(solution)/shard_map/ppermute | solution.py:301
  79.4 46.3 %copy-start = (bf16[1,2048,128]{2,1,0:T(8,128)(2,1)S(1)}, bf16[1,2048,128]{2,1,0:T(8,128)(2,1)}, u32[]{:S(2)}) copy-start(bf16[1,2048,128]{2,1,0:T(8,128)(2,1)} %param.29) | copy-start | bytes 1572868
  79.5 46.2 %all-to-all-start.2 = ((bf16[16,512,128]{2,1,0:T(8,128)(2,1)}), bf16[16,512,128]{2,1,0:T(8,128)(2,1)S(1)}, u32[]{:S(2)}, u32[]{:S(2)}) async-start(bf16[16,512,128]{2,1,0:T(8,128)(2,1)} %shard_map.165), calls=%async_computation.2 | async-start | bytes 4194304 | tf_op jit(solution)/shard_map/all_to_all | solution.py:278
  115.2 8.6 %collective-permute-start.1 = (bf16[1152,128]{1,0:T(8,128)(2,1)S(1)}, bf16[1152,128]{1,0:T(8,128)(2,1)S(1)}, u32[]{:S(2)}, u32[]{:S(2)}) collective-permute-start(bf16[1152,128]{1,0:T(8,128)(2,1)S(1)} %all_gather.10.own_ref), channel_id=1, source_target_pairs={{0,32},{16,48},{32,0},{48,16},{64,96},{80,112},{96,64},{112,80},{1... | collective-permute-start | bytes 884744 | tf_op jit(solution)/shard_map/ppermute | solution.py:304
  117.2 16.9 %collective-permute-start = (bf16[1152,128]{1,0:T(8,128)(2,1)S(1)}, bf16[1152,128]{1,0:T(8,128)(2,1)S(1)}, u32[]{:S(2)}, u32[]{:S(2)}) collective-permute-start(bf16[1152,128]{1,0:T(8,128)(2,1)S(1)} %all_gather.10.own_ref), channel_id=1, source_target_pairs={{0,16},{16,0},{32,48},{48,32},{64,80},{80,64},{96,112},{112,96},{1... | collective-permute-start | bytes 884744 | tf_op jit(solution)/shard_map/ppermute | solution.py:313
  123.8 10.3 %collective-permute-start.2 = (bf16[1152,128]{1,0:T(8,128)(2,1)S(1)}, bf16[1152,128]{1,0:T(8,128)(2,1)}, u32[]{:S(2)}, u32[]{:S(2)}) collective-permute-start(bf16[1152,128]{1,0:T(8,128)(2,1)S(1)} %collective-permute-done.1.far_ref), channel_id=1, source_target_pairs={{0,16},{16,0},{32,48},{48,32},{64,80},{80,64},{96,112},{112,96},{1... | collective-permute-start | bytes 884744 | tf_op jit(solution)/shard_map/ppermute | solution.py:314
  127.1 20.4 %copy-start.4 = (s32[128,2]{0,1:T(2,128)S(1)}, s32[128,2]{0,1:T(2,128)}, u32[]{:S(2)}) copy-start(s32[128,2]{0,1:T(2,128)} %param.24) | copy-start | bytes 3076
  127.1 20.4 %copy-start.5 = (f32[128,4]{0,1:T(4,128)S(1)}, f32[128,4]{0,1:T(4,128)}, u32[]{:S(2)}) copy-start(f32[128,4]{0,1:T(4,128)} %param.25) | copy-start | bytes 6148
  127.1 20.4 %copy-start.6 = (f32[128,2]{0,1:T(2,128)S(1)}, f32[128,2]{0,1:T(2,128)}, u32[]{:S(2)}) copy-start(f32[128,2]{0,1:T(2,128)} %param.26) | copy-start | bytes 3076
  127.1 38.9 %all-to-all-start.3 = ((bf16[32,16,128]{2,1,0:T(8,128)(2,1)}), bf16[32,16,128]{2,1,0:T(8,128)(2,1)S(1)}, u32[]{:S(2)}, u32[]{:S(2)}) async-start(bf16[32,16,128]{2,1,0:T(8,128)(2,1)} %bitcast.15), calls=%async_computation.3 | async-start | bytes 262144 | tf_op jit(solution)/shard_map/all_to_all | solution.py:278
  134.1 30.9 %copy-start.3 = (bf16[1024,128]{1,0:T(8,128)(2,1)S(1)}, bf16[1024,128]{1,0:T(8,128)(2,1)}, u32[]{:S(2)}) copy-start(bf16[1024,128]{1,0:T(8,128)(2,1)} %w_ref.1) | copy-start | bytes 786436
  138.3 9.6 %collective-permute-start.3 = (bf16[64,128]{1,0:T(8,128)(2,1)S(1)}, bf16[64,128]{1,0:T(8,128)(2,1)S(1)}, u32[]{:S(2)}, u32[]{:S(2)}) collective-permute-start(bf16[64,128]{1,0:T(8,128)(2,1)S(1)} %shard_map.159.refs_0_), channel_id=1, source_target_pairs={{1,0},{2,1},{3,2},{0,3},{5,4},{6,5},{7,6},{4,7},{9,8},{10,9},{11,1... | collective-permute-start | bytes 49160 | tf_op jit(solution)/shard_map/ppermute | solution.py:321
  140.6 7.3 %collective-permute-start.4 = (bf16[64,128]{1,0:T(8,128)(2,1)S(1)}, bf16[64,128]{1,0:T(8,128)(2,1)S(1)}, u32[]{:S(2)}, u32[]{:S(2)}) collective-permute-start(bf16[64,128]{1,0:T(8,128)(2,1)S(1)} %shard_map.159.refs_0_), channel_id=1, source_target_pairs={{3,0},{0,1},{1,2},{2,3},{7,4},{4,5},{5,6},{6,7},{11,8},{8,9},{9,10... | collective-permute-start | bytes 49160 | tf_op jit(solution)/shard_map/ppermute | solution.py:321
  145.3 7.1 %collective-permute-start.5 = (bf16[64,128]{1,0:T(8,128)(2,1)S(1)}, bf16[64,128]{1,0:T(8,128)(2,1)S(1)}, u32[]{:S(2)}, u32[]{:S(2)}) collective-permute-start(bf16[64,128]{1,0:T(8,128)(2,1)S(1)} %shard_map.159.refs_0_), channel_id=1, source_target_pairs={{2,0},{3,1},{0,2},{1,3},{6,4},{7,5},{4,6},{5,7},{10,8},{11,9},{8,1... | collective-permute-start | bytes 49160 | tf_op jit(solution)/shard_map/ppermute | solution.py:321

commit v8 on v7

--- a/solution.py
+++ b/solution.py
@@ -114,24 +114,15 @@
         copy.wait()
 
 
-def hidden_body(tp_ref, x_ref, g0_ref, u0_ref, g1_ref, u1_ref, out_ref, hidden_ref, sems):
+def hidden_body(x_ref, g0_ref, u0_ref, g1_ref, u1_ref, out_ref, hidden_ref, sems):
     parts = x_ref.shape[0]
-    even = tp_ref[0] % 2 == 0
-    own_weights = jnp.concatenate([g0_ref[...], u0_ref[...]], axis=1)
-    other_weights = jnp.concatenate([g1_ref[...], u1_ref[...]], axis=1)
-
-    def gated(both):
+    x = jnp.concatenate([x_ref[k] for k in range(parts)], axis=1)
+    copies = []
+    for m, (g_ref, u_ref) in enumerate(((g0_ref, u0_ref), (g1_ref, u1_ref))):
+        both = nn(x, jnp.concatenate([g_ref[...], u_ref[...]], axis=1))
         gate, up = both[:, :BLOCK], both[:, BLOCK:]
-        return gate * jax.nn.sigmoid(gate) * up
-
-    copies = []
-    for m in range(2):
-        x = [x_ref[k, m * BLOCK : (m + 1) * BLOCK, :] for k in range(parts)]
-        x = jnp.concatenate(x, axis=1)
-        own, other = gated(nn(x, own_weights)), gated(nn(x, other_weights))
         span = slice(m * ROWS, (m + 1) * ROWS)
-        hidden_ref[m * ROWS : m * ROWS + BLOCK, :] = jnp.where(even, own, other).astype(bf16)
-        hidden_ref[m * ROWS + BLOCK : (m + 1) * ROWS, :] = jnp.where(even, other, own).astype(bf16)
+        hidden_ref[span, :] = (gate * jax.nn.sigmoid(gate) * up).astype(bf16)
         for k in range(parts):
             target = out_ref.at[k, span, :]
             copies.append(
@@ -146,21 +137,27 @@
     parts = x_ref.shape[0]
     rows = []
     for half in range(2):
-        for m in range(2):
-            at = m * ROWS
-            pieces = [
-                x_ref[k, at + e * BLOCK : at + (e + 1) * BLOCK, :]
-                for k in range(half, parts, 2)
-                for e in range(2)
-            ]
-            rows.append(jnp.concatenate(pieces, axis=1))
+        pieces = []
+        for k in range(half, parts, 2):
+            own, other = x_ref[k, 0:ROWS, :], x_ref[k, ROWS:SLOTS, :]
+            pieces += [own, other] if half == 0 else [other, own]
+        rows.append(jnp.concatenate(pieces, axis=1))
     out_ref[...] = nn(jnp.concatenate(rows, axis=0), w_ref[...]).astype(bf16)
 
 
-def attend_body(pos_ref, q_ref, own_ref, other_ref, far_ref, far_other_ref, out_ref):
+def order_body(pos_ref, own_ref, other_ref, out_ref):
+    core = pos_ref[0] % 2
+    own, other = own_ref[...], other_ref[...]
+    rows = own.shape[0]
+    out_ref[0:rows, :] = jnp.where(core == 1, own, other)
+    out_ref[rows:, :] = jnp.where(core == 1, other, own)
+
+
+def attend_body(pos_ref, q_ref, near_ref, far_ref, far_other_ref, out_ref):
     here = pos_ref[0]
     core = here % 2
-    chips = 2 * own_ref.shape[0] // MSG
+    rows = far_ref.shape[0]
+    chips = 2 * rows // MSG
     odd = (here // 2) % 2
     q = q_ref[...]
     wide = (2 * BLOCK, 2 * BLOCK)
@@ -176,11 +173,13 @@
         messages, starts = [], []
         for w in range(WIDTH):
             z = chips - 1 - (k * WIDTH + w)
-            at = pl.ds(pl.multiple_of((z // 2) * MSG, 16), MSG)
+            at = pl.multiple_of((z // 2) * MSG, 16)
             near = odd == (WIDTH - 1 - w) % 2
-            own = jnp.where(near, own_ref[at, :], far_ref[at, :])
-            other = jnp.where(near, other_ref[at, :], far_other_ref[at, :])
-            messages += [jnp.where(core == 1, own, other), jnp.where(core == 1, other, own)]
+            far, other = far_ref[pl.ds(at, MSG), :], far_other_ref[pl.ds(at, MSG), :]
+            upper = jnp.where(core == 1, far, other)
+            lower = jnp.where(core == 1, other, far)
+            messages.append(jnp.where(near, near_ref[pl.ds(at, MSG), :], upper))
+            messages.append(jnp.where(near, near_ref[pl.ds(rows + at, MSG), :], lower))
             starts += [(here - 2 * z - 1) * BLOCK, (here - 2 * z) * BLOCK]
         scores = [nn(q, m[0:HEAD, :]) + m[BLOCK : BLOCK + 1, :].astype(f32) for m in messages]
         causal = [offset < start for start in starts]
@@ -305,15 +304,17 @@
     routed = call_out(halves_body, 0, 1, struct((tp, ROWS, BLOCK), bf16), 1 << 24, [], tp)(routed)
     routed = exchange(routed, "tp")
     own_hidden = [pltpu.VMEM((SLOTS, BLOCK), bf16)]
-    hidden = call_out(hidden_body, 1, 5, copies, 1 << 29, own_hidden, 2 * tp)(
-        column, routed, gate_weight[0], up_weight[0], other_gate, other_up
+    hidden = call_out(hidden_body, 0, 5, copies, 1 << 29, own_hidden, 2 * tp)(
+        routed, gate_weight[0], up_weight[0], other_gate, other_up
     )
     hidden = exchange(hidden, "tp")
     cores = [(e, e ^ 1) for e in range(ep)]
     own_other = lax.ppermute(own, "ep", cores)
+    ordered = struct((2 * own.shape[0], BLOCK), bf16)
+    near = call(order_body, 1, 2, ordered, 1 << 22)(here.reshape(1), own, own_other)
     far_other = lax.ppermute(far, "ep", cores)
-    attended = call(attend_body, 1, 5, struct((HEAD, BLOCK), bf16), 1 << 30)(
-        here.reshape(1), query, own, own_other, far, far_other
+    attended = call(attend_body, 1, 4, struct((HEAD, BLOCK), bf16), 1 << 30)(
+        here.reshape(1), query, near, far, far_other
     )
     heads = [attended]
     for d in OFFSETS[1:]:

time: 167 us -> 168 us (level)
    pallas_call x10 -> x11, Pallas kernels: 14.3 us -> 14.7 us  [run(): return kernel(*args)]
where the time goes in v8:
time: 168 us; the launch traced here: 167 us
  blocking collectives  71.2 us (42%)
  starting transfers between devices  42.8 us (25%)
  waiting for transfers between devices  37.7 us (22%)
  Pallas kernels  14.7 us (9%)
    all_to_all x1, blocking collectives, exchange(): return lax.all_to_all(x, axis, split_axis=0, concat_axis=0, tiled=True)  32.5 us
    all_to_all x3, starting transfers between devices, exchange(): return lax.all_to_all(x, axis, split_axis=0, concat_axis=0, tiled=True)  22.1 us
    all_gather x1, blocking collectives, shards(): lax.all_gather(keys, 'ep', axis=0, tiled=True, axis_index_groups=strided)  20.6 us
    ppermute x1, waiting for transfers between devices, shards(): other_gate = lax.ppermute(gate_weight[0], 'tp', swaps)  19.2 us
    pallas_call x11, Pallas kernels, run(): return kernel(*args)  14.7 us
    all_gather x1, blocking collectives, shards(): lax.all_gather(attended, 'tp', axis=0, tiled=True, axis_index_groups=alon...  12.5 us
    ppermute x3, starting transfers between devices, shards(): heads.append(lax.ppermute(attended, 'tp', moves))  8.97 us
    ppermute x1, waiting for transfers between devices, shards(): other_up = lax.ppermute(up_weight[0], 'tp', swaps)  8.97 us
  transfers between devices with their start and end apart: 11, of which 4 were waited for; matrix products, arithmetic and copies ran while one was open for 0% of the time, Pallas kernels for 5%

profile of v8, /device:TPU:6, one launch (start us, length us, event | category | flops | bytes accessed | tf_op | source)
XLA Modules:
  0.0 167.2 jit_solution(49235282557735432)
XLA Ops:
  0.7 1.5 shard_map.164
  2.2 32.5 %all_to_all.20 = bf16[32,16,128]{2,1,0:T(8,128)(2,1)S(1)} all-to-all(bf16[32,16,128]{2,1,0:T(8,128)(2,1)S(1)} %bitcast.22), channel_id=1, replica_groups=mesh['ep'=32,'tp'=16] {'ep'}, dimensions={0} | all-to-all | bytes 262144 | tf_op jit(solution)/shard_map/all_to_all | solution.py:277
  35.8 7.4 %all-to-all-start.1 = ((bf16[16,256,128]{2,1,0:T(8,128)(2,1)}), bf16[16,256,128]{2,1,0:T(8,128)(2,1)S(1)}, u32[]{:S(2)}, u32[]{:S(2)}) async-start(bf16[16,256,128]{2,1,0:T(8,128)(2,1)} %shard_map.165), calls=%async_computation.1 | async-start | bytes 2097152 | tf_op jit(solution)/shard_map/all_to_all | solution.py:277
  43.2 2.8 %collective-permute-start.6 = (bf16[2048,128]{1,0:T(8,128)(2,1)S(1)}, bf16[2048,128]{1,0:T(8,128)(2,1)S(1)}, u32[]{:S(2)}, u32[]{:S(2)}) collective-permute-start(bf16[2048,128]{1,0:T(8,128)(2,1)S(1)} %bitcast.17), channel_id=1, source_target_pairs={{0,1},{1,0},{2,3},{3,2},{4,5},{5,4},{6,7},{7,6},{8,9},{9,8},{10,11... | collective-permute-start | bytes 1572872 | tf_op jit(solution)/shard_map/ppermute | solution.py:299
  46.0 3.1 %collective-permute-start.7 = (bf16[2048,128]{1,0:T(8,128)(2,1)S(1)}, bf16[2048,128]{1,0:T(8,128)(2,1)S(1)}, u32[]{:S(2)}, u32[]{:S(2)}) collective-permute-start(bf16[2048,128]{1,0:T(8,128)(2,1)S(1)} %bitcast.19), channel_id=1, source_target_pairs={{0,1},{1,0},{2,3},{3,2},{4,5},{5,4},{6,7},{7,6},{8,9},{9,8},{10,11... | collective-permute-start | bytes 1572872 | tf_op jit(solution)/shard_map/ppermute | solution.py:300
  49.1 19.2 %collective-permute-done.6.g1_ref = bf16[2048,128]{1,0:T(8,128)(2,1)S(1)} collective-permute-done((bf16[2048,128]{1,0:T(8,128)(2,1)S(1)}, bf16[2048,128]{1,0:T(8,128)(2,1)S(1)}, u32[]{:S(2)}, u32[]{:S(2)}) %collective-permute-start.6) | collective-permute-done | bytes 524320 | tf_op jit(solution)/shard_map/ppermute | solution.py:299
  68.3 9.0 %collective-permute-done.7.u1_ref = bf16[2048,128]{1,0:T(8,128)(2,1)S(1)} collective-permute-done((bf16[2048,128]{1,0:T(8,128)(2,1)S(1)}, bf16[2048,128]{1,0:T(8,128)(2,1)S(1)}, u32[]{:S(2)}, u32[]{:S(2)}) %collective-permute-start.7) | collective-permute-done | bytes 524320 | tf_op jit(solution)/shard_map/ppermute | solution.py:300
  77.3 2.4 %shard_map.166 = bf16[16,512,128]{2,1,0:T(8,128)(2,1)} custom-call(bf16[16,256,128]{2,1,0:T(8,128)(2,1)S(1)} %all-to-all-done.1.x_ref, bf16[2048,128]{1,0:T(8,128)(2,1)S(1)} %bitcast.18, bf16[2048,128]{1,0:T(8,128)(2,1)S(1)} %bitcast.20, bf16[2048,128]{1,0:T(8,128)(2,1)S(1)} %collective-permute-done.6.g1_ref, bf16[2048,128]{1,0:T(8,128)(2,1)S(1)} %collective-permute-done.7.u1_ref), custom_call_target="tpu_custom_call" | custom-call | flops 536870912 | bytes 1048576 | tf_op jit(solution)/shard_map/pallas_call | solution.py:35
  79.6 7.7 %all-to-all-start.2 = ((bf16[16,512,128]{2,1,0:T(8,128)(2,1)}), bf16[16,512,128]{2,1,0:T(8,128)(2,1)S(1)}, u32[]{:S(2)}, u32[]{:S(2)}) async-start(bf16[16,512,128]{2,1,0:T(8,128)(2,1)} %shard_map.166), calls=%async_computation.2 | async-start | bytes 4194304 | tf_op jit(solution)/shard_map/all_to_all | solution.py:277
  87.3 1.9 %shard_map.158 = (bf16[128,64]{1,0:T(8,128)(2,1)S(1)}, bf16[144,128]{1,0:T(8,128)(2,1)S(1)}) custom-call(bf16[128,2048]{1,0:T(8,128)(2,1)} %rows_ref.2, f32[1,2048]{1,0:T(1,128)} %bitcast.33, bf16[64,2048]{1,0:T(8,128)(2,1)} %bitcast.29, bf16[64,2048]{1,0:T(8,128)(2,1)} %bitcast.30, bf16[64,2048]{1,0:T(8,128)(2,1)} %bitcast.31, bf16[1,128]{1,0:T(2,128)(2,1)} %bias_ref.1), custom_call_target="tpu_custom_call" | custom-call | flops 268435456 | bytes 1048576 | tf_op jit(solution)/shard_map/pallas_call | solution.py:35
  89.2 5.6 %all_gather.9 = bf16[288,128]{1,0:T(8,128)(2,1)S(1)} all-gather(bf16[144,128]{1,0:T(8,128)(2,1)S(1)} %get-tuple-element.7), channel_id=1, replica_groups={{0,64},{16,80},{32,96},{48,112},{128,192},{144,208},{160,224},{176,240}..., dimensions={0}, use_global_device_ids=true | all-gather | bytes 110592 | tf_op jit(solution)/shard_map/all_gather | solution.py:301
  94.8 20.6 %all_gather.10.own_ref = bf16[1152,128]{1,0:T(8,128)(2,1)S(1)} all-gather(bf16[288,128]{1,0:T(8,128)(2,1)S(1)} %all_gather.9), channel_id=1, replica_groups={{0,128,256,384},{16,144,272,400},{32,160,288,416},{48,176,304,432},{64,..., dimensions={0}, use_global_device_ids=true | all-gather | bytes 368640 | tf_op jit(solution)/shard_map/all_gather | solution.py:302
  115.3 2.0 %collective-permute-start.1 = (bf16[1152,128]{1,0:T(8,128)(2,1)S(1)}, bf16[1152,128]{1,0:T(8,128)(2,1)S(1)}, u32[]{:S(2)}, u32[]{:S(2)}) collective-permute-start(bf16[1152,128]{1,0:T(8,128)(2,1)S(1)} %all_gather.10.own_ref), channel_id=1, source_target_pairs={{0,32},{16,48},{32,0},{48,16},{64,96},{80,112},{96,64},{112,80},{1... | collective-permute-start | bytes 884744 | tf_op jit(solution)/shard_map/ppermute | solution.py:303
  117.3 1.9 %collective-permute-start = (bf16[1152,128]{1,0:T(8,128)(2,1)S(1)}, bf16[1152,128]{1,0:T(8,128)(2,1)S(1)}, u32[]{:S(2)}, u32[]{:S(2)}) collective-permute-start(bf16[1152,128]{1,0:T(8,128)(2,1)S(1)} %all_gather.10.own_ref), channel_id=1, source_target_pairs={{0,16},{16,0},{32,48},{48,32},{64,80},{80,64},{96,112},{112,96},{1... | collective-permute-start | bytes 884744 | tf_op jit(solution)/shard_map/ppermute | solution.py:312
  119.3 4.7 %collective-permute-done.1.far_ref = bf16[1152,128]{1,0:T(8,128)(2,1)S(1)} collective-permute-done((bf16[1152,128]{1,0:T(8,128)(2,1)S(1)}, bf16[1152,128]{1,0:T(8,128)(2,1)S(1)}, u32[]{:S(2)}, u32[]{:S(2)}) %collective-permute-start.1) | collective-permute-done | bytes 294944 | tf_op jit(solution)/shard_map/ppermute | solution.py:303
  124.0 1.9 %collective-permute-start.2 = (bf16[1152,128]{1,0:T(8,128)(2,1)S(1)}, bf16[1152,128]{1,0:T(8,128)(2,1)}, u32[]{:S(2)}, u32[]{:S(2)}) collective-permute-start(bf16[1152,128]{1,0:T(8,128)(2,1)S(1)} %collective-permute-done.1.far_ref), channel_id=1, source_target_pairs={{0,16},{16,0},{32,48},{48,32},{64,80},{80,64},{96,112},{112,96},{1... | collective-permute-start | bytes 884744 | tf_op jit(solution)/shard_map/ppermute | solution.py:315
  125.9 1.4 shard_map.167
  127.3 7.0 %all-to-all-start.3 = ((bf16[32,16,128]{2,1,0:T(8,128)(2,1)}), bf16[32,16,128]{2,1,0:T(8,128)(2,1)S(1)}, u32[]{:S(2)}, u32[]{:S(2)}) async-start(bf16[32,16,128]{2,1,0:T(8,128)(2,1)} %bitcast.15), calls=%async_computation.3 | async-start | bytes 262144 | tf_op jit(solution)/shard_map/all_to_all | solution.py:277
  134.5 4.2 %shard_map.160.refs_0_ = bf16[64,128]{1,0:T(8,128)(2,1)S(1)} custom-call(s32[1]{0:T(128)} %bitcast.1.pos_ref, bf16[128,64]{1,0:T(8,128)(2,1)S(1)} %get-tuple-element.6.q_ref, bf16[2304,128]{1,0:T(8,128)(2,1)S(1)} %shard_map.159.near_ref, bf16[1152,128]{1,0:T(8,128)(2,1)S(1)} %collective-permute-done.1.far_ref, ...), custom_call_target="tpu_custom_call" | custom-call | flops 1073741824 | bytes 1048576 | tf_op jit(solution)/shard_map/pallas_call | solution.py:35
  138.7 1.9 %collective-permute-start.3 = (bf16[64,128]{1,0:T(8,128)(2,1)S(1)}, bf16[64,128]{1,0:T(8,128)(2,1)S(1)}, u32[]{:S(2)}, u32[]{:S(2)}) collective-permute-start(bf16[64,128]{1,0:T(8,128)(2,1)S(1)} %shard_map.160.refs_0_), channel_id=1, source_target_pairs={{1,0},{2,1},{3,2},{0,3},{5,4},{6,5},{7,6},{4,7},{9,8},{10,9},{11,1... | collective-permute-start | bytes 49160 | tf_op jit(solution)/shard_map/ppermute | solution.py:322
  140.6 5.1 %collective-permute-start.4 = (bf16[64,128]{1,0:T(8,128)(2,1)S(1)}, bf16[64,128]{1,0:T(8,128)(2,1)S(1)}, u32[]{:S(2)}, u32[]{:S(2)}) collective-permute-start(bf16[64,128]{1,0:T(8,128)(2,1)S(1)} %shard_map.160.refs_0_), channel_id=1, source_target_pairs={{3,0},{0,1},{1,2},{2,3},{7,4},{4,5},{5,6},{6,7},{11,8},{8,9},{9,10... | collective-permute-start | bytes 49160 | tf_op jit(solution)/shard_map/ppermute | solution.py:322
  145.7 1.9 %collective-permute-start.5 = (bf16[64,128]{1,0:T(8,128)(2,1)S(1)}, bf16[64,128]{1,0:T(8,128)(2,1)S(1)}, u32[]{:S(2)}, u32[]{:S(2)}) collective-permute-start(bf16[64,128]{1,0:T(8,128)(2,1)S(1)} %shard_map.160.refs_0_), channel_id=1, source_target_pairs={{2,0},{3,1},{0,2},{1,3},{6,4},{7,5},{4,6},{5,7},{10,8},{11,9},{8,1... | collective-permute-start | bytes 49160 | tf_op jit(solution)/shard_map/ppermute | solution.py:322
  148.1 4.8 %collective-permute-done.5.refs_3_ = bf16[64,128]{1,0:T(8,128)(2,1)S(1)} collective-permute-done((bf16[64,128]{1,0:T(8,128)(2,1)S(1)}, bf16[64,128]{1,0:T(8,128)(2,1)S(1)}, u32[]{:S(2)}, u32[]{:S(2)}) %collective-permute-start.5) | collective-permute-done | bytes 16416 | tf_op jit(solution)/shard_map/ppermute | solution.py:322
  152.9 12.5 %all_gather.11.x_ref = bf16[1024,128]{1,0:T(8,128)(2,1)S(1)} all-gather(bf16[256,128]{1,0:T(8,128)(2,1)S(1)} %shard_map.161), channel_id=1, replica_groups={{0,4,8,12},{1,5,9,13},{2,6,10,14},{3,7,11,15},{16,20,24,28},{17,21,25,2..., dimensions={0}, use_global_device_ids=true | all-gather | bytes 327680 | tf_op jit(solution)/shard_map/all_gather | solution.py:329
  (27 shorter events, 3.4 us)
Async XLA Ops:
  0.6 42.6 %copy-start = (bf16[1,2048,128]{2,1,0:T(8,128)(2,1)S(1)}, bf16[1,2048,128]{2,1,0:T(8,128)(2,1)}, u32[]{:S(2)}) copy-start(bf16[1,2048,128]{2,1,0:T(8,128)(2,1)} %param.27) | copy-start | bytes 1572868
  0.6 45.4 %copy-start.1 = (bf16[1,2048,128]{2,1,0:T(8,128)(2,1)S(1)}, bf16[1,2048,128]{2,1,0:T(8,128)(2,1)}, u32[]{:S(2)}) copy-start(bf16[1,2048,128]{2,1,0:T(8,128)(2,1)} %param.28) | copy-start | bytes 1572868
  35.8 41.5 %all-to-all-start.1 = ((bf16[16,256,128]{2,1,0:T(8,128)(2,1)}), bf16[16,256,128]{2,1,0:T(8,128)(2,1)S(1)}, u32[]{:S(2)}, u32[]{:S(2)}) async-start(bf16[16,256,128]{2,1,0:T(8,128)(2,1)} %shard_map.165), calls=%async_computation.1 | async-start | bytes 2097152 | tf_op jit(solution)/shard_map/all_to_all | solution.py:277
  43.2 25.1 %collective-permute-start.6 = (bf16[2048,128]{1,0:T(8,128)(2,1)S(1)}, bf16[2048,128]{1,0:T(8,128)(2,1)S(1)}, u32[]{:S(2)}, u32[]{:S(2)}) collective-permute-start(bf16[2048,128]{1,0:T(8,128)(2,1)S(1)} %bitcast.17), channel_id=1, source_target_pairs={{0,1},{1,0},{2,3},{3,2},{4,5},{5,4},{6,7},{7,6},{8,9},{9,8},{10,11... | collective-permute-start | bytes 1572872 | tf_op jit(solution)/shard_map/ppermute | solution.py:299
  46.0 31.2 %collective-permute-start.7 = (bf16[2048,128]{1,0:T(8,128)(2,1)S(1)}, bf16[2048,128]{1,0:T(8,128)(2,1)S(1)}, u32[]{:S(2)}, u32[]{:S(2)}) collective-permute-start(bf16[2048,128]{1,0:T(8,128)(2,1)S(1)} %bitcast.19), channel_id=1, source_target_pairs={{0,1},{1,0},{2,3},{3,2},{4,5},{5,4},{6,7},{7,6},{8,9},{9,8},{10,11... | collective-permute-start | bytes 1572872 | tf_op jit(solution)/shard_map/ppermute | solution.py:300
  79.6 46.3 %copy-start.2 = (bf16[1,2048,128]{2,1,0:T(8,128)(2,1)S(1)}, bf16[1,2048,128]{2,1,0:T(8,128)(2,1)}, u32[]{:S(2)}) copy-start(bf16[1,2048,128]{2,1,0:T(8,128)(2,1)} %param.29) | copy-start | bytes 1572868
  79.6 46.2 %all-to-all-start.2 = ((bf16[16,512,128]{2,1,0:T(8,128)(2,1)}), bf16[16,512,128]{2,1,0:T(8,128)(2,1)S(1)}, u32[]{:S(2)}, u32[]{:S(2)}) async-start(bf16[16,512,128]{2,1,0:T(8,128)(2,1)} %shard_map.166), calls=%async_computation.2 | async-start | bytes 4194304 | tf_op jit(solution)/shard_map/all_to_all | solution.py:277
  115.3 8.6 %collective-permute-start.1 = (bf16[1152,128]{1,0:T(8,128)(2,1)S(1)}, bf16[1152,128]{1,0:T(8,128)(2,1)S(1)}, u32[]{:S(2)}, u32[]{:S(2)}) collective-permute-start(bf16[1152,128]{1,0:T(8,128)(2,1)S(1)} %all_gather.10.own_ref), channel_id=1, source_target_pairs={{0,32},{16,48},{32,0},{48,16},{64,96},{80,112},{96,64},{112,80},{1... | collective-permute-start | bytes 884744 | tf_op jit(solution)/shard_map/ppermute | solution.py:303
  117.3 17.0 %collective-permute-start = (bf16[1152,128]{1,0:T(8,128)(2,1)S(1)}, bf16[1152,128]{1,0:T(8,128)(2,1)S(1)}, u32[]{:S(2)}, u32[]{:S(2)}) collective-permute-start(bf16[1152,128]{1,0:T(8,128)(2,1)S(1)} %all_gather.10.own_ref), channel_id=1, source_target_pairs={{0,16},{16,0},{32,48},{48,32},{64,80},{80,64},{96,112},{112,96},{1... | collective-permute-start | bytes 884744 | tf_op jit(solution)/shard_map/ppermute | solution.py:312
  124.0 10.5 %collective-permute-start.2 = (bf16[1152,128]{1,0:T(8,128)(2,1)S(1)}, bf16[1152,128]{1,0:T(8,128)(2,1)}, u32[]{:S(2)}, u32[]{:S(2)}) collective-permute-start(bf16[1152,128]{1,0:T(8,128)(2,1)S(1)} %collective-permute-done.1.far_ref), channel_id=1, source_target_pairs={{0,16},{16,0},{32,48},{48,32},{64,80},{80,64},{96,112},{112,96},{1... | collective-permute-start | bytes 884744 | tf_op jit(solution)/shard_map/ppermute | solution.py:315
  127.3 39.1 %all-to-all-start.3 = ((bf16[32,16,128]{2,1,0:T(8,128)(2,1)}), bf16[32,16,128]{2,1,0:T(8,128)(2,1)S(1)}, u32[]{:S(2)}, u32[]{:S(2)}) async-start(bf16[32,16,128]{2,1,0:T(8,128)(2,1)} %bitcast.15), calls=%async_computation.3 | async-start | bytes 262144 | tf_op jit(solution)/shard_map/all_to_all | solution.py:277
  134.4 13.3 %copy-start.4 = (s32[128,2]{0,1:T(2,128)S(1)}, s32[128,2]{0,1:T(2,128)}, u32[]{:S(2)}) copy-start(s32[128,2]{0,1:T(2,128)} %param.24) | copy-start | bytes 3076
  134.4 13.3 %copy-start.5 = (f32[128,4]{0,1:T(4,128)S(1)}, f32[128,4]{0,1:T(4,128)}, u32[]{:S(2)}) copy-start(f32[128,4]{0,1:T(4,128)} %param.25) | copy-start | bytes 6148
  134.4 13.3 %copy-start.6 = (f32[128,2]{0,1:T(2,128)S(1)}, f32[128,2]{0,1:T(2,128)}, u32[]{:S(2)}) copy-start(f32[128,2]{0,1:T(2,128)} %param.26) | copy-start | bytes 3076
  134.5 31.0 %copy-start.3 = (bf16[1024,128]{1,0:T(8,128)(2,1)S(1)}, bf16[1024,128]{1,0:T(8,128)(2,1)}, u32[]{:S(2)}) copy-start(bf16[1024,128]{1,0:T(8,128)(2,1)} %w_ref.1) | copy-start | bytes 786436
  138.7 9.4 %collective-permute-start.3 = (bf16[64,128]{1,0:T(8,128)(2,1)S(1)}, bf16[64,128]{1,0:T(8,128)(2,1)S(1)}, u32[]{:S(2)}, u32[]{:S(2)}) collective-permute-start(bf16[64,128]{1,0:T(8,128)(2,1)S(1)} %shard_map.160.refs_0_), channel_id=1, source_target_pairs={{1,0},{2,1},{3,2},{0,3},{5,4},{6,5},{7,6},{4,7},{9,8},{10,9},{11,1... | collective-permute-start | bytes 49160 | tf_op jit(solution)/shard_map/ppermute | solution.py:322
  140.6 7.5 %collective-permute-start.4 = (bf16[64,128]{1,0:T(8,128)(2,1)S(1)}, bf16[64,128]{1,0:T(8,128)(2,1)S(1)}, u32[]{:S(2)}, u32[]{:S(2)}) collective-permute-start(bf16[64,128]{1,0:T(8,128)(2,1)S(1)} %shard_map.160.refs_0_), channel_id=1, source_target_pairs={{3,0},{0,1},{1,2},{2,3},{7,4},{4,5},{5,6},{6,7},{11,8},{8,9},{9,10... | collective-permute-start | bytes 49160 | tf_op jit(solution)/shard_map/ppermute | solution.py:322
  145.7 7.1 %collective-permute-start.5 = (bf16[64,128]{1,0:T(8,128)(2,1)S(1)}, bf16[64,128]{1,0:T(8,128)(2,1)S(1)}, u32[]{:S(2)}, u32[]{:S(2)}) collective-permute-start(bf16[64,128]{1,0:T(8,128)(2,1)S(1)} %shard_map.160.refs_0_), channel_id=1, source_target_pairs={{2,0},{3,1},{0,2},{1,3},{6,4},{7,5},{4,6},{5,7},{10,8},{11,9},{8,1... | collective-permute-start | bytes 49160 | tf_op jit(solution)/shard_map/ppermute | solution.py:322

commit v9 on v8

--- a/solution.py
+++ b/solution.py
@@ -16,6 +16,7 @@
 ROWS = SLOTS // 2
 MSG = 144
 WIDTH = 4
+PARTS = 4
 OFFSETS = (0, 1, 3, 2)
 
 epsilon = 1e-06
@@ -26,7 +27,7 @@
 SMEM = pl.BlockSpec(memory_space=pltpu.SMEM)
 
 
-def call(body, n_scalar, n_in, outs, flops, mib=16, hbm=(), **more):
+def call(body, n_scalar, n_in, outs, flops, mib=16, hbm=(), own=None, **more):
     def run(*args):
         args = [
             pltpu.with_memory_space_constraint(a, pltpu.HBM) if k in hbm else a
@@ -34,10 +35,11 @@
         ]
         return kernel(*args)
 
+    raw = pl.BlockSpec(memory_space=pltpu.HBM)
     kernel = pl.pallas_call(
         body,
         out_shape=outs,
-        in_specs=[SMEM] * n_scalar + [pl.BlockSpec()] * n_in,
+        in_specs=[SMEM] * n_scalar + [raw if k == own else pl.BlockSpec() for k in range(n_in)],
         cost_estimate=pl.CostEstimate(flops=flops, bytes_accessed=1 << 20, transcendentals=0),
         compiler_params=pltpu.CompilerParams(vmem_limit_bytes=mib << 20),
         **more,
@@ -78,18 +80,30 @@
     return place0.astype(i32), place1.astype(i32)
 
 
-def dispatch_body(tp_ref, rows_ref, gain_ref, ids_ref, out_ref):
-    x = rows_ref[...].astype(f32)
-    inv = lax.rsqrt(jnp.mean(x * x, axis=-1, keepdims=True) + epsilon)
-    at = pl.multiple_of(tp_ref[0] * BLOCK, BLOCK)
-    own = rows_ref[:, pl.ds(at, BLOCK)].astype(f32)
-    own = (own * inv * gain_ref[:, pl.ds(at, BLOCK)]).astype(bf16)
+def dispatch_body(tp_ref, rows_ref, gain_ref, ids_ref, out_ref, x_ref, sems):
+    part = BLOCK // PARTS
+    copies = []
+    for k in range(PARTS):
+        span = slice(k * part, (k + 1) * part)
+        copies.append(pltpu.make_async_copy(rows_ref.at[span, :], x_ref.at[span, :], sems.at[k]))
+        copies[-1].start()
     ids = ids_ref[...]
     first, second = ids[0:1, :], ids[1:2, :]
     place0, place1 = places(first, second)
     slot = iota((SLOTS, BLOCK), 0)
     hit = (slot == first * CAP + place0) | (slot == second * CAP + place1)
-    out_ref[...] = nn(ones_where(hit).astype(bf16), own).astype(bf16)
+    hit = ones_where(hit).astype(bf16)
+    at = pl.multiple_of(tp_ref[0] * BLOCK, BLOCK)
+    gain = gain_ref[:, pl.ds(at, BLOCK)]
+    owns = []
+    for k in range(PARTS):
+        copies[k].wait()
+        span = slice(k * part, (k + 1) * part)
+        x = x_ref[span, :].astype(f32)
+        inv = lax.rsqrt(jnp.mean(x * x, axis=-1, keepdims=True) + epsilon)
+        own = x_ref[span, pl.ds(at, BLOCK)].astype(f32)
+        owns.append((own * inv * gain).astype(bf16))
+    out_ref[...] = nn(hit, jnp.concatenate(owns, axis=0)).astype(bf16)
 
 
 def project_body(rows_ref, gain_ref, wq_ref, wk_ref, wv_ref, bias_ref, q_ref, msg_ref):
@@ -207,13 +221,15 @@
         refs[-1][k * HEAD : (k + 1) * HEAD, :] = ref[...]
 
 
-def mix_body(tp_ref, x_ref, w_ref, out_ref):
-    column = tp_ref[0] % 4
-    weights = []
-    for k in range(x_ref.shape[0] // HEAD):
-        head = k - k % 4 + (column + OFFSETS[k % 4]) % 4
-        weights.append(w_ref[pl.ds(pl.multiple_of(head * HEAD, HEAD), HEAD), :])
-    x = jnp.transpose(x_ref[...].astype(f32)).astype(bf16)
+def mix_body(tp_ref, x0_ref, x1_ref, x2_ref, x3_ref, w_ref, out_ref):
+    line, column = tp_ref[0] // 4, tp_ref[0] % 4
+    weights, pieces = [], []
+    for d, x_ref in zip(OFFSETS, (x0_ref, x1_ref, x2_ref, x3_ref)):
+        pieces.append(x_ref[...])
+        for e in OFFSETS:
+            head = (line + d) % 4 * 4 + (column + e) % 4
+            weights.append(w_ref[pl.ds(pl.multiple_of(head * HEAD, HEAD), HEAD), :])
+    x = jnp.transpose(jnp.concatenate(pieces, axis=0).astype(f32)).astype(bf16)
     out_ref[...] = nn(x, jnp.concatenate(weights, axis=0)).astype(bf16)
 
 
@@ -269,8 +285,8 @@
     run = chips // 4
     strided = [[(m + 4 * k) * 2 + c for k in range(run)] for m in range(4) for c in range(2)]
     pairs = [[(z + 2 * b) * 2 + c for b in range(2)] for z in range(chips) if z % 4 < 2 for c in range(2)]
-    side = tp // 4
-    along_y = [[y * 4 + x for y in range(side)] for x in range(4)]
+    row_moves = [[(k - k % 4 + (k + d) % 4, k) for k in range(tp)] for d in range(4)]
+    column_moves = [[((k + 4 * d) % tp, k) for k in range(tp)] for d in range(4)]
     struct = jax.ShapeDtypeStruct
 
     def exchange(x, axis):
@@ -282,7 +298,9 @@
     ids = expert_ids.T
     column = lax.axis_index("tp").reshape(1)
 
-    send = call(dispatch_body, 1, 3, slots, 1 << 27, hbm=(1, 2, 3))(
+    scratch = [pltpu.VMEM((BLOCK, expert_rows.shape[1]), bf16), pltpu.SemaphoreType.DMA((PARTS,))]
+    more = {"own": 0, "scratch_shapes": scratch}
+    send = call(dispatch_body, 1, 3, slots, 1 << 27, hbm=(1, 2, 3), **more)(
         column, expert_rows, expert_gain[None, :], ids
     )
     routed = exchange(send.reshape(ep, CAP, BLOCK), "ep").reshape(SLOTS, BLOCK)
@@ -317,17 +335,19 @@
         here.reshape(1), query, near, far, far_other
     )
     heads = [attended]
-    for d in OFFSETS[1:]:
-        moves = [(k - k % 4 + (k + d) % 4, k) for k in range(tp)]
-        heads.append(lax.ppermute(attended, "tp", moves))
+    for d in OFFSETS[1:3]:
+        heads.append(lax.ppermute(attended, "tp", row_moves[d]))
+    heads.append(lax.ppermute(attended, "tp", row_moves[OFFSETS[3]]))
     stacked = struct((len(heads) * HEAD, BLOCK), bf16)
     attended = call(pack_body, 0, len(heads), stacked, 1 << 20)(*heads)
     result = call(down_body, 0, 2, slots, 1 << 28)(hidden, down_weight[0])
     back = exchange(result.reshape(ep, CAP, BLOCK), "ep").reshape(SLOTS, BLOCK)
     tables = (struct((2 * BLOCK, SLOTS), bf16), struct((BLOCK, BLOCK), f32))
     picks, table = call(plan_body, 0, 3, tables, 1 << 26)(ids, group_logits.T, pair_logits.T)
-    attended = lax.all_gather(attended, "tp", axis=0, tiled=True, axis_index_groups=along_y)
-    mixed = call(mix_body, 1, 2, square, 1 << 26)(column, attended, out_weight)
+    stacks = [attended]
+    for d in OFFSETS[1:]:
+        stacks.append(lax.ppermute(attended, "tp", column_moves[d]))
+    mixed = call(mix_body, 1, 5, square, 1 << 26)(column, *stacks, out_weight)
     expert_out = call(combine_body, 0, 3, square, 1 << 27)(picks, table, back)
     return (mixed, expert_out)
 

time: 168 us -> 167 us (level)
  blocking collectives: 71.2 us -> 58.6 us
  starting transfers between devices: 42.8 us -> 54.1 us
    all_gather x1 -> x0, blocking collectives: 12.5 us -> none  [shards(): lax.all_gather(attended, 'tp', axis=0, tiled=True, axis_index_groups=alon...]
    ppermute x3 -> x6, starting transfers between devices: 8.97 us -> 19.5 us  [the longest x3 10.5 us: shards(): stacks.append(lax.ppermute(attended, 'tp', column_moves[d]))]
    ppermute x1, waiting for transfers between devices: 19.2 us -> 8.97 us  [shards(): other_gate = lax.ppermute(gate_weight[0], 'tp', swaps)]
    ppermute x1, waiting for transfers between devices: 8.97 us -> 19.2 us  [shards(): other_up = lax.ppermute(up_weight[0], 'tp', swaps)]
    ppermute x1, waiting for transfers between devices: 4.69 us -> 0.01 us  [shards(): far = lax.ppermute(own, 'ep', [(e, e ^ 2) for e in range(ep)])]
    ppermute x3 -> x6, waiting for transfers between devices: 4.79 us -> 8.34 us  [the longest x1 5.19 us: shards(): heads.append(lax.ppermute(attended, 'tp', row_moves[OFFSETS[3]]))]
  transfers between devices with their start and end apart: 11 -> 14, of which waited for: 4 -> 6; matrix products, arithmetic and copies ran while one was open for 0% -> 0% of each run, Pallas kernels for 5% -> 5%
where the time goes in v9:
time: 167 us; the launch traced here: 166 us
  blocking collectives  58.6 us (35%)
  starting transfers between devices  54.1 us (32%)
  waiting for transfers between devices  37.7 us (23%)
  Pallas kernels  14.4 us (9%)
    all_to_all x1, blocking collectives, exchange(): return lax.all_to_all(x, axis, split_axis=0, concat_axis=0, tiled=True)  32.5 us
    all_to_all x3, starting transfers between devices, exchange(): return lax.all_to_all(x, axis, split_axis=0, concat_axis=0, tiled=True)  22.5 us
    all_gather x1, blocking collectives, shards(): lax.all_gather(keys, 'ep', axis=0, tiled=True, axis_index_groups=strided)  20.6 us
    ppermute x1, waiting for transfers between devices, shards(): other_up = lax.ppermute(up_weight[0], 'tp', swaps)  19.2 us
    pallas_call x11, Pallas kernels, run(): return kernel(*args)  14.4 us
    ppermute x3, starting transfers between devices, shards(): stacks.append(lax.ppermute(attended, 'tp', column_moves[d]))  10.5 us
    ppermute x1, waiting for transfers between devices, shards(): other_gate = lax.ppermute(gate_weight[0], 'tp', swaps)  8.97 us
    ppermute x2, starting transfers between devices, shards(): heads.append(lax.ppermute(attended, 'tp', row_moves[d]))  7.05 us
  transfers between devices with their start and end apart: 14, of which 6 were waited for; matrix products, arithmetic and copies ran while one was open for 0% of the time, Pallas kernels for 5%

profile of v9, /device:TPU:6, one launch (start us, length us, event | category | flops | bytes accessed | tf_op | source)
XLA Modules:
  0.0 165.8 jit_solution(13610583022523397206)
XLA Ops:
  0.7 2.4 %shard_map.164 = bf16[512,128]{1,0:T(8,128)(2,1)S(1)} custom-call(s32[1]{0:T(128)} %bitcast.tp_ref, bf16[128,2048]{1,0:T(8,128)(2,1)} %rows_ref.3, f32[1,2048]{1,0:T(1,128)} %bitcast.32, s32[2,128]{1,0:T(2,128)} %bitcast.25), custom_call_target="tpu_custom_call" | custom-call | flops 134217728 | bytes 1048576 | tf_op jit(solution)/shard_map/pallas_call | solution.py:36
  3.0 32.5 %all_to_all.20 = bf16[32,16,128]{2,1,0:T(8,128)(2,1)S(1)} all-to-all(bf16[32,16,128]{2,1,0:T(8,128)(2,1)S(1)} %bitcast.22), channel_id=1, replica_groups=mesh['ep'=32,'tp'=16] {'ep'}, dimensions={0} | all-to-all | bytes 262144 | tf_op jit(solution)/shard_map/all_to_all | solution.py:293
  36.7 7.4 %all-to-all-start.1 = ((bf16[16,256,128]{2,1,0:T(8,128)(2,1)}), bf16[16,256,128]{2,1,0:T(8,128)(2,1)S(1)}, u32[]{:S(2)}, u32[]{:S(2)}) async-start(bf16[16,256,128]{2,1,0:T(8,128)(2,1)} %shard_map.165), calls=%async_computation.1 | async-start | bytes 2097152 | tf_op jit(solution)/shard_map/all_to_all | solution.py:293
  44.1 2.8 %collective-permute-start.10 = (bf16[2048,128]{1,0:T(8,128)(2,1)S(1)}, bf16[2048,128]{1,0:T(8,128)(2,1)S(1)}, u32[]{:S(2)}, u32[]{:S(2)}) collective-permute-start(bf16[2048,128]{1,0:T(8,128)(2,1)S(1)} %bitcast.19), channel_id=1, source_target_pairs={{0,1},{1,0},{2,3},{3,2},{4,5},{5,4},{6,7},{7,6},{8,9},{9,8},{10,11... | collective-permute-start | bytes 1572872 | tf_op jit(solution)/shard_map/ppermute | solution.py:318
  46.9 3.1 %collective-permute-start.9 = (bf16[2048,128]{1,0:T(8,128)(2,1)S(1)}, bf16[2048,128]{1,0:T(8,128)(2,1)S(1)}, u32[]{:S(2)}, u32[]{:S(2)}) collective-permute-start(bf16[2048,128]{1,0:T(8,128)(2,1)S(1)} %bitcast.17), channel_id=1, source_target_pairs={{0,1},{1,0},{2,3},{3,2},{4,5},{5,4},{6,7},{7,6},{8,9},{9,8},{10,11... | collective-permute-start | bytes 1572872 | tf_op jit(solution)/shard_map/ppermute | solution.py:317
  50.0 19.2 %collective-permute-done.10.u1_ref = bf16[2048,128]{1,0:T(8,128)(2,1)S(1)} collective-permute-done((bf16[2048,128]{1,0:T(8,128)(2,1)S(1)}, bf16[2048,128]{1,0:T(8,128)(2,1)S(1)}, u32[]{:S(2)}, u32[]{:S(2)}) %collective-permute-start.10) | collective-permute-done | bytes 524320 | tf_op jit(solution)/shard_map/ppermute | solution.py:318
  69.2 9.0 %collective-permute-done.9.g1_ref = bf16[2048,128]{1,0:T(8,128)(2,1)S(1)} collective-permute-done((bf16[2048,128]{1,0:T(8,128)(2,1)S(1)}, bf16[2048,128]{1,0:T(8,128)(2,1)S(1)}, u32[]{:S(2)}, u32[]{:S(2)}) %collective-permute-start.9) | collective-permute-done | bytes 524320 | tf_op jit(solution)/shard_map/ppermute | solution.py:317
  78.1 2.3 %shard_map.166 = bf16[16,512,128]{2,1,0:T(8,128)(2,1)} custom-call(bf16[16,256,128]{2,1,0:T(8,128)(2,1)S(1)} %all-to-all-done.1.x_ref, bf16[2048,128]{1,0:T(8,128)(2,1)S(1)} %bitcast.18, bf16[2048,128]{1,0:T(8,128)(2,1)S(1)} %bitcast.20, bf16[2048,128]{1,0:T(8,128)(2,1)S(1)} %collective-permute-done.9.g1_ref, ...), custom_call_target="tpu_custom_call" | custom-call | flops 536870912 | bytes 1048576 | tf_op jit(solution)/shard_map/pallas_call | solution.py:36
  80.5 7.7 %all-to-all-start.2 = ((bf16[16,512,128]{2,1,0:T(8,128)(2,1)}), bf16[16,512,128]{2,1,0:T(8,128)(2,1)S(1)}, u32[]{:S(2)}, u32[]{:S(2)}) async-start(bf16[16,512,128]{2,1,0:T(8,128)(2,1)} %shard_map.166), calls=%async_computation.2 | async-start | bytes 4194304 | tf_op jit(solution)/shard_map/all_to_all | solution.py:293
  88.2 1.9 %shard_map.158 = (bf16[128,64]{1,0:T(8,128)(2,1)S(1)}, bf16[144,128]{1,0:T(8,128)(2,1)S(1)}) custom-call(bf16[128,2048]{1,0:T(8,128)(2,1)} %rows_ref.2, f32[1,2048]{1,0:T(1,128)} %bitcast.33, bf16[64,2048]{1,0:T(8,128)(2,1)} %bitcast.29, bf16[64,2048]{1,0:T(8,128)(2,1)} %bitcast.30, bf16[64,2048]{1,0:T(8,128)(2,1)} %bitcast.31, bf16[1,128]{1,0:T(2,128)(2,1)} %bias_ref.1), custom_call_target="tpu_custom_call" | custom-call | flops 268435456 | bytes 1048576 | tf_op jit(solution)/shard_map/pallas_call | solution.py:36
  90.0 5.6 %all_gather.6 = bf16[288,128]{1,0:T(8,128)(2,1)S(1)} all-gather(bf16[144,128]{1,0:T(8,128)(2,1)S(1)} %get-tuple-element.7), channel_id=1, replica_groups={{0,64},{16,80},{32,96},{48,112},{128,192},{144,208},{160,224},{176,240}..., dimensions={0}, use_global_device_ids=true | all-gather | bytes 110592 | tf_op jit(solution)/shard_map/all_gather | solution.py:319
  95.6 20.6 %all_gather.7.own_ref = bf16[1152,128]{1,0:T(8,128)(2,1)S(1)} all-gather(bf16[288,128]{1,0:T(8,128)(2,1)S(1)} %all_gather.6), channel_id=1, replica_groups={{0,128,256,384},{16,144,272,400},{32,160,288,416},{48,176,304,432},{64,..., dimensions={0}, use_global_device_ids=true | all-gather | bytes 368640 | tf_op jit(solution)/shard_map/all_gather | solution.py:320
  116.2 2.0 %collective-permute-start.1 = (bf16[1152,128]{1,0:T(8,128)(2,1)S(1)}, bf16[1152,128]{1,0:T(8,128)(2,1)S(1)}, u32[]{:S(2)}, u32[]{:S(2)}) collective-permute-start(bf16[1152,128]{1,0:T(8,128)(2,1)S(1)} %all_gather.7.own_ref), channel_id=1, source_target_pairs={{0,32},{16,48},{32,0},{48,16},{64,96},{80,112},{96,64},{112,80},{1... | collective-permute-start | bytes 884744 | tf_op jit(solution)/shard_map/ppermute | solution.py:321
  119.5 7.4 %all-to-all-start.3 = ((bf16[32,16,128]{2,1,0:T(8,128)(2,1)}), bf16[32,16,128]{2,1,0:T(8,128)(2,1)S(1)}, u32[]{:S(2)}, u32[]{:S(2)}) async-start(bf16[32,16,128]{2,1,0:T(8,128)(2,1)} %bitcast.15), calls=%async_computation.3 | async-start | bytes 262144 | tf_op jit(solution)/shard_map/all_to_all | solution.py:293
  127.0 2.2 %collective-permute-start = (bf16[1152,128]{1,0:T(8,128)(2,1)S(1)}, bf16[1152,128]{1,0:T(8,128)(2,1)S(1)}, u32[]{:S(2)}, u32[]{:S(2)}) collective-permute-start(bf16[1152,128]{1,0:T(8,128)(2,1)S(1)} %all_gather.7.own_ref), channel_id=1, source_target_pairs={{0,16},{16,0},{32,48},{48,32},{64,80},{80,64},{96,112},{112,96},{1... | collective-permute-start | bytes 884744 | tf_op jit(solution)/shard_map/ppermute | solution.py:330
  129.2 2.1 %collective-permute-start.2 = (bf16[1152,128]{1,0:T(8,128)(2,1)S(1)}, bf16[1152,128]{1,0:T(8,128)(2,1)S(1)}, u32[]{:S(2)}, u32[]{:S(2)}) collective-permute-start(bf16[1152,128]{1,0:T(8,128)(2,1)S(1)} %collective-permute-done.1.far_ref), channel_id=1, source_target_pairs={{0,16},{16,0},{32,48},{48,32},{64,80},{80,64},{96,112},{112,96},{1... | collective-permute-start | bytes 884744 | tf_op jit(solution)/shard_map/ppermute | solution.py:333
  132.6 3.2 %shard_map.160.refs_0_ = bf16[64,128]{1,0:T(8,128)(2,1)S(1)} custom-call(s32[1]{0:T(128)} %bitcast.1.pos_ref, bf16[128,64]{1,0:T(8,128)(2,1)S(1)} %get-tuple-element.6.q_ref, bf16[2304,128]{1,0:T(8,128)(2,1)S(1)} %shard_map.159.near_ref, bf16[1152,128]{1,0:T(8,128)(2,1)S(1)} %collective-permute-done.1.far_ref, ...), custom_call_target="tpu_custom_call" | custom-call | flops 1073741824 | bytes 1048576 | tf_op jit(solution)/shard_map/pallas_call | solution.py:36
  135.8 2.7 %collective-permute-start.3 = (bf16[64,128]{1,0:T(8,128)(2,1)S(1)}, bf16[64,128]{1,0:T(8,128)(2,1)S(1)}, u32[]{:S(2)}, u32[]{:S(2)}) collective-permute-start(bf16[64,128]{1,0:T(8,128)(2,1)S(1)} %shard_map.160.refs_0_), channel_id=1, source_target_pairs={{1,0},{2,1},{3,2},{0,3},{5,4},{6,5},{7,6},{4,7},{9,8},{10,9},{11,1... | collective-permute-start | bytes 49160 | tf_op jit(solution)/shard_map/ppermute | solution.py:339
  138.5 4.4 %collective-permute-start.4 = (bf16[64,128]{1,0:T(8,128)(2,1)S(1)}, bf16[64,128]{1,0:T(8,128)(2,1)S(1)}, u32[]{:S(2)}, u32[]{:S(2)}) collective-permute-start(bf16[64,128]{1,0:T(8,128)(2,1)S(1)} %shard_map.160.refs_0_), channel_id=1, source_target_pairs={{3,0},{0,1},{1,2},{2,3},{7,4},{4,5},{5,6},{6,7},{11,8},{8,9},{9,10... | collective-permute-start | bytes 49160 | tf_op jit(solution)/shard_map/ppermute | solution.py:339
  142.9 1.9 %collective-permute-start.5 = (bf16[64,128]{1,0:T(8,128)(2,1)S(1)}, bf16[64,128]{1,0:T(8,128)(2,1)S(1)}, u32[]{:S(2)}, u32[]{:S(2)}) collective-permute-start(bf16[64,128]{1,0:T(8,128)(2,1)S(1)} %shard_map.160.refs_0_), channel_id=1, source_target_pairs={{2,0},{3,1},{0,2},{1,3},{6,4},{7,5},{4,6},{5,7},{10,8},{11,9},{8,1... | collective-permute-start | bytes 49160 | tf_op jit(solution)/shard_map/ppermute | solution.py:340
  144.8 5.2 %collective-permute-done.5.refs_3_ = bf16[64,128]{1,0:T(8,128)(2,1)S(1)} collective-permute-done((bf16[64,128]{1,0:T(8,128)(2,1)S(1)}, bf16[64,128]{1,0:T(8,128)(2,1)S(1)}, u32[]{:S(2)}, u32[]{:S(2)}) %collective-permute-start.5) | collective-permute-done | bytes 16416 | tf_op jit(solution)/shard_map/ppermute | solution.py:340
  150.0 4.5 %collective-permute-start.6 = (bf16[256,128]{1,0:T(8,128)(2,1)S(1)}, bf16[256,128]{1,0:T(8,128)(2,1)S(1)}, u32[]{:S(2)}, u32[]{:S(2)}) collective-permute-start(bf16[256,128]{1,0:T(8,128)(2,1)S(1)} %shard_map.161.x0_ref), channel_id=1, source_target_pairs={{4,0},{5,1},{6,2},{7,3},{8,4},{9,5},{10,6},{11,7},{12,8},{13,9},{1... | collective-permute-start | bytes 196616 | tf_op jit(solution)/shard_map/ppermute | solution.py:349
  154.5 1.9 %collective-permute-start.7 = (bf16[256,128]{1,0:T(8,128)(2,1)S(1)}, bf16[256,128]{1,0:T(8,128)(2,1)S(1)}, u32[]{:S(2)}, u32[]{:S(2)}) collective-permute-start(bf16[256,128]{1,0:T(8,128)(2,1)S(1)} %shard_map.161.x0_ref), channel_id=1, source_target_pairs={{12,0},{13,1},{14,2},{15,3},{0,4},{1,5},{2,6},{3,7},{4,8},{5,9},{6... | collective-permute-start | bytes 196616 | tf_op jit(solution)/shard_map/ppermute | solution.py:349
  156.4 4.1 %collective-permute-start.8 = (bf16[256,128]{1,0:T(8,128)(2,1)S(1)}, bf16[256,128]{1,0:T(8,128)(2,1)S(1)}, u32[]{:S(2)}, u32[]{:S(2)}) collective-permute-start(bf16[256,128]{1,0:T(8,128)(2,1)S(1)} %shard_map.161.x0_ref), channel_id=1, source_target_pairs={{8,0},{9,1},{10,2},{11,3},{12,4},{13,5},{14,6},{15,7},{0,8},{1,9},... | collective-permute-start | bytes 196616 | tf_op jit(solution)/shard_map/ppermute | solution.py:349
  (32 shorter events, 9.1 us)
Async XLA Ops:
  0.6 43.5 %copy-start.1 = (bf16[1,2048,128]{2,1,0:T(8,128)(2,1)S(1)}, bf16[1,2048,128]{2,1,0:T(8,128)(2,1)}, u32[]{:S(2)}) copy-start(bf16[1,2048,128]{2,1,0:T(8,128)(2,1)} %param.28) | copy-start | bytes 1572868
  0.6 46.2 %copy-start = (bf16[1,2048,128]{2,1,0:T(8,128)(2,1)S(1)}, bf16[1,2048,128]{2,1,0:T(8,128)(2,1)}, u32[]{:S(2)}) copy-start(bf16[1,2048,128]{2,1,0:T(8,128)(2,1)} %param.27) | copy-start | bytes 1572868
  36.7 41.5 %all-to-all-start.1 = ((bf16[16,256,128]{2,1,0:T(8,128)(2,1)}), bf16[16,256,128]{2,1,0:T(8,128)(2,1)S(1)}, u32[]{:S(2)}, u32[]{:S(2)}) async-start(bf16[16,256,128]{2,1,0:T(8,128)(2,1)} %shard_map.165), calls=%async_computation.1 | async-start | bytes 2097152 | tf_op jit(solution)/shard_map/all_to_all | solution.py:293
  44.1 25.1 %collective-permute-start.10 = (bf16[2048,128]{1,0:T(8,128)(2,1)S(1)}, bf16[2048,128]{1,0:T(8,128)(2,1)S(1)}, u32[]{:S(2)}, u32[]{:S(2)}) collective-permute-start(bf16[2048,128]{1,0:T(8,128)(2,1)S(1)} %bitcast.19), channel_id=1, source_target_pairs={{0,1},{1,0},{2,3},{3,2},{4,5},{5,4},{6,7},{7,6},{8,9},{9,8},{10,11... | collective-permute-start | bytes 1572872 | tf_op jit(solution)/shard_map/ppermute | solution.py:318
  46.9 31.2 %collective-permute-start.9 = (bf16[2048,128]{1,0:T(8,128)(2,1)S(1)}, bf16[2048,128]{1,0:T(8,128)(2,1)S(1)}, u32[]{:S(2)}, u32[]{:S(2)}) collective-permute-start(bf16[2048,128]{1,0:T(8,128)(2,1)S(1)} %bitcast.17), channel_id=1, source_target_pairs={{0,1},{1,0},{2,3},{3,2},{4,5},{5,4},{6,7},{7,6},{8,9},{9,8},{10,11... | collective-permute-start | bytes 1572872 | tf_op jit(solution)/shard_map/ppermute | solution.py:317
  80.5 37.7 %copy-start.2 = (bf16[1,2048,128]{2,1,0:T(8,128)(2,1)S(1)}, bf16[1,2048,128]{2,1,0:T(8,128)(2,1)}, u32[]{:S(2)}) copy-start(bf16[1,2048,128]{2,1,0:T(8,128)(2,1)} %param.29) | copy-start | bytes 1572868
  80.5 37.7 %all-to-all-start.2 = ((bf16[16,512,128]{2,1,0:T(8,128)(2,1)}), bf16[16,512,128]{2,1,0:T(8,128)(2,1)S(1)}, u32[]{:S(2)}, u32[]{:S(2)}) async-start(bf16[16,512,128]{2,1,0:T(8,128)(2,1)} %shard_map.166), calls=%async_computation.2 | async-start | bytes 4194304 | tf_op jit(solution)/shard_map/all_to_all | solution.py:293
  116.2 13.0 %collective-permute-start.1 = (bf16[1152,128]{1,0:T(8,128)(2,1)S(1)}, bf16[1152,128]{1,0:T(8,128)(2,1)S(1)}, u32[]{:S(2)}, u32[]{:S(2)}) collective-permute-start(bf16[1152,128]{1,0:T(8,128)(2,1)S(1)} %all_gather.7.own_ref), channel_id=1, source_target_pairs={{0,32},{16,48},{32,0},{48,16},{64,96},{80,112},{96,64},{112,80},{1... | collective-permute-start | bytes 884744 | tf_op jit(solution)/shard_map/ppermute | solution.py:321
  119.5 45.4 %all-to-all-start.3 = ((bf16[32,16,128]{2,1,0:T(8,128)(2,1)}), bf16[32,16,128]{2,1,0:T(8,128)(2,1)S(1)}, u32[]{:S(2)}, u32[]{:S(2)}) async-start(bf16[32,16,128]{2,1,0:T(8,128)(2,1)} %bitcast.15), calls=%async_computation.3 | async-start | bytes 262144 | tf_op jit(solution)/shard_map/all_to_all | solution.py:293
  127.0 4.4 %collective-permute-start = (bf16[1152,128]{1,0:T(8,128)(2,1)S(1)}, bf16[1152,128]{1,0:T(8,128)(2,1)S(1)}, u32[]{:S(2)}, u32[]{:S(2)}) collective-permute-start(bf16[1152,128]{1,0:T(8,128)(2,1)S(1)} %all_gather.7.own_ref), channel_id=1, source_target_pairs={{0,16},{16,0},{32,48},{48,32},{64,80},{80,64},{96,112},{112,96},{1... | collective-permute-start | bytes 884744 | tf_op jit(solution)/shard_map/ppermute | solution.py:330
  129.2 3.5 %collective-permute-start.2 = (bf16[1152,128]{1,0:T(8,128)(2,1)S(1)}, bf16[1152,128]{1,0:T(8,128)(2,1)S(1)}, u32[]{:S(2)}, u32[]{:S(2)}) collective-permute-start(bf16[1152,128]{1,0:T(8,128)(2,1)S(1)} %collective-permute-done.1.far_ref), channel_id=1, source_target_pairs={{0,16},{16,0},{32,48},{48,32},{64,80},{80,64},{96,112},{112,96},{1... | collective-permute-start | bytes 884744 | tf_op jit(solution)/shard_map/ppermute | solution.py:333
  131.4 29.1 %copy-start.4 = (s32[128,2]{0,1:T(2,128)S(1)}, s32[128,2]{0,1:T(2,128)}, u32[]{:S(2)}) copy-start(s32[128,2]{0,1:T(2,128)} %param.24) | copy-start | bytes 3076
  131.5 29.1 %copy-start.5 = (f32[128,4]{0,1:T(4,128)S(1)}, f32[128,4]{0,1:T(4,128)}, u32[]{:S(2)}) copy-start(f32[128,4]{0,1:T(4,128)} %param.25) | copy-start | bytes 6148
  131.5 29.1 %copy-start.6 = (f32[128,2]{0,1:T(2,128)S(1)}, f32[128,2]{0,1:T(2,128)}, u32[]{:S(2)}) copy-start(f32[128,2]{0,1:T(2,128)} %param.26) | copy-start | bytes 3076
  132.6 31.4 %copy-start.3 = (bf16[1024,128]{1,0:T(8,128)(2,1)S(1)}, bf16[1024,128]{1,0:T(8,128)(2,1)}, u32[]{:S(2)}) copy-start(bf16[1024,128]{1,0:T(8,128)(2,1)} %w_ref.1) | copy-start | bytes 786436
  135.8 9.0 %collective-permute-start.3 = (bf16[64,128]{1,0:T(8,128)(2,1)S(1)}, bf16[64,128]{1,0:T(8,128)(2,1)S(1)}, u32[]{:S(2)}, u32[]{:S(2)}) collective-permute-start(bf16[64,128]{1,0:T(8,128)(2,1)S(1)} %shard_map.160.refs_0_), channel_id=1, source_target_pairs={{1,0},{2,1},{3,2},{0,3},{5,4},{6,5},{7,6},{4,7},{9,8},{10,9},{11,1... | collective-permute-start | bytes 49160 | tf_op jit(solution)/shard_map/ppermute | solution.py:339
  138.5 6.3 %collective-permute-start.4 = (bf16[64,128]{1,0:T(8,128)(2,1)S(1)}, bf16[64,128]{1,0:T(8,128)(2,1)S(1)}, u32[]{:S(2)}, u32[]{:S(2)}) collective-permute-start(bf16[64,128]{1,0:T(8,128)(2,1)S(1)} %shard_map.160.refs_0_), channel_id=1, source_target_pairs={{3,0},{0,1},{1,2},{2,3},{7,4},{4,5},{5,6},{6,7},{11,8},{8,9},{9,10... | collective-permute-start | bytes 49160 | tf_op jit(solution)/shard_map/ppermute | solution.py:339
  142.9 7.1 %collective-permute-start.5 = (bf16[64,128]{1,0:T(8,128)(2,1)S(1)}, bf16[64,128]{1,0:T(8,128)(2,1)S(1)}, u32[]{:S(2)}, u32[]{:S(2)}) collective-permute-start(bf16[64,128]{1,0:T(8,128)(2,1)S(1)} %shard_map.160.refs_0_), channel_id=1, source_target_pairs={{2,0},{3,1},{0,2},{1,3},{6,4},{7,5},{4,6},{5,7},{10,8},{11,9},{8,1... | collective-permute-start | bytes 49160 | tf_op jit(solution)/shard_map/ppermute | solution.py:340
  150.0 10.9 %collective-permute-start.6 = (bf16[256,128]{1,0:T(8,128)(2,1)S(1)}, bf16[256,128]{1,0:T(8,128)(2,1)S(1)}, u32[]{:S(2)}, u32[]{:S(2)}) collective-permute-start(bf16[256,128]{1,0:T(8,128)(2,1)S(1)} %shard_map.161.x0_ref), channel_id=1, source_target_pairs={{4,0},{5,1},{6,2},{7,3},{8,4},{9,5},{10,6},{11,7},{12,8},{13,9},{1... | collective-permute-start | bytes 196616 | tf_op jit(solution)/shard_map/ppermute | solution.py:349
  154.5 7.7 %collective-permute-start.7 = (bf16[256,128]{1,0:T(8,128)(2,1)S(1)}, bf16[256,128]{1,0:T(8,128)(2,1)S(1)}, u32[]{:S(2)}, u32[]{:S(2)}) collective-permute-start(bf16[256,128]{1,0:T(8,128)(2,1)S(1)} %shard_map.161.x0_ref), channel_id=1, source_target_pairs={{12,0},{13,1},{14,2},{15,3},{0,4},{1,5},{2,6},{3,7},{4,8},{5,9},{6... | collective-permute-start | bytes 196616 | tf_op jit(solution)/shard_map/ppermute | solution.py:349
  156.4 7.7 %collective-permute-start.8 = (bf16[256,128]{1,0:T(8,128)(2,1)S(1)}, bf16[256,128]{1,0:T(8,128)(2,1)S(1)}, u32[]{:S(2)}, u32[]{:S(2)}) collective-permute-start(bf16[256,128]{1,0:T(8,128)(2,1)S(1)} %shard_map.161.x0_ref), channel_id=1, source_target_pairs={{8,0},{9,1},{10,2},{11,3},{12,4},{13,5},{14,6},{15,7},{0,8},{1,9},... | collective-permute-start | bytes 196616 | tf_op jit(solution)/shard_map/ppermute | solution.py:349

commit v10 on v7

--- a/solution.py
+++ b/solution.py
@@ -16,7 +16,6 @@
 ROWS = SLOTS // 2
 MSG = 144
 WIDTH = 4
-OFFSETS = (0, 1, 3, 2)
 
 epsilon = 1e-06
 f32 = jnp.float32
@@ -157,10 +156,19 @@
     out_ref[...] = nn(jnp.concatenate(rows, axis=0), w_ref[...]).astype(bf16)
 
 
-def attend_body(pos_ref, q_ref, own_ref, other_ref, far_ref, far_other_ref, out_ref):
+def order_body(pos_ref, own_ref, other_ref, out_ref):
+    core = pos_ref[0] % 2
+    own, other = own_ref[...], other_ref[...]
+    rows = own.shape[0]
+    out_ref[0:rows, :] = jnp.where(core == 1, own, other)
+    out_ref[rows:, :] = jnp.where(core == 1, other, own)
+
+
+def attend_body(pos_ref, q_ref, near_ref, far_ref, far_other_ref, out_ref):
     here = pos_ref[0]
     core = here % 2
-    chips = 2 * own_ref.shape[0] // MSG
+    rows = far_ref.shape[0]
+    chips = 2 * rows // MSG
     odd = (here // 2) % 2
     q = q_ref[...]
     wide = (2 * BLOCK, 2 * BLOCK)
@@ -176,11 +184,13 @@
         messages, starts = [], []
         for w in range(WIDTH):
             z = chips - 1 - (k * WIDTH + w)
-            at = pl.ds(pl.multiple_of((z // 2) * MSG, 16), MSG)
+            at = pl.multiple_of((z // 2) * MSG, 16)
             near = odd == (WIDTH - 1 - w) % 2
-            own = jnp.where(near, own_ref[at, :], far_ref[at, :])
-            other = jnp.where(near, other_ref[at, :], far_other_ref[at, :])
-            messages += [jnp.where(core == 1, own, other), jnp.where(core == 1, other, own)]
+            far, other = far_ref[pl.ds(at, MSG), :], far_other_ref[pl.ds(at, MSG), :]
+            upper = jnp.where(core == 1, far, other)
+            lower = jnp.where(core == 1, other, far)
+            messages.append(jnp.where(near, near_ref[pl.ds(at, MSG), :], upper))
+            messages.append(jnp.where(near, near_ref[pl.ds(rows + at, MSG), :], lower))
             starts += [(here - 2 * z - 1) * BLOCK, (here - 2 * z) * BLOCK]
         scores = [nn(q, m[0:HEAD, :]) + m[BLOCK : BLOCK + 1, :].astype(f32) for m in messages]
         causal = [offset < start for start in starts]
@@ -212,7 +222,7 @@
     column = tp_ref[0] % 4
     weights = []
     for k in range(x_ref.shape[0] // HEAD):
-        head = k - k % 4 + (column + OFFSETS[k % 4]) % 4
+        head = k - k % 4 + jnp.bitwise_xor(column, k % 4)
         weights.append(w_ref[pl.ds(pl.multiple_of(head * HEAD, HEAD), HEAD), :])
     x = jnp.transpose(x_ref[...].astype(f32)).astype(bf16)
     out_ref[...] = nn(x, jnp.concatenate(weights, axis=0)).astype(bf16)
@@ -311,14 +321,15 @@
     hidden = exchange(hidden, "tp")
     cores = [(e, e ^ 1) for e in range(ep)]
     own_other = lax.ppermute(own, "ep", cores)
+    ordered = struct((2 * own.shape[0], BLOCK), bf16)
+    near = call(order_body, 1, 2, ordered, 1 << 22)(here.reshape(1), own, own_other)
     far_other = lax.ppermute(far, "ep", cores)
-    attended = call(attend_body, 1, 5, struct((HEAD, BLOCK), bf16), 1 << 30)(
-        here.reshape(1), query, own, own_other, far, far_other
+    attended = call(attend_body, 1, 4, struct((HEAD, BLOCK), bf16), 1 << 30)(
+        here.reshape(1), query, near, far, far_other
     )
     heads = [attended]
-    for d in OFFSETS[1:]:
-        moves = [(k - k % 4 + (k + d) % 4, k) for k in range(tp)]
-        heads.append(lax.ppermute(attended, "tp", moves))
+    for d in range(1, 4):
+        heads.append(lax.ppermute(attended, "tp", [(k ^ d, k) for k in range(tp)]))
     stacked = struct((len(heads) * HEAD, BLOCK), bf16)
     attended = call(pack_body, 0, len(heads), stacked, 1 << 20)(*heads)
     result = call(down_body, 0, 2, slots, 1 << 28)(hidden, down_weight[0])

time: 167 us -> 168 us (level); the launches traced: 167 us -> 165 us
  waiting for transfers between devices: 37.5 us -> 34.7 us
    ppermute x3, waiting for transfers between devices: 4.6 us -> 1.82 us  [shards(): heads.append(lax.ppermute(attended, 'tp', [(k ^ d, k) for k in range(tp)]))]
    pallas_call x10 -> x11, Pallas kernels: 14.3 us -> 14.5 us  [run(): return kernel(*args)]
where the time goes in v10:
time: 168 us; the launch traced here: 165 us
  blocking collectives  70.9 us (42%)
  starting transfers between devices  44 us (26%)
  waiting for transfers between devices  34.7 us (21%)
  Pallas kernels  14.5 us (9%)
    all_to_all x1, blocking collectives, exchange(): return lax.all_to_all(x, axis, split_axis=0, concat_axis=0, tiled=True)  32.5 us
    all_to_all x3, starting transfers between devices, exchange(): return lax.all_to_all(x, axis, split_axis=0, concat_axis=0, tiled=True)  22 us
    all_gather x1, blocking collectives, shards(): lax.all_gather(keys, 'ep', axis=0, tiled=True, axis_index_groups=strided)  20.6 us
    ppermute x1, waiting for transfers between devices, shards(): other_gate = lax.ppermute(gate_weight[0], 'tp', swaps)  19.2 us
    pallas_call x11, Pallas kernels, run(): return kernel(*args)  14.5 us
    all_gather x1, blocking collectives, shards(): lax.all_gather(attended, 'tp', axis=0, tiled=True, axis_index_groups=alon...  12.2 us
    ppermute x3, starting transfers between devices, shards(): heads.append(lax.ppermute(attended, 'tp', [(k ^ d, k) for k in range(tp)]))  10.4 us
    ppermute x1, waiting for transfers between devices, shards(): other_up = lax.ppermute(up_weight[0], 'tp', swaps)  8.97 us
  transfers between devices with their start and end apart: 11, of which 4 were waited for; matrix products, arithmetic and copies ran while one was open for 0% of the time, Pallas kernels for 5%

profile of v10, /device:TPU:6, one launch (start us, length us, event | category | flops | bytes accessed | tf_op | source)
XLA Modules:
  0.0 165.0 jit_solution(3288341382605535364)
XLA Ops:
  0.7 1.5 shard_map.164
  2.2 32.5 %all_to_all.20 = bf16[32,16,128]{2,1,0:T(8,128)(2,1)S(1)} all-to-all(bf16[32,16,128]{2,1,0:T(8,128)(2,1)S(1)} %bitcast.18), channel_id=1, replica_groups=mesh['ep'=32,'tp'=16] {'ep'}, dimensions={0} | all-to-all | bytes 262144 | tf_op jit(solution)/shard_map/all_to_all | solution.py:288
  35.8 7.4 %all-to-all-start.1 = ((bf16[16,256,128]{2,1,0:T(8,128)(2,1)}), bf16[16,256,128]{2,1,0:T(8,128)(2,1)S(1)}, u32[]{:S(2)}, u32[]{:S(2)}) async-start(bf16[16,256,128]{2,1,0:T(8,128)(2,1)} %shard_map.165), calls=%async_computation.1 | async-start | bytes 2097152 | tf_op jit(solution)/shard_map/all_to_all | solution.py:288
  43.2 2.8 %collective-permute-start.6 = (bf16[2048,128]{1,0:T(8,128)(2,1)S(1)}, bf16[2048,128]{1,0:T(8,128)(2,1)S(1)}, u32[]{:S(2)}, u32[]{:S(2)}) collective-permute-start(bf16[2048,128]{1,0:T(8,128)(2,1)S(1)} %bitcast.20), channel_id=1, source_target_pairs={{0,1},{1,0},{2,3},{3,2},{4,5},{5,4},{6,7},{7,6},{8,9},{9,8},{10,11... | collective-permute-start | bytes 1572872 | tf_op jit(solution)/shard_map/ppermute | solution.py:310
  46.0 3.1 %collective-permute-start.7 = (bf16[2048,128]{1,0:T(8,128)(2,1)S(1)}, bf16[2048,128]{1,0:T(8,128)(2,1)S(1)}, u32[]{:S(2)}, u32[]{:S(2)}) collective-permute-start(bf16[2048,128]{1,0:T(8,128)(2,1)S(1)} %bitcast.22), channel_id=1, source_target_pairs={{0,1},{1,0},{2,3},{3,2},{4,5},{5,4},{6,7},{7,6},{8,9},{9,8},{10,11... | collective-permute-start | bytes 1572872 | tf_op jit(solution)/shard_map/ppermute | solution.py:311
  49.1 19.2 %collective-permute-done.6.g1_ref = bf16[2048,128]{1,0:T(8,128)(2,1)S(1)} collective-permute-done((bf16[2048,128]{1,0:T(8,128)(2,1)S(1)}, bf16[2048,128]{1,0:T(8,128)(2,1)S(1)}, u32[]{:S(2)}, u32[]{:S(2)}) %collective-permute-start.6) | collective-permute-done | bytes 524320 | tf_op jit(solution)/shard_map/ppermute | solution.py:310
  68.3 9.0 %collective-permute-done.7.u1_ref = bf16[2048,128]{1,0:T(8,128)(2,1)S(1)} collective-permute-done((bf16[2048,128]{1,0:T(8,128)(2,1)S(1)}, bf16[2048,128]{1,0:T(8,128)(2,1)S(1)}, u32[]{:S(2)}, u32[]{:S(2)}) %collective-permute-start.7) | collective-permute-done | bytes 524320 | tf_op jit(solution)/shard_map/ppermute | solution.py:311
  77.3 2.2 %shard_map.166 = bf16[16,512,128]{2,1,0:T(8,128)(2,1)} custom-call(s32[1]{0:T(128)} %bitcast.tp_ref, bf16[16,256,128]{2,1,0:T(8,128)(2,1)S(1)} %all-to-all-done.1.x_ref, bf16[2048,128]{1,0:T(8,128)(2,1)S(1)} %bitcast.21, bf16[2048,128]{1,0:T(8,128)(2,1)S(1)} %bitcast.23, bf16[2048,128]{1,0:T(8,128)(2,1)S(1)} %collective-permute-done.6.g1_ref, ...), custom_call_target="tpu_custom_call" | custom-call | flops 536870912 | bytes 1048576 | tf_op jit(solution)/shard_map/pallas_call | solution.py:34
  79.5 7.7 %all-to-all-start.2 = ((bf16[16,512,128]{2,1,0:T(8,128)(2,1)}), bf16[16,512,128]{2,1,0:T(8,128)(2,1)S(1)}, u32[]{:S(2)}, u32[]{:S(2)}) async-start(bf16[16,512,128]{2,1,0:T(8,128)(2,1)} %shard_map.166), calls=%async_computation.2 | async-start | bytes 4194304 | tf_op jit(solution)/shard_map/all_to_all | solution.py:288
  87.1 1.9 %shard_map.158 = (bf16[128,64]{1,0:T(8,128)(2,1)S(1)}, bf16[144,128]{1,0:T(8,128)(2,1)S(1)}) custom-call(bf16[128,2048]{1,0:T(8,128)(2,1)} %rows_ref.2, f32[1,2048]{1,0:T(1,128)} %bitcast.33, bf16[64,2048]{1,0:T(8,128)(2,1)} %bitcast.29, bf16[64,2048]{1,0:T(8,128)(2,1)} %bitcast.30, bf16[64,2048]{1,0:T(8,128)(2,1)} %bitcast.31, bf16[1,128]{1,0:T(2,128)(2,1)} %bias_ref.1), custom_call_target="tpu_custom_call" | custom-call | flops 268435456 | bytes 1048576 | tf_op jit(solution)/shard_map/pallas_call | solution.py:34
  89.0 5.6 %all_gather.9 = bf16[288,128]{1,0:T(8,128)(2,1)S(1)} all-gather(bf16[144,128]{1,0:T(8,128)(2,1)S(1)} %get-tuple-element.7), channel_id=1, replica_groups={{0,64},{16,80},{32,96},{48,112},{128,192},{144,208},{160,224},{176,240}..., dimensions={0}, use_global_device_ids=true | all-gather | bytes 110592 | tf_op jit(solution)/shard_map/all_gather | solution.py:312
  94.6 20.6 %all_gather.10.own_ref = bf16[1152,128]{1,0:T(8,128)(2,1)S(1)} all-gather(bf16[288,128]{1,0:T(8,128)(2,1)S(1)} %all_gather.9), channel_id=1, replica_groups={{0,128,256,384},{16,144,272,400},{32,160,288,416},{48,176,304,432},{64,..., dimensions={0}, use_global_device_ids=true | all-gather | bytes 368640 | tf_op jit(solution)/shard_map/all_gather | solution.py:313
  115.2 2.0 %collective-permute-start.1 = (bf16[1152,128]{1,0:T(8,128)(2,1)S(1)}, bf16[1152,128]{1,0:T(8,128)(2,1)S(1)}, u32[]{:S(2)}, u32[]{:S(2)}) collective-permute-start(bf16[1152,128]{1,0:T(8,128)(2,1)S(1)} %all_gather.10.own_ref), channel_id=1, source_target_pairs={{0,32},{16,48},{32,0},{48,16},{64,96},{80,112},{96,64},{112,80},{1... | collective-permute-start | bytes 884744 | tf_op jit(solution)/shard_map/ppermute | solution.py:314
  117.2 1.9 %collective-permute-start = (bf16[1152,128]{1,0:T(8,128)(2,1)S(1)}, bf16[1152,128]{1,0:T(8,128)(2,1)S(1)}, u32[]{:S(2)}, u32[]{:S(2)}) collective-permute-start(bf16[1152,128]{1,0:T(8,128)(2,1)S(1)} %all_gather.10.own_ref), channel_id=1, source_target_pairs={{0,16},{16,0},{32,48},{48,32},{64,80},{80,64},{96,112},{112,96},{1... | collective-permute-start | bytes 884744 | tf_op jit(solution)/shard_map/ppermute | solution.py:323
  119.1 4.7 %collective-permute-done.1.far_ref = bf16[1152,128]{1,0:T(8,128)(2,1)S(1)} collective-permute-done((bf16[1152,128]{1,0:T(8,128)(2,1)S(1)}, bf16[1152,128]{1,0:T(8,128)(2,1)S(1)}, u32[]{:S(2)}, u32[]{:S(2)}) %collective-permute-start.1) | collective-permute-done | bytes 294944 | tf_op jit(solution)/shard_map/ppermute | solution.py:314
  123.8 1.9 %collective-permute-start.2 = (bf16[1152,128]{1,0:T(8,128)(2,1)S(1)}, bf16[1152,128]{1,0:T(8,128)(2,1)}, u32[]{:S(2)}, u32[]{:S(2)}) collective-permute-start(bf16[1152,128]{1,0:T(8,128)(2,1)S(1)} %collective-permute-done.1.far_ref), channel_id=1, source_target_pairs={{0,16},{16,0},{32,48},{48,32},{64,80},{80,64},{96,112},{112,96},{1... | collective-permute-start | bytes 884744 | tf_op jit(solution)/shard_map/ppermute | solution.py:326
  125.7 1.4 shard_map.167
  127.1 6.9 %all-to-all-start.3 = ((bf16[32,16,128]{2,1,0:T(8,128)(2,1)}), bf16[32,16,128]{2,1,0:T(8,128)(2,1)S(1)}, u32[]{:S(2)}, u32[]{:S(2)}) async-start(bf16[32,16,128]{2,1,0:T(8,128)(2,1)} %bitcast.15), calls=%async_computation.3 | async-start | bytes 262144 | tf_op jit(solution)/shard_map/all_to_all | solution.py:288
  134.1 4.2 %shard_map.160.refs_0_ = bf16[64,128]{1,0:T(8,128)(2,1)S(1)} custom-call(s32[1]{0:T(128)} %bitcast.1.pos_ref, bf16[128,64]{1,0:T(8,128)(2,1)S(1)} %get-tuple-element.6.q_ref, bf16[2304,128]{1,0:T(8,128)(2,1)S(1)} %shard_map.159.near_ref, bf16[1152,128]{1,0:T(8,128)(2,1)S(1)} %collective-permute-done.1.far_ref, ...), custom_call_target="tpu_custom_call" | custom-call | flops 1073741824 | bytes 1048576 | tf_op jit(solution)/shard_map/pallas_call | solution.py:34
  138.3 2.3 %collective-permute-start.3 = (bf16[64,128]{1,0:T(8,128)(2,1)S(1)}, bf16[64,128]{1,0:T(8,128)(2,1)S(1)}, u32[]{:S(2)}, u32[]{:S(2)}) collective-permute-start(bf16[64,128]{1,0:T(8,128)(2,1)S(1)} %shard_map.160.refs_0_), channel_id=1, source_target_pairs={{1,0},{0,1},{3,2},{2,3},{5,4},{4,5},{7,6},{6,7},{9,8},{8,9},{11,10... | collective-permute-start | bytes 49160 | tf_op jit(solution)/shard_map/ppermute | solution.py:332
  140.6 3.5 %collective-permute-start.4 = (bf16[64,128]{1,0:T(8,128)(2,1)S(1)}, bf16[64,128]{1,0:T(8,128)(2,1)S(1)}, u32[]{:S(2)}, u32[]{:S(2)}) collective-permute-start(bf16[64,128]{1,0:T(8,128)(2,1)S(1)} %shard_map.160.refs_0_), channel_id=1, source_target_pairs={{2,0},{3,1},{0,2},{1,3},{6,4},{7,5},{4,6},{5,7},{10,8},{11,9},{8,1... | collective-permute-start | bytes 49160 | tf_op jit(solution)/shard_map/ppermute | solution.py:332
  144.2 4.6 %collective-permute-start.5 = (bf16[64,128]{1,0:T(8,128)(2,1)S(1)}, bf16[64,128]{1,0:T(8,128)(2,1)S(1)}, u32[]{:S(2)}, u32[]{:S(2)}) collective-permute-start(bf16[64,128]{1,0:T(8,128)(2,1)S(1)} %shard_map.160.refs_0_), channel_id=1, source_target_pairs={{3,0},{2,1},{1,2},{0,3},{7,4},{6,5},{5,6},{4,7},{11,8},{10,9},{9,1... | collective-permute-start | bytes 49160 | tf_op jit(solution)/shard_map/ppermute | solution.py:332
  149.2 1.8 %collective-permute-done.5.refs_3_ = bf16[64,128]{1,0:T(8,128)(2,1)S(1)} collective-permute-done((bf16[64,128]{1,0:T(8,128)(2,1)S(1)}, bf16[64,128]{1,0:T(8,128)(2,1)S(1)}, u32[]{:S(2)}, u32[]{:S(2)}) %collective-permute-start.5) | collective-permute-done | bytes 16416 | tf_op jit(solution)/shard_map/ppermute | solution.py:332
  151.0 12.2 %all_gather.11.x_ref = bf16[1024,128]{1,0:T(8,128)(2,1)S(1)} all-gather(bf16[256,128]{1,0:T(8,128)(2,1)S(1)} %shard_map.161), channel_id=1, replica_groups={{0,4,8,12},{1,5,9,13},{2,6,10,14},{3,7,11,15},{16,20,24,28},{17,21,25,2..., dimensions={0}, use_global_device_ids=true | all-gather | bytes 327680 | tf_op jit(solution)/shard_map/all_gather | solution.py:339
  (27 shorter events, 3.4 us)
Async XLA Ops:
  0.6 42.6 %copy-start.1 = (bf16[1,2048,128]{2,1,0:T(8,128)(2,1)S(1)}, bf16[1,2048,128]{2,1,0:T(8,128)(2,1)}, u32[]{:S(2)}) copy-start(bf16[1,2048,128]{2,1,0:T(8,128)(2,1)} %param.27) | copy-start | bytes 1572868
  0.6 45.4 %copy-start.2 = (bf16[1,2048,128]{2,1,0:T(8,128)(2,1)S(1)}, bf16[1,2048,128]{2,1,0:T(8,128)(2,1)}, u32[]{:S(2)}) copy-start(bf16[1,2048,128]{2,1,0:T(8,128)(2,1)} %param.28) | copy-start | bytes 1572868
  35.8 41.5 %all-to-all-start.1 = ((bf16[16,256,128]{2,1,0:T(8,128)(2,1)}), bf16[16,256,128]{2,1,0:T(8,128)(2,1)S(1)}, u32[]{:S(2)}, u32[]{:S(2)}) async-start(bf16[16,256,128]{2,1,0:T(8,128)(2,1)} %shard_map.165), calls=%async_computation.1 | async-start | bytes 2097152 | tf_op jit(solution)/shard_map/all_to_all | solution.py:288
  43.2 25.1 %collective-permute-start.6 = (bf16[2048,128]{1,0:T(8,128)(2,1)S(1)}, bf16[2048,128]{1,0:T(8,128)(2,1)S(1)}, u32[]{:S(2)}, u32[]{:S(2)}) collective-permute-start(bf16[2048,128]{1,0:T(8,128)(2,1)S(1)} %bitcast.20), channel_id=1, source_target_pairs={{0,1},{1,0},{2,3},{3,2},{4,5},{5,4},{6,7},{7,6},{8,9},{9,8},{10,11... | collective-permute-start | bytes 1572872 | tf_op jit(solution)/shard_map/ppermute | solution.py:310
  46.0 31.2 %collective-permute-start.7 = (bf16[2048,128]{1,0:T(8,128)(2,1)S(1)}, bf16[2048,128]{1,0:T(8,128)(2,1)S(1)}, u32[]{:S(2)}, u32[]{:S(2)}) collective-permute-start(bf16[2048,128]{1,0:T(8,128)(2,1)S(1)} %bitcast.22), channel_id=1, source_target_pairs={{0,1},{1,0},{2,3},{3,2},{4,5},{5,4},{6,7},{7,6},{8,9},{9,8},{10,11... | collective-permute-start | bytes 1572872 | tf_op jit(solution)/shard_map/ppermute | solution.py:311
  79.4 46.3 %copy-start = (bf16[1,2048,128]{2,1,0:T(8,128)(2,1)S(1)}, bf16[1,2048,128]{2,1,0:T(8,128)(2,1)}, u32[]{:S(2)}) copy-start(bf16[1,2048,128]{2,1,0:T(8,128)(2,1)} %param.29) | copy-start | bytes 1572868
  79.5 46.2 %all-to-all-start.2 = ((bf16[16,512,128]{2,1,0:T(8,128)(2,1)}), bf16[16,512,128]{2,1,0:T(8,128)(2,1)S(1)}, u32[]{:S(2)}, u32[]{:S(2)}) async-start(bf16[16,512,128]{2,1,0:T(8,128)(2,1)} %shard_map.166), calls=%async_computation.2 | async-start | bytes 4194304 | tf_op jit(solution)/shard_map/all_to_all | solution.py:288
  115.2 8.6 %collective-permute-start.1 = (bf16[1152,128]{1,0:T(8,128)(2,1)S(1)}, bf16[1152,128]{1,0:T(8,128)(2,1)S(1)}, u32[]{:S(2)}, u32[]{:S(2)}) collective-permute-start(bf16[1152,128]{1,0:T(8,128)(2,1)S(1)} %all_gather.10.own_ref), channel_id=1, source_target_pairs={{0,32},{16,48},{32,0},{48,16},{64,96},{80,112},{96,64},{112,80},{1... | collective-permute-start | bytes 884744 | tf_op jit(solution)/shard_map/ppermute | solution.py:314
  117.2 16.8 %collective-permute-start = (bf16[1152,128]{1,0:T(8,128)(2,1)S(1)}, bf16[1152,128]{1,0:T(8,128)(2,1)S(1)}, u32[]{:S(2)}, u32[]{:S(2)}) collective-permute-start(bf16[1152,128]{1,0:T(8,128)(2,1)S(1)} %all_gather.10.own_ref), channel_id=1, source_target_pairs={{0,16},{16,0},{32,48},{48,32},{64,80},{80,64},{96,112},{112,96},{1... | collective-permute-start | bytes 884744 | tf_op jit(solution)/shard_map/ppermute | solution.py:323
  123.8 10.3 %collective-permute-start.2 = (bf16[1152,128]{1,0:T(8,128)(2,1)S(1)}, bf16[1152,128]{1,0:T(8,128)(2,1)}, u32[]{:S(2)}, u32[]{:S(2)}) collective-permute-start(bf16[1152,128]{1,0:T(8,128)(2,1)S(1)} %collective-permute-done.1.far_ref), channel_id=1, source_target_pairs={{0,16},{16,0},{32,48},{48,32},{64,80},{80,64},{96,112},{112,96},{1... | collective-permute-start | bytes 884744 | tf_op jit(solution)/shard_map/ppermute | solution.py:326
  127.1 37.1 %all-to-all-start.3 = ((bf16[32,16,128]{2,1,0:T(8,128)(2,1)}), bf16[32,16,128]{2,1,0:T(8,128)(2,1)S(1)}, u32[]{:S(2)}, u32[]{:S(2)}) async-start(bf16[32,16,128]{2,1,0:T(8,128)(2,1)} %bitcast.15), calls=%async_computation.3 | async-start | bytes 262144 | tf_op jit(solution)/shard_map/all_to_all | solution.py:288
  134.1 14.7 %copy-start.4 = (s32[128,2]{0,1:T(2,128)S(1)}, s32[128,2]{0,1:T(2,128)}, u32[]{:S(2)}) copy-start(s32[128,2]{0,1:T(2,128)} %param.24) | copy-start | bytes 3076
  134.1 14.7 %copy-start.5 = (f32[128,4]{0,1:T(4,128)S(1)}, f32[128,4]{0,1:T(4,128)}, u32[]{:S(2)}) copy-start(f32[128,4]{0,1:T(4,128)} %param.25) | copy-start | bytes 6148
  134.1 14.7 %copy-start.6 = (f32[128,2]{0,1:T(2,128)S(1)}, f32[128,2]{0,1:T(2,128)}, u32[]{:S(2)}) copy-start(f32[128,2]{0,1:T(2,128)} %param.26) | copy-start | bytes 3076
  134.1 29.2 %copy-start.3 = (bf16[1024,128]{1,0:T(8,128)(2,1)S(1)}, bf16[1024,128]{1,0:T(8,128)(2,1)}, u32[]{:S(2)}) copy-start(bf16[1024,128]{1,0:T(8,128)(2,1)} %w_ref.1) | copy-start | bytes 786436
  138.3 10.8 %collective-permute-start.3 = (bf16[64,128]{1,0:T(8,128)(2,1)S(1)}, bf16[64,128]{1,0:T(8,128)(2,1)S(1)}, u32[]{:S(2)}, u32[]{:S(2)}) collective-permute-start(bf16[64,128]{1,0:T(8,128)(2,1)S(1)} %shard_map.160.refs_0_), channel_id=1, source_target_pairs={{1,0},{0,1},{3,2},{2,3},{5,4},{4,5},{7,6},{6,7},{9,8},{8,9},{11,10... | collective-permute-start | bytes 49160 | tf_op jit(solution)/shard_map/ppermute | solution.py:332
  140.6 8.6 %collective-permute-start.4 = (bf16[64,128]{1,0:T(8,128)(2,1)S(1)}, bf16[64,128]{1,0:T(8,128)(2,1)S(1)}, u32[]{:S(2)}, u32[]{:S(2)}) collective-permute-start(bf16[64,128]{1,0:T(8,128)(2,1)S(1)} %shard_map.160.refs_0_), channel_id=1, source_target_pairs={{2,0},{3,1},{0,2},{1,3},{6,4},{7,5},{4,6},{5,7},{10,8},{11,9},{8,1... | collective-permute-start | bytes 49160 | tf_op jit(solution)/shard_map/ppermute | solution.py:332
  144.2 6.8 %collective-permute-start.5 = (bf16[64,128]{1,0:T(8,128)(2,1)S(1)}, bf16[64,128]{1,0:T(8,128)(2,1)S(1)}, u32[]{:S(2)}, u32[]{:S(2)}) collective-permute-start(bf16[64,128]{1,0:T(8,128)(2,1)S(1)} %shard_map.160.refs_0_), channel_id=1, source_target_pairs={{3,0},{2,1},{1,2},{0,3},{7,4},{6,5},{5,6},{4,7},{11,8},{10,9},{9,1... | collective-permute-start | bytes 49160 | tf_op jit(solution)/shard_map/ppermute | solution.py:332

commit v11 on v10

--- a/solution.py
+++ b/solution.py
@@ -327,9 +327,8 @@
     attended = call(attend_body, 1, 4, struct((HEAD, BLOCK), bf16), 1 << 30)(
         here.reshape(1), query, near, far, far_other
     )
-    heads = [attended]
-    for d in range(1, 4):
-        heads.append(lax.ppermute(attended, "tp", [(k ^ d, k) for k in range(tp)]))
+    far_heads = [lax.ppermute(attended, "tp", [(k ^ d, k) for k in range(tp)]) for d in range(2, 4)]
+    heads = [attended, lax.ppermute(attended, "tp", [(k ^ 1, k) for k in range(tp)]), *far_heads]
     stacked = struct((len(heads) * HEAD, BLOCK), bf16)
     attended = call(pack_body, 0, len(heads), stacked, 1 << 20)(*heads)
     result = call(down_body, 0, 2, slots, 1 << 28)(hidden, down_weight[0])

time: 168 us -> 168 us (level)
  no operation moved by 1% of the time
where the time goes in v11:
time: 168 us; the launch traced here: 165 us
  blocking collectives  70.9 us (42%)
  starting transfers between devices  44 us (26%)
  waiting for transfers between devices  34.7 us (21%)
  Pallas kernels  14.5 us (9%)
    all_to_all x1, blocking collectives, exchange(): return lax.all_to_all(x, axis, split_axis=0, concat_axis=0, tiled=True)  32.5 us
    all_to_all x3, starting transfers between devices, exchange(): return lax.all_to_all(x, axis, split_axis=0, concat_axis=0, tiled=True)  22 us
    all_gather x1, blocking collectives, shards(): lax.all_gather(keys, 'ep', axis=0, tiled=True, axis_index_groups=strided)  20.6 us
    ppermute x1, waiting for transfers between devices, shards(): other_gate = lax.ppermute(gate_weight[0], 'tp', swaps)  19.2 us
    pallas_call x11, Pallas kernels, run(): return kernel(*args)  14.5 us
    all_gather x1, blocking collectives, shards(): lax.all_gather(attended, 'tp', axis=0, tiled=True, axis_index_groups=alon...  12.2 us
    ppermute x1, waiting for transfers between devices, shards(): other_up = lax.ppermute(up_weight[0], 'tp', swaps)  8.97 us
    ppermute x2, starting transfers between devices, shards(): lax.ppermute(attended, 'tp', [(k ^ d, k) for k in range(tp)])  8.15 us
  transfers between devices with their start and end apart: 11, of which 4 were waited for; matrix products, arithmetic and copies ran while one was open for 0% of the time, Pallas kernels for 5%

profile of v11, /device:TPU:6, one launch (start us, length us, event | category | flops | bytes accessed | tf_op | source)
XLA Modules:
  0.0 165.0 jit_solution(3288341382605535364)
XLA Ops:
  0.7 1.5 shard_map.164
  2.2 32.5 %all_to_all.20 = bf16[32,16,128]{2,1,0:T(8,128)(2,1)S(1)} all-to-all(bf16[32,16,128]{2,1,0:T(8,128)(2,1)S(1)} %bitcast.18), channel_id=1, replica_groups=mesh['ep'=32,'tp'=16] {'ep'}, dimensions={0} | all-to-all | bytes 262144 | tf_op jit(solution)/shard_map/all_to_all | solution.py:288
  35.8 7.4 %all-to-all-start.1 = ((bf16[16,256,128]{2,1,0:T(8,128)(2,1)}), bf16[16,256,128]{2,1,0:T(8,128)(2,1)S(1)}, u32[]{:S(2)}, u32[]{:S(2)}) async-start(bf16[16,256,128]{2,1,0:T(8,128)(2,1)} %shard_map.165), calls=%async_computation.1 | async-start | bytes 2097152 | tf_op jit(solution)/shard_map/all_to_all | solution.py:288
  43.2 2.8 %collective-permute-start.6 = (bf16[2048,128]{1,0:T(8,128)(2,1)S(1)}, bf16[2048,128]{1,0:T(8,128)(2,1)S(1)}, u32[]{:S(2)}, u32[]{:S(2)}) collective-permute-start(bf16[2048,128]{1,0:T(8,128)(2,1)S(1)} %bitcast.20), channel_id=1, source_target_pairs={{0,1},{1,0},{2,3},{3,2},{4,5},{5,4},{6,7},{7,6},{8,9},{9,8},{10,11... | collective-permute-start | bytes 1572872 | tf_op jit(solution)/shard_map/ppermute | solution.py:310
  46.0 3.1 %collective-permute-start.7 = (bf16[2048,128]{1,0:T(8,128)(2,1)S(1)}, bf16[2048,128]{1,0:T(8,128)(2,1)S(1)}, u32[]{:S(2)}, u32[]{:S(2)}) collective-permute-start(bf16[2048,128]{1,0:T(8,128)(2,1)S(1)} %bitcast.22), channel_id=1, source_target_pairs={{0,1},{1,0},{2,3},{3,2},{4,5},{5,4},{6,7},{7,6},{8,9},{9,8},{10,11... | collective-permute-start | bytes 1572872 | tf_op jit(solution)/shard_map/ppermute | solution.py:311
  49.1 19.2 %collective-permute-done.6.g1_ref = bf16[2048,128]{1,0:T(8,128)(2,1)S(1)} collective-permute-done((bf16[2048,128]{1,0:T(8,128)(2,1)S(1)}, bf16[2048,128]{1,0:T(8,128)(2,1)S(1)}, u32[]{:S(2)}, u32[]{:S(2)}) %collective-permute-start.6) | collective-permute-done | bytes 524320 | tf_op jit(solution)/shard_map/ppermute | solution.py:310
  68.3 9.0 %collective-permute-done.7.u1_ref = bf16[2048,128]{1,0:T(8,128)(2,1)S(1)} collective-permute-done((bf16[2048,128]{1,0:T(8,128)(2,1)S(1)}, bf16[2048,128]{1,0:T(8,128)(2,1)S(1)}, u32[]{:S(2)}, u32[]{:S(2)}) %collective-permute-start.7) | collective-permute-done | bytes 524320 | tf_op jit(solution)/shard_map/ppermute | solution.py:311
  77.3 2.2 %shard_map.166 = bf16[16,512,128]{2,1,0:T(8,128)(2,1)} custom-call(s32[1]{0:T(128)} %bitcast.tp_ref, bf16[16,256,128]{2,1,0:T(8,128)(2,1)S(1)} %all-to-all-done.1.x_ref, bf16[2048,128]{1,0:T(8,128)(2,1)S(1)} %bitcast.21, bf16[2048,128]{1,0:T(8,128)(2,1)S(1)} %bitcast.23, bf16[2048,128]{1,0:T(8,128)(2,1)S(1)} %collective-permute-done.6.g1_ref, ...), custom_call_target="tpu_custom_call" | custom-call | flops 536870912 | bytes 1048576 | tf_op jit(solution)/shard_map/pallas_call | solution.py:34
  79.5 7.7 %all-to-all-start.2 = ((bf16[16,512,128]{2,1,0:T(8,128)(2,1)}), bf16[16,512,128]{2,1,0:T(8,128)(2,1)S(1)}, u32[]{:S(2)}, u32[]{:S(2)}) async-start(bf16[16,512,128]{2,1,0:T(8,128)(2,1)} %shard_map.166), calls=%async_computation.2 | async-start | bytes 4194304 | tf_op jit(solution)/shard_map/all_to_all | solution.py:288
  87.1 1.9 %shard_map.158 = (bf16[128,64]{1,0:T(8,128)(2,1)S(1)}, bf16[144,128]{1,0:T(8,128)(2,1)S(1)}) custom-call(bf16[128,2048]{1,0:T(8,128)(2,1)} %rows_ref.2, f32[1,2048]{1,0:T(1,128)} %bitcast.33, bf16[64,2048]{1,0:T(8,128)(2,1)} %bitcast.29, bf16[64,2048]{1,0:T(8,128)(2,1)} %bitcast.30, bf16[64,2048]{1,0:T(8,128)(2,1)} %bitcast.31, bf16[1,128]{1,0:T(2,128)(2,1)} %bias_ref.1), custom_call_target="tpu_custom_call" | custom-call | flops 268435456 | bytes 1048576 | tf_op jit(solution)/shard_map/pallas_call | solution.py:34
  89.0 5.6 %all_gather.9 = bf16[288,128]{1,0:T(8,128)(2,1)S(1)} all-gather(bf16[144,128]{1,0:T(8,128)(2,1)S(1)} %get-tuple-element.7), channel_id=1, replica_groups={{0,64},{16,80},{32,96},{48,112},{128,192},{144,208},{160,224},{176,240}..., dimensions={0}, use_global_device_ids=true | all-gather | bytes 110592 | tf_op jit(solution)/shard_map/all_gather | solution.py:312
  94.6 20.6 %all_gather.10.own_ref = bf16[1152,128]{1,0:T(8,128)(2,1)S(1)} all-gather(bf16[288,128]{1,0:T(8,128)(2,1)S(1)} %all_gather.9), channel_id=1, replica_groups={{0,128,256,384},{16,144,272,400},{32,160,288,416},{48,176,304,432},{64,..., dimensions={0}, use_global_device_ids=true | all-gather | bytes 368640 | tf_op jit(solution)/shard_map/all_gather | solution.py:313
  115.2 2.0 %collective-permute-start.1 = (bf16[1152,128]{1,0:T(8,128)(2,1)S(1)}, bf16[1152,128]{1,0:T(8,128)(2,1)S(1)}, u32[]{:S(2)}, u32[]{:S(2)}) collective-permute-start(bf16[1152,128]{1,0:T(8,128)(2,1)S(1)} %all_gather.10.own_ref), channel_id=1, source_target_pairs={{0,32},{16,48},{32,0},{48,16},{64,96},{80,112},{96,64},{112,80},{1... | collective-permute-start | bytes 884744 | tf_op jit(solution)/shard_map/ppermute | solution.py:314
  117.2 1.9 %collective-permute-start = (bf16[1152,128]{1,0:T(8,128)(2,1)S(1)}, bf16[1152,128]{1,0:T(8,128)(2,1)S(1)}, u32[]{:S(2)}, u32[]{:S(2)}) collective-permute-start(bf16[1152,128]{1,0:T(8,128)(2,1)S(1)} %all_gather.10.own_ref), channel_id=1, source_target_pairs={{0,16},{16,0},{32,48},{48,32},{64,80},{80,64},{96,112},{112,96},{1... | collective-permute-start | bytes 884744 | tf_op jit(solution)/shard_map/ppermute | solution.py:323
  119.1 4.7 %collective-permute-done.1.far_ref = bf16[1152,128]{1,0:T(8,128)(2,1)S(1)} collective-permute-done((bf16[1152,128]{1,0:T(8,128)(2,1)S(1)}, bf16[1152,128]{1,0:T(8,128)(2,1)S(1)}, u32[]{:S(2)}, u32[]{:S(2)}) %collective-permute-start.1) | collective-permute-done | bytes 294944 | tf_op jit(solution)/shard_map/ppermute | solution.py:314
  123.8 1.9 %collective-permute-start.2 = (bf16[1152,128]{1,0:T(8,128)(2,1)S(1)}, bf16[1152,128]{1,0:T(8,128)(2,1)}, u32[]{:S(2)}, u32[]{:S(2)}) collective-permute-start(bf16[1152,128]{1,0:T(8,128)(2,1)S(1)} %collective-permute-done.1.far_ref), channel_id=1, source_target_pairs={{0,16},{16,0},{32,48},{48,32},{64,80},{80,64},{96,112},{112,96},{1... | collective-permute-start | bytes 884744 | tf_op jit(solution)/shard_map/ppermute | solution.py:326
  125.7 1.4 shard_map.167
  127.1 6.9 %all-to-all-start.3 = ((bf16[32,16,128]{2,1,0:T(8,128)(2,1)}), bf16[32,16,128]{2,1,0:T(8,128)(2,1)S(1)}, u32[]{:S(2)}, u32[]{:S(2)}) async-start(bf16[32,16,128]{2,1,0:T(8,128)(2,1)} %bitcast.15), calls=%async_computation.3 | async-start | bytes 262144 | tf_op jit(solution)/shard_map/all_to_all | solution.py:288
  134.1 4.2 %shard_map.160.refs_0_ = bf16[64,128]{1,0:T(8,128)(2,1)S(1)} custom-call(s32[1]{0:T(128)} %bitcast.1.pos_ref, bf16[128,64]{1,0:T(8,128)(2,1)S(1)} %get-tuple-element.6.q_ref, bf16[2304,128]{1,0:T(8,128)(2,1)S(1)} %shard_map.159.near_ref, bf16[1152,128]{1,0:T(8,128)(2,1)S(1)} %collective-permute-done.1.far_ref, ...), custom_call_target="tpu_custom_call" | custom-call | flops 1073741824 | bytes 1048576 | tf_op jit(solution)/shard_map/pallas_call | solution.py:34
  138.3 2.3 %collective-permute-start.3 = (bf16[64,128]{1,0:T(8,128)(2,1)S(1)}, bf16[64,128]{1,0:T(8,128)(2,1)S(1)}, u32[]{:S(2)}, u32[]{:S(2)}) collective-permute-start(bf16[64,128]{1,0:T(8,128)(2,1)S(1)} %shard_map.160.refs_0_), channel_id=1, source_target_pairs={{1,0},{0,1},{3,2},{2,3},{5,4},{4,5},{7,6},{6,7},{9,8},{8,9},{11,10... | collective-permute-start | bytes 49160 | tf_op jit(solution)/shard_map/ppermute | solution.py:331
  140.6 3.5 %collective-permute-start.4 = (bf16[64,128]{1,0:T(8,128)(2,1)S(1)}, bf16[64,128]{1,0:T(8,128)(2,1)S(1)}, u32[]{:S(2)}, u32[]{:S(2)}) collective-permute-start(bf16[64,128]{1,0:T(8,128)(2,1)S(1)} %shard_map.160.refs_0_), channel_id=1, source_target_pairs={{2,0},{3,1},{0,2},{1,3},{6,4},{7,5},{4,6},{5,7},{10,8},{11,9},{8,1... | collective-permute-start | bytes 49160 | tf_op jit(solution)/shard_map/ppermute | solution.py:330
  144.2 4.6 %collective-permute-start.5 = (bf16[64,128]{1,0:T(8,128)(2,1)S(1)}, bf16[64,128]{1,0:T(8,128)(2,1)S(1)}, u32[]{:S(2)}, u32[]{:S(2)}) collective-permute-start(bf16[64,128]{1,0:T(8,128)(2,1)S(1)} %shard_map.160.refs_0_), channel_id=1, source_target_pairs={{3,0},{2,1},{1,2},{0,3},{7,4},{6,5},{5,6},{4,7},{11,8},{10,9},{9,1... | collective-permute-start | bytes 49160 | tf_op jit(solution)/shard_map/ppermute | solution.py:330
  149.2 1.8 %collective-permute-done.5.refs_3_ = bf16[64,128]{1,0:T(8,128)(2,1)S(1)} collective-permute-done((bf16[64,128]{1,0:T(8,128)(2,1)S(1)}, bf16[64,128]{1,0:T(8,128)(2,1)S(1)}, u32[]{:S(2)}, u32[]{:S(2)}) %collective-permute-start.5) | collective-permute-done | bytes 16416 | tf_op jit(solution)/shard_map/ppermute | solution.py:330
  151.0 12.2 %all_gather.11.x_ref = bf16[1024,128]{1,0:T(8,128)(2,1)S(1)} all-gather(bf16[256,128]{1,0:T(8,128)(2,1)S(1)} %shard_map.161), channel_id=1, replica_groups={{0,4,8,12},{1,5,9,13},{2,6,10,14},{3,7,11,15},{16,20,24,28},{17,21,25,2..., dimensions={0}, use_global_device_ids=true | all-gather | bytes 327680 | tf_op jit(solution)/shard_map/all_gather | solution.py:338
  (27 shorter events, 3.4 us)
Async XLA Ops:
  0.6 42.6 %copy-start.1 = (bf16[1,2048,128]{2,1,0:T(8,128)(2,1)S(1)}, bf16[1,2048,128]{2,1,0:T(8,128)(2,1)}, u32[]{:S(2)}) copy-start(bf16[1,2048,128]{2,1,0:T(8,128)(2,1)} %param.27) | copy-start | bytes 1572868
  0.6 45.4 %copy-start.2 = (bf16[1,2048,128]{2,1,0:T(8,128)(2,1)S(1)}, bf16[1,2048,128]{2,1,0:T(8,128)(2,1)}, u32[]{:S(2)}) copy-start(bf16[1,2048,128]{2,1,0:T(8,128)(2,1)} %param.28) | copy-start | bytes 1572868
  35.8 41.5 %all-to-all-start.1 = ((bf16[16,256,128]{2,1,0:T(8,128)(2,1)}), bf16[16,256,128]{2,1,0:T(8,128)(2,1)S(1)}, u32[]{:S(2)}, u32[]{:S(2)}) async-start(bf16[16,256,128]{2,1,0:T(8,128)(2,1)} %shard_map.165), calls=%async_computation.1 | async-start | bytes 2097152 | tf_op jit(solution)/shard_map/all_to_all | solution.py:288
  43.2 25.1 %collective-permute-start.6 = (bf16[2048,128]{1,0:T(8,128)(2,1)S(1)}, bf16[2048,128]{1,0:T(8,128)(2,1)S(1)}, u32[]{:S(2)}, u32[]{:S(2)}) collective-permute-start(bf16[2048,128]{1,0:T(8,128)(2,1)S(1)} %bitcast.20), channel_id=1, source_target_pairs={{0,1},{1,0},{2,3},{3,2},{4,5},{5,4},{6,7},{7,6},{8,9},{9,8},{10,11... | collective-permute-start | bytes 1572872 | tf_op jit(solution)/shard_map/ppermute | solution.py:310
  46.0 31.2 %collective-permute-start.7 = (bf16[2048,128]{1,0:T(8,128)(2,1)S(1)}, bf16[2048,128]{1,0:T(8,128)(2,1)S(1)}, u32[]{:S(2)}, u32[]{:S(2)}) collective-permute-start(bf16[2048,128]{1,0:T(8,128)(2,1)S(1)} %bitcast.22), channel_id=1, source_target_pairs={{0,1},{1,0},{2,3},{3,2},{4,5},{5,4},{6,7},{7,6},{8,9},{9,8},{10,11... | collective-permute-start | bytes 1572872 | tf_op jit(solution)/shard_map/ppermute | solution.py:311
  79.4 46.3 %copy-start = (bf16[1,2048,128]{2,1,0:T(8,128)(2,1)S(1)}, bf16[1,2048,128]{2,1,0:T(8,128)(2,1)}, u32[]{:S(2)}) copy-start(bf16[1,2048,128]{2,1,0:T(8,128)(2,1)} %param.29) | copy-start | bytes 1572868
  79.5 46.2 %all-to-all-start.2 = ((bf16[16,512,128]{2,1,0:T(8,128)(2,1)}), bf16[16,512,128]{2,1,0:T(8,128)(2,1)S(1)}, u32[]{:S(2)}, u32[]{:S(2)}) async-start(bf16[16,512,128]{2,1,0:T(8,128)(2,1)} %shard_map.166), calls=%async_computation.2 | async-start | bytes 4194304 | tf_op jit(solution)/shard_map/all_to_all | solution.py:288
  115.2 8.6 %collective-permute-start.1 = (bf16[1152,128]{1,0:T(8,128)(2,1)S(1)}, bf16[1152,128]{1,0:T(8,128)(2,1)S(1)}, u32[]{:S(2)}, u32[]{:S(2)}) collective-permute-start(bf16[1152,128]{1,0:T(8,128)(2,1)S(1)} %all_gather.10.own_ref), channel_id=1, source_target_pairs={{0,32},{16,48},{32,0},{48,16},{64,96},{80,112},{96,64},{112,80},{1... | collective-permute-start | bytes 884744 | tf_op jit(solution)/shard_map/ppermute | solution.py:314
  117.2 16.8 %collective-permute-start = (bf16[1152,128]{1,0:T(8,128)(2,1)S(1)}, bf16[1152,128]{1,0:T(8,128)(2,1)S(1)}, u32[]{:S(2)}, u32[]{:S(2)}) collective-permute-start(bf16[1152,128]{1,0:T(8,128)(2,1)S(1)} %all_gather.10.own_ref), channel_id=1, source_target_pairs={{0,16},{16,0},{32,48},{48,32},{64,80},{80,64},{96,112},{112,96},{1... | collective-permute-start | bytes 884744 | tf_op jit(solution)/shard_map/ppermute | solution.py:323
  123.8 10.3 %collective-permute-start.2 = (bf16[1152,128]{1,0:T(8,128)(2,1)S(1)}, bf16[1152,128]{1,0:T(8,128)(2,1)}, u32[]{:S(2)}, u32[]{:S(2)}) collective-permute-start(bf16[1152,128]{1,0:T(8,128)(2,1)S(1)} %collective-permute-done.1.far_ref), channel_id=1, source_target_pairs={{0,16},{16,0},{32,48},{48,32},{64,80},{80,64},{96,112},{112,96},{1... | collective-permute-start | bytes 884744 | tf_op jit(solution)/shard_map/ppermute | solution.py:326
  127.1 37.1 %all-to-all-start.3 = ((bf16[32,16,128]{2,1,0:T(8,128)(2,1)}), bf16[32,16,128]{2,1,0:T(8,128)(2,1)S(1)}, u32[]{:S(2)}, u32[]{:S(2)}) async-start(bf16[32,16,128]{2,1,0:T(8,128)(2,1)} %bitcast.15), calls=%async_computation.3 | async-start | bytes 262144 | tf_op jit(solution)/shard_map/all_to_all | solution.py:288
  134.1 14.7 %copy-start.4 = (s32[128,2]{0,1:T(2,128)S(1)}, s32[128,2]{0,1:T(2,128)}, u32[]{:S(2)}) copy-start(s32[128,2]{0,1:T(2,128)} %param.24) | copy-start | bytes 3076
  134.1 14.7 %copy-start.5 = (f32[128,4]{0,1:T(4,128)S(1)}, f32[128,4]{0,1:T(4,128)}, u32[]{:S(2)}) copy-start(f32[128,4]{0,1:T(4,128)} %param.25) | copy-start | bytes 6148
  134.1 14.7 %copy-start.6 = (f32[128,2]{0,1:T(2,128)S(1)}, f32[128,2]{0,1:T(2,128)}, u32[]{:S(2)}) copy-start(f32[128,2]{0,1:T(2,128)} %param.26) | copy-start | bytes 3076
  134.1 29.2 %copy-start.3 = (bf16[1024,128]{1,0:T(8,128)(2,1)S(1)}, bf16[1024,128]{1,0:T(8,128)(2,1)}, u32[]{:S(2)}) copy-start(bf16[1024,128]{1,0:T(8,128)(2,1)} %w_ref.1) | copy-start | bytes 786436
  138.3 10.8 %collective-permute-start.3 = (bf16[64,128]{1,0:T(8,128)(2,1)S(1)}, bf16[64,128]{1,0:T(8,128)(2,1)S(1)}, u32[]{:S(2)}, u32[]{:S(2)}) collective-permute-start(bf16[64,128]{1,0:T(8,128)(2,1)S(1)} %shard_map.160.refs_0_), channel_id=1, source_target_pairs={{1,0},{0,1},{3,2},{2,3},{5,4},{4,5},{7,6},{6,7},{9,8},{8,9},{11,10... | collective-permute-start | bytes 49160 | tf_op jit(solution)/shard_map/ppermute | solution.py:331
  140.6 8.6 %collective-permute-start.4 = (bf16[64,128]{1,0:T(8,128)(2,1)S(1)}, bf16[64,128]{1,0:T(8,128)(2,1)S(1)}, u32[]{:S(2)}, u32[]{:S(2)}) collective-permute-start(bf16[64,128]{1,0:T(8,128)(2,1)S(1)} %shard_map.160.refs_0_), channel_id=1, source_target_pairs={{2,0},{3,1},{0,2},{1,3},{6,4},{7,5},{4,6},{5,7},{10,8},{11,9},{8,1... | collective-permute-start | bytes 49160 | tf_op jit(solution)/shard_map/ppermute | solution.py:330
  144.2 6.8 %collective-permute-start.5 = (bf16[64,128]{1,0:T(8,128)(2,1)S(1)}, bf16[64,128]{1,0:T(8,128)(2,1)S(1)}, u32[]{:S(2)}, u32[]{:S(2)}) collective-permute-start(bf16[64,128]{1,0:T(8,128)(2,1)S(1)} %shard_map.160.refs_0_), channel_id=1, source_target_pairs={{3,0},{2,1},{1,2},{0,3},{7,4},{6,5},{5,6},{4,7},{11,8},{10,9},{9,1... | collective-permute-start | bytes 49160 | tf_op jit(solution)/shard_map/ppermute | solution.py:330

commit v12 on v10

--- a/solution.py
+++ b/solution.py
@@ -15,6 +15,7 @@
 SLOTS = EXPERTS * CAP
 ROWS = SLOTS // 2
 MSG = 144
+PAIR = 272
 WIDTH = 4
 
 epsilon = 1e-06
@@ -156,6 +157,14 @@
     out_ref[...] = nn(jnp.concatenate(rows, axis=0), w_ref[...]).astype(bf16)
 
 
+def trim_body(x_ref, out_ref):
+    for b in range(2):
+        out_ref[b * BLOCK : (b + 1) * BLOCK, :] = x_ref[b * MSG : b * MSG + BLOCK, :]
+    bias = [x_ref[b * MSG + BLOCK : (b + 1) * MSG, :] for b in range(2)]
+    first = iota((16, BLOCK), 0) < 8
+    out_ref[2 * BLOCK : PAIR, :] = jnp.where(first, bias[0], bias[1])
+
+
 def order_body(pos_ref, own_ref, other_ref, out_ref):
     core = pos_ref[0] % 2
     own, other = own_ref[...], other_ref[...]
@@ -168,7 +177,7 @@
     here = pos_ref[0]
     core = here % 2
     rows = far_ref.shape[0]
-    chips = 2 * rows // MSG
+    chips = 4 * rows // PAIR
     odd = (here // 2) % 2
     q = q_ref[...]
     wide = (2 * BLOCK, 2 * BLOCK)
@@ -181,18 +190,25 @@
 
     def step(k, carry):
         later, total = carry
-        messages, starts = [], []
+        messages, biases, starts = [], [], []
         for w in range(WIDTH):
             z = chips - 1 - (k * WIDTH + w)
-            at = pl.multiple_of((z // 2) * MSG, 16)
+            base = (z // 4) * PAIR
+            which = (WIDTH - 1 - w) // 2
             near = odd == (WIDTH - 1 - w) % 2
-            far, other = far_ref[pl.ds(at, MSG), :], far_other_ref[pl.ds(at, MSG), :]
-            upper = jnp.where(core == 1, far, other)
-            lower = jnp.where(core == 1, other, far)
-            messages.append(jnp.where(near, near_ref[pl.ds(at, MSG), :], upper))
-            messages.append(jnp.where(near, near_ref[pl.ds(rows + at, MSG), :], lower))
+
+            def piece(at, size):
+                at = pl.multiple_of(base + at, 16)
+                far, other = far_ref[pl.ds(at, size), :], far_other_ref[pl.ds(at, size), :]
+                upper = jnp.where(core == 1, far, other)
+                lower = jnp.where(core == 1, other, far)
+                upper = jnp.where(near, near_ref[pl.ds(at, size), :], upper)
+                return upper, jnp.where(near, near_ref[pl.ds(rows + at, size), :], lower)
+
+            messages += piece(which * BLOCK, BLOCK)
+            biases += [x[which * 8 : which * 8 + 1, :] for x in piece(2 * BLOCK, 16)]
             starts += [(here - 2 * z - 1) * BLOCK, (here - 2 * z) * BLOCK]
-        scores = [nn(q, m[0:HEAD, :]) + m[BLOCK : BLOCK + 1, :].astype(f32) for m in messages]
+        scores = [nn(q, m[0:HEAD, :]) + x.astype(f32) for m, x in zip(messages, biases)]
         causal = [offset < start for start in starts]
         logs = [jnp.log(1.0 + jnp.exp(-jnp.abs(x))) for x in scores]
         keep = [-(jnp.maximum(x, 0.0) + y) for x, y in zip(scores, logs)]
@@ -310,6 +326,7 @@
     other_gate = lax.ppermute(gate_weight[0], "tp", swaps)
     other_up = lax.ppermute(up_weight[0], "tp", swaps)
     keys = lax.all_gather(message, "ep", axis=0, tiled=True, axis_index_groups=pairs)
+    keys = call(trim_body, 0, 1, struct((PAIR, BLOCK), bf16), 1 << 20)(keys)
     own = lax.all_gather(keys, "ep", axis=0, tiled=True, axis_index_groups=strided)
     far = lax.ppermute(own, "ep", [(e, e ^ 2) for e in range(ep)])
     routed = call_out(halves_body, 0, 1, struct((tp, ROWS, BLOCK), bf16), 1 << 24, [], tp)(routed)

time: 168 us -> 164 us (0.976)
  waiting for transfers between devices: 34.7 us -> 31.7 us
    ppermute x1, waiting for transfers between devices: 4.7 us -> 0.01 us  [shards(): far = lax.ppermute(own, 'ep', [(e, e ^ 2) for e in range(ep)])]
    pallas_call x11 -> x12, Pallas kernels: 14.5 us -> 13.4 us  [run(): return kernel(*args)]
where the time goes in v12:
time: 164 us; the launch traced here: 162 us
  blocking collectives  70.6 us (43%)
  starting transfers between devices  45.3 us (28%)
  waiting for transfers between devices  31.7 us (19%)
  Pallas kernels  13.4 us (8%)
    all_to_all x1, blocking collectives, exchange(): return lax.all_to_all(x, axis, split_axis=0, concat_axis=0, tiled=True)  32.5 us
    all_to_all x3, starting transfers between devices, exchange(): return lax.all_to_all(x, axis, split_axis=0, concat_axis=0, tiled=True)  22.3 us
    all_gather x1, blocking collectives, shards(): lax.all_gather(keys, 'ep', axis=0, tiled=True, axis_index_groups=strided)  20.2 us
    ppermute x1, waiting for transfers between devices, shards(): other_gate = lax.ppermute(gate_weight[0], 'tp', swaps)  19.2 us
    pallas_call x12, Pallas kernels, run(): return kernel(*args)  13.4 us
    all_gather x1, blocking collectives, shards(): lax.all_gather(attended, 'tp', axis=0, tiled=True, axis_index_groups=alon...  12.4 us
    ppermute x3, starting transfers between devices, shards(): heads.append(lax.ppermute(attended, 'tp', [(k ^ d, k) for k in range(tp)]))  10.4 us
    ppermute x1, waiting for transfers between devices, shards(): other_up = lax.ppermute(up_weight[0], 'tp', swaps)  8.97 us
  transfers between devices with their start and end apart: 11, of which 4 were waited for; matrix products, arithmetic and copies ran while one was open for 0% of the time, Pallas kernels for 5%

profile of v12, /device:TPU:6, one launch (start us, length us, event | category | flops | bytes accessed | tf_op | source)
XLA Modules:
  0.0 161.9 jit_solution(9962431532086033271)
XLA Ops:
  0.7 1.5 shard_map.165
  2.2 32.5 %all_to_all.20 = bf16[32,16,128]{2,1,0:T(8,128)(2,1)S(1)} all-to-all(bf16[32,16,128]{2,1,0:T(8,128)(2,1)S(1)} %bitcast.18), channel_id=1, replica_groups=mesh['ep'=32,'tp'=16] {'ep'}, dimensions={0} | all-to-all | bytes 262144 | tf_op jit(solution)/shard_map/all_to_all | solution.py:304
  34.6 1.1 shard_map.166
  35.8 7.4 %all-to-all-start.1 = ((bf16[16,256,128]{2,1,0:T(8,128)(2,1)}), bf16[16,256,128]{2,1,0:T(8,128)(2,1)S(1)}, u32[]{:S(2)}, u32[]{:S(2)}) async-start(bf16[16,256,128]{2,1,0:T(8,128)(2,1)} %shard_map.166), calls=%async_computation.1 | async-start | bytes 2097152 | tf_op jit(solution)/shard_map/all_to_all | solution.py:304
  43.2 2.8 %collective-permute-start.6 = (bf16[2048,128]{1,0:T(8,128)(2,1)S(1)}, bf16[2048,128]{1,0:T(8,128)(2,1)S(1)}, u32[]{:S(2)}, u32[]{:S(2)}) collective-permute-start(bf16[2048,128]{1,0:T(8,128)(2,1)S(1)} %bitcast.20), channel_id=1, source_target_pairs={{0,1},{1,0},{2,3},{3,2},{4,5},{5,4},{6,7},{7,6},{8,9},{9,8},{10,11... | collective-permute-start | bytes 1572872 | tf_op jit(solution)/shard_map/ppermute | solution.py:326
  46.0 3.1 %collective-permute-start.7 = (bf16[2048,128]{1,0:T(8,128)(2,1)S(1)}, bf16[2048,128]{1,0:T(8,128)(2,1)S(1)}, u32[]{:S(2)}, u32[]{:S(2)}) collective-permute-start(bf16[2048,128]{1,0:T(8,128)(2,1)S(1)} %bitcast.22), channel_id=1, source_target_pairs={{0,1},{1,0},{2,3},{3,2},{4,5},{5,4},{6,7},{7,6},{8,9},{9,8},{10,11... | collective-permute-start | bytes 1572872 | tf_op jit(solution)/shard_map/ppermute | solution.py:327
  49.1 19.2 %collective-permute-done.6.g1_ref = bf16[2048,128]{1,0:T(8,128)(2,1)S(1)} collective-permute-done((bf16[2048,128]{1,0:T(8,128)(2,1)S(1)}, bf16[2048,128]{1,0:T(8,128)(2,1)S(1)}, u32[]{:S(2)}, u32[]{:S(2)}) %collective-permute-start.6) | collective-permute-done | bytes 524320 | tf_op jit(solution)/shard_map/ppermute | solution.py:326
  68.3 9.0 %collective-permute-done.7.u1_ref = bf16[2048,128]{1,0:T(8,128)(2,1)S(1)} collective-permute-done((bf16[2048,128]{1,0:T(8,128)(2,1)S(1)}, bf16[2048,128]{1,0:T(8,128)(2,1)S(1)}, u32[]{:S(2)}, u32[]{:S(2)}) %collective-permute-start.7) | collective-permute-done | bytes 524320 | tf_op jit(solution)/shard_map/ppermute | solution.py:327
  77.3 2.2 %shard_map.167 = bf16[16,512,128]{2,1,0:T(8,128)(2,1)} custom-call(s32[1]{0:T(128)} %bitcast.tp_ref, bf16[16,256,128]{2,1,0:T(8,128)(2,1)S(1)} %all-to-all-done.1.x_ref, bf16[2048,128]{1,0:T(8,128)(2,1)S(1)} %bitcast.21, bf16[2048,128]{1,0:T(8,128)(2,1)S(1)} %bitcast.23, bf16[2048,128]{1,0:T(8,128)(2,1)S(1)} %collective-permute-done.6.g1_ref, ...), custom_call_target="tpu_custom_call" | custom-call | flops 536870912 | bytes 1048576 | tf_op jit(solution)/shard_map/pallas_call | solution.py:35
  79.5 7.7 %all-to-all-start.2 = ((bf16[16,512,128]{2,1,0:T(8,128)(2,1)}), bf16[16,512,128]{2,1,0:T(8,128)(2,1)S(1)}, u32[]{:S(2)}, u32[]{:S(2)}) async-start(bf16[16,512,128]{2,1,0:T(8,128)(2,1)} %shard_map.167), calls=%async_computation.2 | async-start | bytes 4194304 | tf_op jit(solution)/shard_map/all_to_all | solution.py:304
  87.1 1.9 %shard_map.158 = (bf16[128,64]{1,0:T(8,128)(2,1)S(1)}, bf16[144,128]{1,0:T(8,128)(2,1)S(1)}) custom-call(bf16[128,2048]{1,0:T(8,128)(2,1)} %rows_ref.2, f32[1,2048]{1,0:T(1,128)} %bitcast.33, bf16[64,2048]{1,0:T(8,128)(2,1)} %bitcast.29, bf16[64,2048]{1,0:T(8,128)(2,1)} %bitcast.30, bf16[64,2048]{1,0:T(8,128)(2,1)} %bitcast.31, bf16[1,128]{1,0:T(2,128)(2,1)} %bias_ref.1), custom_call_target="tpu_custom_call" | custom-call | flops 268435456 | bytes 1048576 | tf_op jit(solution)/shard_map/pallas_call | solution.py:35
  89.0 5.6 %all_gather.9.x_ref = bf16[288,128]{1,0:T(8,128)(2,1)S(1)} all-gather(bf16[144,128]{1,0:T(8,128)(2,1)S(1)} %get-tuple-element.7), channel_id=1, replica_groups={{0,64},{16,80},{32,96},{48,112},{128,192},{144,208},{160,224},{176,240}..., dimensions={0}, use_global_device_ids=true | all-gather | bytes 110592 | tf_op jit(solution)/shard_map/all_gather | solution.py:328
  94.6 20.2 %all_gather.10.own_ref = bf16[1088,128]{1,0:T(8,128)(2,1)S(1)} all-gather(bf16[272,128]{1,0:T(8,128)(2,1)S(1)} %shard_map.159), channel_id=1, replica_groups={{0,128,256,384},{16,144,272,400},{32,160,288,416},{48,176,304,432},{64,..., dimensions={0}, use_global_device_ids=true | all-gather | bytes 348160 | tf_op jit(solution)/shard_map/all_gather | solution.py:330
  114.8 2.4 %collective-permute-start.1 = (bf16[1088,128]{1,0:T(8,128)(2,1)S(1)}, bf16[1088,128]{1,0:T(8,128)(2,1)S(1)}, u32[]{:S(2)}, u32[]{:S(2)}) collective-permute-start(bf16[1088,128]{1,0:T(8,128)(2,1)S(1)} %all_gather.10.own_ref), channel_id=1, source_target_pairs={{0,32},{16,48},{32,0},{48,16},{64,96},{80,112},{96,64},{112,80},{1... | collective-permute-start | bytes 835592 | tf_op jit(solution)/shard_map/ppermute | solution.py:331
  117.2 1.4 shard_map.168
  118.6 7.2 %all-to-all-start.3 = ((bf16[32,16,128]{2,1,0:T(8,128)(2,1)}), bf16[32,16,128]{2,1,0:T(8,128)(2,1)S(1)}, u32[]{:S(2)}, u32[]{:S(2)}) async-start(bf16[32,16,128]{2,1,0:T(8,128)(2,1)} %bitcast.15), calls=%async_computation.3 | async-start | bytes 262144 | tf_op jit(solution)/shard_map/all_to_all | solution.py:304
  125.8 2.2 %collective-permute-start = (bf16[1088,128]{1,0:T(8,128)(2,1)S(1)}, bf16[1088,128]{1,0:T(8,128)(2,1)S(1)}, u32[]{:S(2)}, u32[]{:S(2)}) collective-permute-start(bf16[1088,128]{1,0:T(8,128)(2,1)S(1)} %all_gather.10.own_ref), channel_id=1, source_target_pairs={{0,16},{16,0},{32,48},{48,32},{64,80},{80,64},{96,112},{112,96},{1... | collective-permute-start | bytes 835592 | tf_op jit(solution)/shard_map/ppermute | solution.py:340
  128.0 2.1 %collective-permute-start.2 = (bf16[1088,128]{1,0:T(8,128)(2,1)S(1)}, bf16[1088,128]{1,0:T(8,128)(2,1)S(1)}, u32[]{:S(2)}, u32[]{:S(2)}) collective-permute-start(bf16[1088,128]{1,0:T(8,128)(2,1)S(1)} %collective-permute-done.1.far_ref), channel_id=1, source_target_pairs={{0,16},{16,0},{32,48},{48,32},{64,80},{80,64},{96,112},{112,96},{1... | collective-permute-start | bytes 835592 | tf_op jit(solution)/shard_map/ppermute | solution.py:343
  131.4 3.1 %shard_map.161.refs_0_ = bf16[64,128]{1,0:T(8,128)(2,1)S(1)} custom-call(s32[1]{0:T(128)} %bitcast.1.pos_ref, bf16[128,64]{1,0:T(8,128)(2,1)S(1)} %get-tuple-element.6.q_ref, bf16[2176,128]{1,0:T(8,128)(2,1)S(1)} %shard_map.160.near_ref, bf16[1088,128]{1,0:T(8,128)(2,1)S(1)} %collective-permute-done.1.far_ref, ...), custom_call_target="tpu_custom_call" | custom-call | flops 1073741824 | bytes 1048576 | tf_op jit(solution)/shard_map/pallas_call | solution.py:35
  134.5 2.7 %collective-permute-start.3 = (bf16[64,128]{1,0:T(8,128)(2,1)S(1)}, bf16[64,128]{1,0:T(8,128)(2,1)S(1)}, u32[]{:S(2)}, u32[]{:S(2)}) collective-permute-start(bf16[64,128]{1,0:T(8,128)(2,1)S(1)} %shard_map.161.refs_0_), channel_id=1, source_target_pairs={{1,0},{0,1},{3,2},{2,3},{5,4},{4,5},{7,6},{6,7},{9,8},{8,9},{11,10... | collective-permute-start | bytes 49160 | tf_op jit(solution)/shard_map/ppermute | solution.py:349
  137.2 3.7 %collective-permute-start.4 = (bf16[64,128]{1,0:T(8,128)(2,1)S(1)}, bf16[64,128]{1,0:T(8,128)(2,1)S(1)}, u32[]{:S(2)}, u32[]{:S(2)}) collective-permute-start(bf16[64,128]{1,0:T(8,128)(2,1)S(1)} %shard_map.161.refs_0_), channel_id=1, source_target_pairs={{2,0},{3,1},{0,2},{1,3},{6,4},{7,5},{4,6},{5,7},{10,8},{11,9},{8,1... | collective-permute-start | bytes 49160 | tf_op jit(solution)/shard_map/ppermute | solution.py:349
  140.9 4.0 %collective-permute-start.5 = (bf16[64,128]{1,0:T(8,128)(2,1)S(1)}, bf16[64,128]{1,0:T(8,128)(2,1)S(1)}, u32[]{:S(2)}, u32[]{:S(2)}) collective-permute-start(bf16[64,128]{1,0:T(8,128)(2,1)S(1)} %shard_map.161.refs_0_), channel_id=1, source_target_pairs={{3,0},{2,1},{1,2},{0,3},{7,4},{6,5},{5,6},{4,7},{11,8},{10,9},{9,1... | collective-permute-start | bytes 49160 | tf_op jit(solution)/shard_map/ppermute | solution.py:349
  145.4 2.4 %collective-permute-done.5.refs_3_ = bf16[64,128]{1,0:T(8,128)(2,1)S(1)} collective-permute-done((bf16[64,128]{1,0:T(8,128)(2,1)S(1)}, bf16[64,128]{1,0:T(8,128)(2,1)S(1)}, u32[]{:S(2)}, u32[]{:S(2)}) %collective-permute-start.5) | collective-permute-done | bytes 16416 | tf_op jit(solution)/shard_map/ppermute | solution.py:349
  147.8 12.4 %all_gather.11.x_ref = bf16[1024,128]{1,0:T(8,128)(2,1)S(1)} all-gather(bf16[256,128]{1,0:T(8,128)(2,1)S(1)} %shard_map.162), channel_id=1, replica_groups={{0,4,8,12},{1,5,9,13},{2,6,10,14},{3,7,11,15},{16,20,24,28},{17,21,25,2..., dimensions={0}, use_global_device_ids=true | all-gather | bytes 327680 | tf_op jit(solution)/shard_map/all_gather | solution.py:356
  (28 shorter events, 3.4 us)
Async XLA Ops:
  0.6 42.6 %copy-start.1 = (bf16[1,2048,128]{2,1,0:T(8,128)(2,1)S(1)}, bf16[1,2048,128]{2,1,0:T(8,128)(2,1)}, u32[]{:S(2)}) copy-start(bf16[1,2048,128]{2,1,0:T(8,128)(2,1)} %param.27) | copy-start | bytes 1572868
  0.6 45.4 %copy-start.2 = (bf16[1,2048,128]{2,1,0:T(8,128)(2,1)S(1)}, bf16[1,2048,128]{2,1,0:T(8,128)(2,1)}, u32[]{:S(2)}) copy-start(bf16[1,2048,128]{2,1,0:T(8,128)(2,1)} %param.28) | copy-start | bytes 1572868
  35.8 41.5 %all-to-all-start.1 = ((bf16[16,256,128]{2,1,0:T(8,128)(2,1)}), bf16[16,256,128]{2,1,0:T(8,128)(2,1)S(1)}, u32[]{:S(2)}, u32[]{:S(2)}) async-start(bf16[16,256,128]{2,1,0:T(8,128)(2,1)} %shard_map.166), calls=%async_computation.1 | async-start | bytes 2097152 | tf_op jit(solution)/shard_map/all_to_all | solution.py:304
  43.2 25.1 %collective-permute-start.6 = (bf16[2048,128]{1,0:T(8,128)(2,1)S(1)}, bf16[2048,128]{1,0:T(8,128)(2,1)S(1)}, u32[]{:S(2)}, u32[]{:S(2)}) collective-permute-start(bf16[2048,128]{1,0:T(8,128)(2,1)S(1)} %bitcast.20), channel_id=1, source_target_pairs={{0,1},{1,0},{2,3},{3,2},{4,5},{5,4},{6,7},{7,6},{8,9},{9,8},{10,11... | collective-permute-start | bytes 1572872 | tf_op jit(solution)/shard_map/ppermute | solution.py:326
  46.0 31.2 %collective-permute-start.7 = (bf16[2048,128]{1,0:T(8,128)(2,1)S(1)}, bf16[2048,128]{1,0:T(8,128)(2,1)S(1)}, u32[]{:S(2)}, u32[]{:S(2)}) collective-permute-start(bf16[2048,128]{1,0:T(8,128)(2,1)S(1)} %bitcast.22), channel_id=1, source_target_pairs={{0,1},{1,0},{2,3},{3,2},{4,5},{5,4},{6,7},{7,6},{8,9},{9,8},{10,11... | collective-permute-start | bytes 1572872 | tf_op jit(solution)/shard_map/ppermute | solution.py:327
  79.4 37.8 %copy-start = (bf16[1,2048,128]{2,1,0:T(8,128)(2,1)S(1)}, bf16[1,2048,128]{2,1,0:T(8,128)(2,1)}, u32[]{:S(2)}) copy-start(bf16[1,2048,128]{2,1,0:T(8,128)(2,1)} %param.29) | copy-start | bytes 1572868
  79.5 37.7 %all-to-all-start.2 = ((bf16[16,512,128]{2,1,0:T(8,128)(2,1)}), bf16[16,512,128]{2,1,0:T(8,128)(2,1)S(1)}, u32[]{:S(2)}, u32[]{:S(2)}) async-start(bf16[16,512,128]{2,1,0:T(8,128)(2,1)} %shard_map.167), calls=%async_computation.2 | async-start | bytes 4194304 | tf_op jit(solution)/shard_map/all_to_all | solution.py:304
  114.8 13.2 %collective-permute-start.1 = (bf16[1088,128]{1,0:T(8,128)(2,1)S(1)}, bf16[1088,128]{1,0:T(8,128)(2,1)S(1)}, u32[]{:S(2)}, u32[]{:S(2)}) collective-permute-start(bf16[1088,128]{1,0:T(8,128)(2,1)S(1)} %all_gather.10.own_ref), channel_id=1, source_target_pairs={{0,32},{16,48},{32,0},{48,16},{64,96},{80,112},{96,64},{112,80},{1... | collective-permute-start | bytes 835592 | tf_op jit(solution)/shard_map/ppermute | solution.py:331
  118.6 42.5 %all-to-all-start.3 = ((bf16[32,16,128]{2,1,0:T(8,128)(2,1)}), bf16[32,16,128]{2,1,0:T(8,128)(2,1)S(1)}, u32[]{:S(2)}, u32[]{:S(2)}) async-start(bf16[32,16,128]{2,1,0:T(8,128)(2,1)} %bitcast.15), calls=%async_computation.3 | async-start | bytes 262144 | tf_op jit(solution)/shard_map/all_to_all | solution.py:304
  125.8 4.4 %collective-permute-start = (bf16[1088,128]{1,0:T(8,128)(2,1)S(1)}, bf16[1088,128]{1,0:T(8,128)(2,1)S(1)}, u32[]{:S(2)}, u32[]{:S(2)}) collective-permute-start(bf16[1088,128]{1,0:T(8,128)(2,1)S(1)} %all_gather.10.own_ref), channel_id=1, source_target_pairs={{0,16},{16,0},{32,48},{48,32},{64,80},{80,64},{96,112},{112,96},{1... | collective-permute-start | bytes 835592 | tf_op jit(solution)/shard_map/ppermute | solution.py:340
  128.0 3.5 %collective-permute-start.2 = (bf16[1088,128]{1,0:T(8,128)(2,1)S(1)}, bf16[1088,128]{1,0:T(8,128)(2,1)S(1)}, u32[]{:S(2)}, u32[]{:S(2)}) collective-permute-start(bf16[1088,128]{1,0:T(8,128)(2,1)S(1)} %collective-permute-done.1.far_ref), channel_id=1, source_target_pairs={{0,16},{16,0},{32,48},{48,32},{64,80},{80,64},{96,112},{112,96},{1... | collective-permute-start | bytes 835592 | tf_op jit(solution)/shard_map/ppermute | solution.py:343
  130.2 14.7 %copy-start.4 = (s32[128,2]{0,1:T(2,128)S(1)}, s32[128,2]{0,1:T(2,128)}, u32[]{:S(2)}) copy-start(s32[128,2]{0,1:T(2,128)} %param.24) | copy-start | bytes 3076
  130.3 14.7 %copy-start.5 = (f32[128,4]{0,1:T(4,128)S(1)}, f32[128,4]{0,1:T(4,128)}, u32[]{:S(2)}) copy-start(f32[128,4]{0,1:T(4,128)} %param.25) | copy-start | bytes 6148
  130.3 14.7 %copy-start.6 = (f32[128,2]{0,1:T(2,128)S(1)}, f32[128,2]{0,1:T(2,128)}, u32[]{:S(2)}) copy-start(f32[128,2]{0,1:T(2,128)} %param.26) | copy-start | bytes 3076
  131.4 28.7 %copy-start.3 = (bf16[1024,128]{1,0:T(8,128)(2,1)S(1)}, bf16[1024,128]{1,0:T(8,128)(2,1)}, u32[]{:S(2)}) copy-start(bf16[1024,128]{1,0:T(8,128)(2,1)} %w_ref.1) | copy-start | bytes 786436
  134.5 10.9 %collective-permute-start.3 = (bf16[64,128]{1,0:T(8,128)(2,1)S(1)}, bf16[64,128]{1,0:T(8,128)(2,1)S(1)}, u32[]{:S(2)}, u32[]{:S(2)}) collective-permute-start(bf16[64,128]{1,0:T(8,128)(2,1)S(1)} %shard_map.161.refs_0_), channel_id=1, source_target_pairs={{1,0},{0,1},{3,2},{2,3},{5,4},{4,5},{7,6},{6,7},{9,8},{8,9},{11,10... | collective-permute-start | bytes 49160 | tf_op jit(solution)/shard_map/ppermute | solution.py:349
  137.2 8.2 %collective-permute-start.4 = (bf16[64,128]{1,0:T(8,128)(2,1)S(1)}, bf16[64,128]{1,0:T(8,128)(2,1)S(1)}, u32[]{:S(2)}, u32[]{:S(2)}) collective-permute-start(bf16[64,128]{1,0:T(8,128)(2,1)S(1)} %shard_map.161.refs_0_), channel_id=1, source_target_pairs={{2,0},{3,1},{0,2},{1,3},{6,4},{7,5},{4,6},{5,7},{10,8},{11,9},{8,1... | collective-permute-start | bytes 49160 | tf_op jit(solution)/shard_map/ppermute | solution.py:349
  140.9 6.8 %collective-permute-start.5 = (bf16[64,128]{1,0:T(8,128)(2,1)S(1)}, bf16[64,128]{1,0:T(8,128)(2,1)S(1)}, u32[]{:S(2)}, u32[]{:S(2)}) collective-permute-start(bf16[64,128]{1,0:T(8,128)(2,1)S(1)} %shard_map.161.refs_0_), channel_id=1, source_target_pairs={{3,0},{2,1},{1,2},{0,3},{7,4},{6,5},{5,6},{4,7},{11,8},{10,9},{9,1... | collective-permute-start | bytes 49160 | tf_op jit(solution)/shard_map/ppermute | solution.py:349
